TPU v7x, 768 devices: a whole 4x8x12 slice. The times are simulated.
768 devices in a mesh: ep: 48 (over z, x), tp: 16 (over y, core).
Axes of the slice: x: 4, y: 8, z: 12, core: 2. Of those that a mesh axis runs over, the one named last changes fastest.
Arguments:
- stream: bfloat16 [960, 2048], P('ep'), may hold values from -8 to 8
- norm_gain_mix: bfloat16 [2048], replicated, may hold values from 0.099609375 to 1.8984375
- query_weight: bfloat16 [1024, 2048], P('tp'), may hold values from -0.125 to 0.125
- key_weight: bfloat16 [1024, 2048], P('tp'), may hold values from -0.125 to 0.125
- value_weight: bfloat16 [1024, 2048], P('tp'), may hold values from -0.125 to 0.125
- score_offset: float32 [16], P('tp'), may hold values from -9 to -3
- cache_keys: bfloat16 [960, 1024, 256], P('ep', 'tp'), may hold values from -6 to 6
- cache_values: bfloat16 [960, 1024, 256], P('ep', 'tp'), may hold values from -6 to 6
- lengths: int32 [960], P('ep'), may hold values from 32 to 256, as said below
- out_weight: bfloat16 [1024, 2048], P('tp'), may hold values from -0.75 to 0.75
- norm_gain_ffn: bfloat16 [2048], replicated, may hold values from 0.099609375 to 1.8984375
- group_weight: bfloat16 [2048, 4], replicated, may hold values from -0.25 to 0.25
- router_weight: bfloat16 [2048, 48], replicated, may hold values from -0.25 to 0.25
- routing: int32 [960, 2], P('ep'), may hold values from 0 to 47, as said below
- expert_gate: bfloat16 [48, 2048, 4096], P('ep', None, 'tp'), may hold values from -0.125 to 0.125
- expert_up: bfloat16 [48, 2048, 4096], P('ep', None, 'tp'), may hold values from -0.125 to 0.125
- expert_down: bfloat16 [48, 4096, 2048], P('ep', 'tp'), may hold values from -0.1875 to 0.1875
- branch_gate: bfloat16 [2048], replicated, may hold values from -0.25 to 0.25
- dense_gate: bfloat16 [2048, 6144], P('tp', 'ep'), may hold values from -0.125 to 0.125
- dense_up: bfloat16 [2048, 6144], P('tp', 'ep'), may hold values from -0.125 to 0.125
- dense_down: bfloat16 [6144, 2048], P('ep', 'tp'), may hold values from -0.15625 to 0.15625
Outputs:
- mixed: bfloat16 [960, 2048], P('ep', 'tp')
- fresh_keys: bfloat16 [960, 1024], P('ep', 'tp')
- fresh_values: bfloat16 [960, 1024], P('ep', 'tp')
Inputs may be any that keep to these rules, and one draw needn't show every extreme that they name: `routing`: each aligned block of 20 rows (the sequences of one index of ep) names no expert more than 2 times, and some expert exactly 2 times; a row's two experts differ and lie in the same group of 12 consecutive experts. `lengths`: in every aligned block of 20 sequences one sequence has all 256 positions filled.
All inputs are finite; a program needn't handle non-finite values.
Results may differ from a plain program's by a relative error of at most 0.02.
Values may be sent and summed in bfloat16 or wider, within the bound.
No kernel may reach another device: no remote copies, remote signals or barrier semaphores. Data moves between devices by JAX's collectives and lax.ppermute only.
A program may use at most 64 MiB of HBM per device.

v0:
```python
import jax
import jax.numpy as jnp
from jax import lax
from jax.sharding import PartitionSpec as P

epsilon = 1e-06


def cut_along(array, dim, length):
    shape = array.shape
    tiles = array.reshape(*shape[:dim], length, shape[dim] // length, *shape[dim + 1 :])
    return jnp.moveaxis(tiles, dim, 0)


def sum_at_owner(array, axis, dim):
    length = lax.axis_size(axis)
    tiles = lax.all_to_all(cut_along(array, dim, length), axis, 0, 0, tiled=True)
    return jnp.sum(tiles.astype(jnp.float32), axis=0)


def from_everyone(array, axis):
    length = lax.axis_size(axis)
    return lax.all_to_all(
        jnp.broadcast_to(array[None], (length, *array.shape)), axis, 0, 0, tiled=True
    )


def of_everyone(array, axis):
    return from_everyone(array, axis).sum(axis=0)


def together(arrays, axis):
    ends = [0]
    for a in arrays:
        ends.append(ends[-1] + a.size)
    so_far = of_everyone(jnp.concatenate([a.ravel() for a in arrays]), axis)
    return tuple((so_far[b:e].reshape(a.shape) for a, b, e in zip(arrays, ends, ends[1:])))


def in_order(tiles, dim):
    shape = list(tiles.shape[1:])
    shape[dim] *= tiles.shape[0]
    return jnp.moveaxis(tiles, 0, dim).reshape(shape)


def gather_directly(array, axis, dim):
    tiles = from_everyone(array, axis)
    return in_order(tiles, dim)


def total_of_pieces(array, axis):
    tiles = lax.all_gather(array, axis).astype(jnp.float32)
    return tiles.sum(axis=0)


def sent_and_summed(array, axis, dim):
    tiles = cut_along(array, dim, lax.axis_size(axis))
    arrived = lax.all_to_all(tiles, axis, split_axis=0, concat_axis=0, tiled=True)
    return arrived.sum(axis=0)


def project_rows(normed, weight):
    return lax.dot_general(
        normed, weight, (((1,), (1,)), ((), ())), preferred_element_type=jnp.float32
    )


def stick_weights(scores, inside):
    log_keep = jnp.where(inside, jax.nn.log_sigmoid(-scores), 0.0)
    remain = lax.cumsum(log_keep, axis=2, reverse=True) - log_keep
    return jnp.where(inside, jnp.exp(jax.nn.log_sigmoid(scores) + remain), 0.0)


def local(
    stream,
    norm_gain_mix,
    query_weight,
    key_weight,
    value_weight,
    score_offset,
    cache_keys,
    cache_values,
    lengths,
    out_weight,
    norm_gain_ffn,
    group_weight,
    router_weight,
    routing,
    expert_gate,
    expert_up,
    expert_down,
    branch_gate,
    dense_gate,
    dense_up,
    dense_down,
):
    seq_count = stream.shape[0]
    width = stream.shape[1]
    tp_rank = lax.axis_index("tp")
    feat = width // lax.axis_size("tp")
    offset = tp_rank * feat
    stream_f = stream.astype(jnp.float32)
    inverse = lax.rsqrt(jnp.mean(stream_f * stream_f, -1, keepdims=True) + epsilon)
    normed = (stream_f * inverse * norm_gain_mix.astype(jnp.float32)).astype(jnp.bfloat16)
    queries = project_rows(normed, query_weight).astype(jnp.bfloat16)
    fresh_keys = project_rows(normed, key_weight).astype(jnp.bfloat16)
    fresh_values = project_rows(normed, value_weight).astype(jnp.bfloat16)
    head_count = score_offset.shape[0]
    head_size = queries.shape[1] // head_count
    cache_len = cache_keys.shape[2]
    query_h = queries.reshape(seq_count, head_count, head_size)
    key_h = cache_keys.reshape(seq_count, head_count, head_size, cache_len)
    value_h = cache_values.reshape(seq_count, head_count, head_size, cache_len)
    scores = jnp.einsum("shd,shdl->shl", query_h, key_h, preferred_element_type=jnp.float32)
    scores = scores * head_size ** (-0.5) + score_offset[None, :, None]
    inside = lax.broadcasted_iota(jnp.int32, (1, 1, cache_len), 2) < lengths[:, None, None]
    weights = stick_weights(scores, inside).astype(jnp.bfloat16)
    heads_out = jnp.einsum("shl,shdl->shd", weights, value_h, preferred_element_type=jnp.float32)
    heads_out = heads_out.astype(jnp.bfloat16).reshape(seq_count, head_count * head_size)
    partial_value = jnp.dot(heads_out, out_weight, preferred_element_type=jnp.float32)
    gain_ffn = norm_gain_ffn.astype(jnp.float32)
    attn = sum_at_owner(partial_value.astype(jnp.bfloat16), "tp", 1).astype(jnp.bfloat16)
    residual = (
        lax.dynamic_slice_in_dim(stream_f, offset, feat, 1) + attn.astype(jnp.float32)
    ).astype(jnp.bfloat16)
    residual_own = residual.astype(jnp.float32)
    group_rows = lax.dynamic_slice_in_dim(group_weight, offset, feat, 0)
    router_rows = lax.dynamic_slice_in_dim(router_weight, offset, feat, 0)
    gate_rows = lax.dynamic_slice_in_dim(branch_gate, offset, feat, 0)
    squares, group_part, expert_part, gate_part = together(
        (
            jnp.sum(residual_own * residual_own, -1),
            jnp.dot(residual, group_rows, preferred_element_type=jnp.float32),
            jnp.dot(residual, router_rows, preferred_element_type=jnp.float32),
            jnp.dot(residual, gate_rows, preferred_element_type=jnp.float32),
        ),
        "tp",
    )
    inverse_two = lax.rsqrt(squares / width + epsilon)
    gain_own = lax.dynamic_slice_in_dim(gain_ffn, offset, feat, 0)
    hidden_in = (residual_own * inverse_two[:, None] * gain_own).astype(jnp.bfloat16)
    group_logits = group_part * inverse_two[:, None]
    expert_logits = expert_part * inverse_two[:, None]
    gate_logit = gate_part * inverse_two
    experts = router_weight.shape[1]
    groups = group_weight.shape[1]
    per_group = experts // groups
    top = routing.shape[1]
    cap = 2 * ((seq_count + experts - 1) // experts)
    group_index = routing[:, 0] // per_group
    group_exp = jnp.exp(group_logits)
    group_iota = lax.broadcasted_iota(jnp.int32, (1, groups), 1)
    own_group = jnp.sum(jnp.where(group_iota == group_index[:, None], group_exp, 0.0), 1)
    group_prob = own_group / jnp.sum(group_exp, 1)
    expert_iota = lax.broadcasted_iota(jnp.int32, (1, experts), 1)
    chosen = jnp.stack(
        [
            jnp.sum(jnp.where(expert_iota == routing[:, which : which + 1], expert_logits, 0.0), 1)
            for which in range(top)
        ],
        1,
    )
    chosen_exp = jnp.exp(chosen)
    route_gate = group_prob[:, None] * chosen_exp / jnp.sum(chosen_exp, 1, keepdims=True)
    pair_expert = routing.reshape(seq_count * top)
    onehot = (pair_expert[:, None] == expert_iota).astype(jnp.int32)
    before = jnp.cumsum(onehot, 0) - onehot
    slot = jnp.sum(before * onehot, 1)
    index = (pair_expert * cap + slot).reshape(seq_count, top)
    slot_iota = lax.broadcasted_iota(jnp.int32, (experts * cap, 1, 1), 0)
    dispatch = jnp.sum((index[None, :, :] == slot_iota).astype(jnp.int32), 2).astype(jnp.bfloat16)
    send = jnp.dot(dispatch, hidden_in, preferred_element_type=jnp.float32).astype(jnp.bfloat16)
    send = send.reshape(experts, cap, hidden_in.shape[1])

    def run_experts(block):
        sources = block.shape[0]
        count = block.shape[1]
        flat = block.reshape(sources * count, block.shape[2])
        piece = lax.all_gather(flat, "tp", axis=1, tiled=True)
        rows_gate = expert_gate[0]
        rows_up = expert_up[0]
        gate_acc = jnp.dot(piece, rows_gate, preferred_element_type=jnp.float32)
        up_acc = jnp.dot(piece, rows_up, preferred_element_type=jnp.float32)
        hidden = (jax.nn.silu(gate_acc) * up_acc).astype(jnp.bfloat16)
        terms = jnp.dot(hidden, expert_down[0], preferred_element_type=jnp.float32)
        result = sum_at_owner(terms.astype(jnp.bfloat16), "tp", 1).astype(jnp.bfloat16)
        return lax.all_to_all(
            result.reshape(sources, count, result.shape[1]),
            "ep",
            split_axis=0,
            concat_axis=0,
            tiled=True,
        )

    returned = (lambda block: run_experts(block))(
        lax.all_to_all(send, "ep", split_axis=0, concat_axis=0, tiled=True)
    )
    flat_back = returned.reshape(experts * cap, feat)
    row_iota = lax.broadcasted_iota(jnp.int32, (1, experts * cap), 1)
    moe = jnp.zeros((seq_count, feat), jnp.float32)
    for which in range(top):
        select = (index[:, which : which + 1] == row_iota).astype(jnp.bfloat16)
        moe = moe + route_gate[:, which : which + 1] * jnp.dot(
            select, flat_back, preferred_element_type=jnp.float32
        )
    units = dense_gate.shape[1]
    piece = gather_directly(hidden_in, "ep", 0)
    dense_terms = jnp.concatenate(
        [
            jnp.dot(piece, dense_gate, preferred_element_type=jnp.float32),
            jnp.dot(piece, dense_up, preferred_element_type=jnp.float32),
        ],
        1,
    )
    dense_both = total_of_pieces(dense_terms.astype(jnp.bfloat16), "tp").astype(jnp.float32)
    dense_act = (jax.nn.silu(dense_both[:, :units]) * dense_both[:, units:]).astype(jnp.bfloat16)
    dense_term = jnp.dot(dense_act, dense_down, preferred_element_type=jnp.float32)
    dense = sent_and_summed(dense_term, "ep", 0)
    mixed = (residual_own + moe + jax.nn.sigmoid(gate_logit)[:, None] * dense).astype(jnp.bfloat16)
    return (mixed, fresh_keys, fresh_values)


def solution(mesh):
    placed = (
        P("ep", None),
        P(),
        P("tp", None),
        P("tp", None),
        P("tp", None),
        P("tp"),
        P("ep", "tp", None),
        P("ep", "tp", None),
        P("ep"),
        P("tp", None),
        P(),
        P(),
        P(),
        P("ep", None),
        P("ep", None, "tp"),
        P("ep", None, "tp"),
        P("ep", "tp", None),
        P(),
        P("tp", "ep"),
        P("tp", "ep"),
        P("ep", "tp"),
    )
    return jax.shard_map(
        local,
        mesh=mesh,
        in_specs=placed,
        out_specs=(P("ep", "tp"), P("ep", "tp"), P("ep", "tp")),
        check_vma=False,
    )
```

profile of v0, /device:TPU:1, one launch (start us, length us, event | category | flops | bytes accessed | tf_op | source)
XLA Modules:
  0.0 209.9 jit_solution(14439322314260574681)
XLA Ops:
  7.2 0.8 convert_element_type.86
  8.0 1.0 multiply_reduce_fusion
  9.7 1.2 fusion.8
  11.0 1.3 fusion.42
  12.3 0.7 fusion.29
  13.0 2.5 %reduce-window.6 = f32[20,1,2,128]{3,0,1,2:T(8,128)S(1)} reduce-window(f32[20,1,2,128]{3,0,1,2:T(8,128)S(1)} %copy.64, f32[]{:T(128)} %constant.43.clone.1), window={size=1x1x1x128 pad=0_0x0_0x0_0x0_127}, to_apply=%region_1.2 | reduce-window | flops 650240 | bytes 40964 | tf_op jit(solution)/shard_map/reduce-window
  15.9 0.7 fusion.40
  16.7 1.4 fusion.32
  18.0 1.1 convolution_convert_fusion.1
  19.2 0.6 copy.107
  19.9 13.8 %all-to-all-start = ((bf16[16,20,128]{2,1,0:T(8,128)(2,1)}), bf16[16,20,128]{2,1,0:T(8,128)(2,1)S(1)}, u32[]{:S(2)}, u32[]{:S(2)}) async-start(bf16[16,20,128]{2,1,0:T(8,128)(2,1)} %bitcast.103), calls=%async_computation | async-start | bytes 196608 | tf_op jit(solution)/shard_map/all_to_all | solution.py:17
  33.6 0.9 convert_element_type.85
  34.5 7.6 %all-to-all-done = bf16[16,20,128]{2,1,0:T(8,128)(2,1)S(1)} async-done(((bf16[16,20,128]{2,1,0:T(8,128)(2,1)}), bf16[16,20,128]{2,1,0:T(8,128)(2,1)S(1)}, u32[]{:S(2)}, u32[]{:S(2)}) %all-to-all-start) | async-done | bytes 81952 | tf_op jit(solution)/shard_map/all_to_all | solution.py:17
  42.2 0.1 fusion.35
  42.3 0.8 fusion.38
  43.2 0.8 fusion.47
  44.1 0.9 convolution_bitcast_fusion
  45.1 0.7 broadcast_in_dim.14
  45.7 3.4 %all-to-all-start.1 = ((f32[16,1,1080]{2,1,0:T(1,128)}), f32[16,1,1080]{2,1,0:T(1,128)S(1)}, u32[]{:S(2)}, u32[]{:S(2)}) async-start(f32[16,1,1080]{2,1,0:T(1,128)} %broadcast_in_dim.14), calls=%async_computation.1 | async-start | bytes 147456 | tf_op jit(solution)/shard_map/all_to_all | solution.py:23
  49.2 0.8 dynamic-slice_convert_fusion
  49.9 7.0 %all-to-all-done.1 = f32[16,1,1080]{2,1,0:T(1,128)S(1)} async-done(((f32[16,1,1080]{2,1,0:T(1,128)}), f32[16,1,1080]{2,1,0:T(1,128)S(1)}, u32[]{:S(2)}, u32[]{:S(2)}) %all-to-all-start.1) | async-done | bytes 69152 | tf_op jit(solution)/shard_map/all_to_all | solution.py:23
  57.2 29.9 %all_to_all.36 = bf16[48,20,128]{2,1,0:T(8,128)(2,1)S(1)} all-to-all(bf16[48,20,128]{2,1,0:T(8,128)(2,1)S(1)} %broadcast_in_dim.19), channel_id=1, replica_groups=mesh['ep'=48,'tp'=16] {'ep'}, dimensions={0} | all-to-all | bytes 491520 | tf_op jit(solution)/shard_map/all_to_all | solution.py:23
  87.2 1.0 fusion.1
  88.2 1.0 fusion.2
  89.1 0.8 pad_maximum_fusion
  90.4 0.2 select_reduce_fusion
  91.0 0.2 convolution_convert_fusion.4
  91.1 16.7 %all_to_all.37 = bf16[48,2,128]{2,1,0:T(2,128)(2,1)S(1)} all-to-all(bf16[48,2,128]{2,1,0:T(2,128)(2,1)S(1)} %bitcast.112), channel_id=1, replica_groups=mesh['ep'=48,'tp'=16] {'ep'}, dimensions={0} | all-to-all | bytes 49152 | tf_op jit(solution)/shard_map/all_to_all | solution.py:196
  107.8 20.8 %all_gather.7 = bf16[96,2048]{1,0:T(8,128)(2,1)S(1)} all-gather(bf16[96,128]{1,0:T(8,128)(2,1)S(1)} %bitcast.111), channel_id=1, replica_groups=mesh['ep'=48,'tp'=16] {'tp'}, dimensions={1}, use_global_device_ids=true | all-gather | bytes 417792 | tf_op jit(solution)/shard_map/all_gather | solution.py:179
  128.6 1.5 fusion.12
  130.2 0.8 fusion
  131.0 0.9 copy.106
  131.8 4.4 %all-to-all-start.3 = ((bf16[16,96,128]{2,1,0:T(8,128)(2,1)}), bf16[16,96,128]{2,1,0:T(8,128)(2,1)S(1)}, u32[]{:S(2)}, u32[]{:S(2)}) async-start(bf16[16,96,128]{2,1,0:T(8,128)(2,1)} %bitcast.102), calls=%async_computation.3 | async-start | bytes 786432 | tf_op jit(solution)/shard_map/all_to_all | solution.py:17
  136.3 14.5 %all-to-all-done.3 = bf16[16,96,128]{2,1,0:T(8,128)(2,1)S(1)} async-done(((bf16[16,96,128]{2,1,0:T(8,128)(2,1)}), bf16[16,96,128]{2,1,0:T(8,128)(2,1)S(1)}, u32[]{:S(2)}, u32[]{:S(2)}) %all-to-all-start.3) | async-done | bytes 393248 | tf_op jit(solution)/shard_map/all_to_all | solution.py:17
  150.8 0.7 reduce_sum.146
  151.4 7.8 %all-to-all-start.4 = ((bf16[48,2,128]{2,1,0:T(2,128)(2,1)}), bf16[48,2,128]{2,1,0:T(2,128)(2,1)S(1)}, u32[]{:S(2)}, u32[]{:S(2)}) async-start(bf16[48,2,128]{2,1,0:T(2,128)(2,1)} %bitcast.22), calls=%async_computation.4 | async-start | bytes 49152 | tf_op jit(solution)/shard_map/all_to_all | solution.py:187
  159.2 4.4 %convert_reduce_fusion = f32[960,256]{1,0:T(8,128)S(1)} fusion(bf16[16,960,256]{2,1,0:T(8,128)(2,1)} %all-gather.2.cloned.1.call-done), kind=kLoop, calls=%fused_computation | loop fusion | flops 7618560 | bytes 8847360 | tf_op jit(solution)/shard_map/reduce_sum | solution.py:53
  163.6 0.3 fusion.15
  163.9 0.9 reshape.203
  164.8 5.4 %all-to-all-done.4 = bf16[48,2,128]{2,1,0:T(2,128)(2,1)S(1)} async-done(((bf16[48,2,128]{2,1,0:T(2,128)(2,1)}), bf16[48,2,128]{2,1,0:T(2,128)(2,1)S(1)}, u32[]{:S(2)}, u32[]{:S(2)}) %all-to-all-start.4) | async-done | bytes 24608 | tf_op jit(solution)/shard_map/all_to_all | solution.py:187
  170.1 6.5 %all-to-all-start.6 = ((f32[48,20,128]{2,1,0:T(8,128)}), f32[48,20,128]{2,1,0:T(8,128)S(1)}, u32[]{:S(2)}, u32[]{:S(2)}) async-start(f32[48,20,128]{2,1,0:T(8,128)} %reshape.203), calls=%async_computation.6 | async-start | bytes 1179648 | tf_op jit(solution)/shard_map/all_to_all | solution.py:58
  176.7 0.9 convolution_convert_fusion.5
  177.5 0.8 convolution_convert_fusion.6
  178.7 0.2 fusion.41
  178.9 0.2 select_reduce_fusion.2
  179.1 0.2 convolution_multiply_fusion.2
  179.3 22.9 %all-to-all-done.6 = f32[48,20,128]{2,1,0:T(8,128)S(1)} async-done(((f32[48,20,128]{2,1,0:T(8,128)}), f32[48,20,128]{2,1,0:T(8,128)S(1)}, u32[]{:S(2)}, u32[]{:S(2)}) %all-to-all-start.6) | async-done | bytes 491552 | tf_op jit(solution)/shard_map/all_to_all | solution.py:58
  202.3 0.8 fusion.7
  (61 shorter events, 2.3 us)
Async XLA Ops:
  7.2 123.0 %copy-start = (bf16[1,256,2048]{2,1,0:T(8,128)(2,1)S(1)}, bf16[1,256,2048]{2,1,0:T(8,128)(2,1)}, u32[]{:S(2)}) copy-start(bf16[1,256,2048]{2,1,0:T(8,128)(2,1)} %param.37) | copy-start | bytes 3145732
  7.2 82.8 %copy-start.3 = (s32[20,2]{0,1:T(2,128)S(1)}, s32[20,2]{0,1:T(2,128)}, u32[]{:S(2)}) copy-start(s32[20,2]{0,1:T(2,128)} %param.34) | copy-start | bytes 484
  7.2 123.0 %copy-start.1 = (bf16[1,2048,256]{2,1,0:T(8,128)(2,1)S(1)}, bf16[1,2048,256]{2,1,0:T(8,128)(2,1)}, u32[]{:S(2)}) copy-start(bf16[1,2048,256]{2,1,0:T(8,128)(2,1)} %param.36) | copy-start | bytes 3145732
  19.9 22.3 %all-to-all-start = ((bf16[16,20,128]{2,1,0:T(8,128)(2,1)}), bf16[16,20,128]{2,1,0:T(8,128)(2,1)S(1)}, u32[]{:S(2)}, u32[]{:S(2)}) async-start(bf16[16,20,128]{2,1,0:T(8,128)(2,1)} %bitcast.103), calls=%async_computation | async-start | bytes 196608 | tf_op jit(solution)/shard_map/all_to_all | solution.py:17
  45.7 11.2 %all-to-all-start.1 = ((f32[16,1,1080]{2,1,0:T(1,128)}), f32[16,1,1080]{2,1,0:T(1,128)S(1)}, u32[]{:S(2)}, u32[]{:S(2)}) async-start(f32[16,1,1080]{2,1,0:T(1,128)} %broadcast_in_dim.14), calls=%async_computation.1 | async-start | bytes 147456 | tf_op jit(solution)/shard_map/all_to_all | solution.py:23
  49.1 110.1 %all-gather.2.cloned.1.call-start = ((), (), s32[]{:S(2)}) async-start(), calls=%async_computation.7 | async-start | bytes 8355840 | tf_op jit(solution)/shard_map/all_gather | solution.py:52
  107.8 55.8 %copy-start.6 = (bf16[128,128]{1,0:T(8,128)(2,1)S(1)}, bf16[128,128]{1,0:T(8,128)(2,1)}, u32[]{:S(2)}) copy-start(bf16[128,128]{1,0:T(8,128)(2,1)} %param.41) | copy-start | bytes 98308
  130.9 45.7 %copy-start.2 = (bf16[20,2048]{1,0:T(8,128)(2,1)S(1)}, bf16[20,2048]{1,0:T(8,128)(2,1)}, u32[]{:S(2)}) copy-start(bf16[20,2048]{1,0:T(8,128)(2,1)} %param.21) | copy-start | bytes 245764
  131.0 45.7 %copy-start.4 = (bf16[64,2048]{1,0:T(8,128)(2,1)S(1)}, bf16[64,2048]{1,0:T(8,128)(2,1)}, u32[]{:S(2)}) copy-start(bf16[64,2048]{1,0:T(8,128)(2,1)} %param.25) | copy-start | bytes 786436
  131.0 46.6 %copy-start.5 = (bf16[64,2048]{1,0:T(8,128)(2,1)S(1)}, bf16[64,2048]{1,0:T(8,128)(2,1)}, u32[]{:S(2)}) copy-start(bf16[64,2048]{1,0:T(8,128)(2,1)} %param.24) | copy-start | bytes 786436
  131.8 18.9 %all-to-all-start.3 = ((bf16[16,96,128]{2,1,0:T(8,128)(2,1)}), bf16[16,96,128]{2,1,0:T(8,128)(2,1)S(1)}, u32[]{:S(2)}, u32[]{:S(2)}) async-start(bf16[16,96,128]{2,1,0:T(8,128)(2,1)} %bitcast.102), calls=%async_computation.3 | async-start | bytes 786432 | tf_op jit(solution)/shard_map/all_to_all | solution.py:17
  151.4 18.7 %all-to-all-start.4 = ((bf16[48,2,128]{2,1,0:T(2,128)(2,1)}), bf16[48,2,128]{2,1,0:T(2,128)(2,1)S(1)}, u32[]{:S(2)}, u32[]{:S(2)}) async-start(bf16[48,2,128]{2,1,0:T(2,128)(2,1)} %bitcast.22), calls=%async_computation.4 | async-start | bytes 49152 | tf_op jit(solution)/shard_map/all_to_all | solution.py:187
  170.1 32.1 %all-to-all-start.6 = ((f32[48,20,128]{2,1,0:T(8,128)}), f32[48,20,128]{2,1,0:T(8,128)S(1)}, u32[]{:S(2)}, u32[]{:S(2)}) async-start(f32[48,20,128]{2,1,0:T(8,128)} %reshape.203), calls=%async_computation.6 | async-start | bytes 1179648 | tf_op jit(solution)/shard_map/all_to_all | solution.py:58
Sparse Core Ops, SparseCore 0:
  90.1 51.1 all-gather.1
where the time goes:
time: 212 us; the launch traced here: 210 us
  blocking collectives  67.4 us (32%)
  waiting for transfers between devices  57.4 us (27%)
  starting transfers between devices  35.9 us (17%)
  between operations  15 us (7%)
  matrix products  14.9 us (7%)
  other arithmetic  14.8 us (7%)
  local copies, waits for them, and re-layouts  4.55 us (2%)
    all_to_all x1, blocking collectives, from_everyone(): lax.all_to_all(jnp.broadcast_to(array[None], (length, *array.shape)), axi...  29.9 us
    all_to_all x1, waiting for transfers between devices, sent_and_summed(): lax.all_to_all(tiles, axis, split_axis=0, concat_axis=0, tiled=True)  22.9 us
    all_to_all x2, waiting for transfers between devices, sum_at_owner(): lax.all_to_all(cut_along(array, dim, length), axis, 0, 0, tiled=True)  22.1 us
    all_gather x1, blocking collectives, run_experts(): piece = lax.all_gather(flat, 'tp', axis=1, tiled=True)  20.8 us
    all_to_all x2, starting transfers between devices, sum_at_owner(): lax.all_to_all(cut_along(array, dim, length), axis, 0, 0, tiled=True)  18.2 us
    all_to_all x1, blocking collectives, local(): lax.all_to_all(send, 'ep', split_axis=0, concat_axis=0, tiled=True)  16.7 us
    all_to_all x1, starting transfers between devices, run_experts(): lax.all_to_all(result.reshape(sources, count, result.shape[1]), 'ep', spl...  7.76 us
    all_to_all x1, waiting for transfers between devices, from_everyone(): lax.all_to_all(jnp.broadcast_to(array[None], (length, *array.shape)), axi...  7 us
  transfers between devices with their start and end apart: 6, of which 5 were waited for; matrix products, arithmetic and copies ran while one was open for 7% of the time, Pallas kernels for 0%

commit v1 on v0

v1 whole, which is shorter than its diff:
```python
import jax
import jax.numpy as jnp
from jax import lax
from jax.sharding import PartitionSpec as P

epsilon = 1e-06


def project_rows(normed, weight):
    return lax.dot_general(
        normed, weight, (((1,), (1,)), ((), ())), preferred_element_type=jnp.float32
    )


def stick_weights(scores, inside):
    positions = scores.shape[1]
    log_keep = jnp.where(inside, jax.nn.log_sigmoid(-scores), 0.0)
    rows = lax.broadcasted_iota(jnp.int32, (positions, positions), 0)
    columns = lax.broadcasted_iota(jnp.int32, (positions, positions), 1)
    after = (rows > columns).astype(jnp.float32)
    remain = jnp.dot(
        log_keep, after, precision=lax.Precision.HIGHEST, preferred_element_type=jnp.float32
    )
    return jnp.where(inside, jnp.exp(jax.nn.log_sigmoid(scores) + remain), 0.0)


def exchange(array, axis):
    return lax.all_to_all(array, axis, 0, 0, tiled=True)


def to_pair(value):
    high = lax.reduce_precision(value, 8, 7)
    return high.astype(jnp.bfloat16), (value - high).astype(jnp.bfloat16)


def round_up(count, unit=8):
    return -(-count // unit) * unit


def sum_lead(array):
    return jnp.sum(array.astype(jnp.float32), axis=0)


def local(
    stream,
    norm_gain_mix,
    query_weight,
    key_weight,
    value_weight,
    score_offset,
    cache_keys,
    cache_values,
    lengths,
    out_weight,
    norm_gain_ffn,
    group_weight,
    router_weight,
    routing,
    expert_gate,
    expert_up,
    expert_down,
    branch_gate,
    dense_gate,
    dense_up,
    dense_down,
):
    seq_count = stream.shape[0]
    width = stream.shape[1]
    n_tp = lax.axis_size("tp")
    n_ep = lax.axis_size("ep")
    tp_rank = lax.axis_index("tp")
    feat = width // n_tp
    offset = tp_rank * feat
    rows_pad = round_up(seq_count)

    stream_f = stream.astype(jnp.float32)
    inverse = lax.rsqrt(jnp.mean(stream_f * stream_f, -1, keepdims=True) + epsilon)
    normed = (stream_f * inverse * norm_gain_mix.astype(jnp.float32)).astype(jnp.bfloat16)
    queries = project_rows(normed, query_weight).astype(jnp.bfloat16)
    fresh_keys = project_rows(normed, key_weight).astype(jnp.bfloat16)
    fresh_values = project_rows(normed, value_weight).astype(jnp.bfloat16)
    head_size = queries.shape[1]
    cache_len = cache_keys.shape[2]
    scores = jnp.einsum("sd,sdl->sl", queries, cache_keys, preferred_element_type=jnp.float32)
    scores = scores * head_size ** (-0.5) + score_offset[0]
    inside = lax.broadcasted_iota(jnp.int32, (1, cache_len), 1) < lengths[:, None]
    weights = stick_weights(scores, inside).astype(jnp.bfloat16)
    heads_out = jnp.einsum("sl,sdl->sd", weights, cache_values, preferred_element_type=jnp.float32)
    heads_out = jnp.pad(heads_out.astype(jnp.bfloat16), ((0, rows_pad - seq_count), (0, 0)))
    partial_value = jnp.dot(heads_out, out_weight, preferred_element_type=jnp.float32)
    terms = partial_value.astype(jnp.bfloat16).reshape(rows_pad, n_tp, feat)
    attn = sum_lead(exchange(jnp.moveaxis(terms, 1, 0), "tp"))[:seq_count]

    residual = (
        lax.dynamic_slice_in_dim(stream, offset, feat, 1).astype(jnp.float32)
        + attn.astype(jnp.bfloat16).astype(jnp.float32)
    ).astype(jnp.bfloat16)
    residual_own = residual.astype(jnp.float32)

    experts = router_weight.shape[1]
    groups = group_weight.shape[1]
    per_group = experts // groups
    top = routing.shape[1]
    cap = 2 * ((seq_count + experts - 1) // experts)
    expert_iota = lax.broadcasted_iota(jnp.int32, (1, experts), 1)
    pair_expert = routing.reshape(seq_count * top)
    onehot = (pair_expert[:, None] == expert_iota).astype(jnp.int32)
    before = jnp.cumsum(onehot, 0) - onehot
    slot = jnp.sum(before * onehot, 1)
    index = (pair_expert * cap + slot).reshape(seq_count, top)
    slot_iota = lax.broadcasted_iota(jnp.int32, (experts * cap, 1, 1), 0)
    dispatch = jnp.sum((index[None, :, :] == slot_iota).astype(jnp.int32), 2).astype(jnp.bfloat16)
    send = jnp.dot(dispatch, residual, preferred_element_type=jnp.float32).astype(jnp.bfloat16)

    both = seq_count + cap
    both_pad = round_up(both)
    arrived = exchange(
        jnp.concatenate(
            [
                jnp.broadcast_to(residual[None], (n_ep, seq_count, feat)),
                send.reshape(n_ep, cap, feat),
                jnp.zeros((n_ep, both_pad - both, feat), jnp.bfloat16),
            ],
            1,
        ),
        "ep",
    )
    total = n_ep * seq_count
    rows = arrived[:, :seq_count].reshape(total, feat).astype(jnp.float32)
    picked = arrived[:, seq_count:both].reshape(n_ep * cap, feat)

    home_weights = jnp.concatenate(
        [
            lax.dynamic_slice_in_dim(group_weight, offset, feat, 0),
            lax.dynamic_slice_in_dim(router_weight, offset, feat, 0),
            lax.dynamic_slice_in_dim(branch_gate, offset, feat, 0)[:, None],
        ],
        1,
    )
    products = jnp.dot(residual, home_weights, preferred_element_type=jnp.float32)
    expert_part = products[:, groups : groups + experts]
    home_part = jnp.concatenate(
        [products[:, :groups]]
        + [
            jnp.sum(jnp.where(expert_iota == routing[:, k : k + 1], expert_part, 0.0), 1, keepdims=True)
            for k in range(top)
        ]
        + [products[:, groups + experts :], jnp.sum(residual_own * residual_own, 1, keepdims=True)],
        1,
    )
    home_count = home_part.shape[1]

    gain_ffn = norm_gain_ffn.astype(jnp.float32)
    gain_own = lax.dynamic_slice_in_dim(gain_ffn, offset, feat, 0)
    units = dense_gate.shape[1]
    share = total // n_tp
    scaled = (rows * gain_own).astype(jnp.bfloat16)
    dense_terms = jnp.dot(
        scaled, jnp.concatenate([dense_gate, dense_up], 1), preferred_element_type=jnp.float32
    ).astype(jnp.bfloat16)
    squares_high, squares_low = to_pair(jnp.sum(rows * rows, 1).reshape(n_tp, 1, share))
    home_high, home_low = to_pair(home_part.reshape(1, seq_count * home_count))
    lanes = 2 * units
    half = n_ep * cap // 2

    def lane_pad(array):
        return jnp.pad(array, [(0, 0)] * (array.ndim - 1) + [(0, lanes - array.shape[-1])])

    common = jnp.concatenate(
        [
            jnp.concatenate([picked[:half], picked[half:]], 1),
            lane_pad(home_high),
            lane_pad(home_low),
        ],
        0,
    )
    gathered = exchange(
        jnp.concatenate(
            [
                dense_terms.reshape(n_tp, share, lanes),
                jnp.broadcast_to(common[None], (n_tp, *common.shape)),
                lane_pad(squares_high),
                lane_pad(squares_low),
            ],
            1,
        ),
        "tp",
    )
    at_home = share + half
    at_squares = at_home + 2
    dense_both = sum_lead(gathered[:, :share])
    home_sum = jnp.sum(
        gathered[:, at_home:at_squares, : seq_count * home_count].astype(jnp.float32), (0, 1)
    ).reshape(seq_count, home_count)
    squares = jnp.sum(gathered[:, at_squares:, :share].astype(jnp.float32), (0, 1))
    scale = lax.rsqrt(squares / width + epsilon)[:, None]
    dense_act = (
        jax.nn.silu(dense_both[:, :units] * scale) * (dense_both[:, units:] * scale)
    ).astype(jnp.bfloat16)

    whole = (
        gathered[:, share:at_home]
        .reshape(n_tp, half, 2, feat)
        .transpose(2, 1, 0, 3)
        .reshape(2 * half, width)
        .astype(jnp.float32)
    )
    inverse_rows = lax.rsqrt(jnp.mean(whole * whole, -1, keepdims=True) + epsilon)
    hidden_in = (whole * inverse_rows * gain_ffn).astype(jnp.bfloat16)
    gate_acc = jnp.dot(hidden_in, expert_gate[0], preferred_element_type=jnp.float32)
    up_acc = jnp.dot(hidden_in, expert_up[0], preferred_element_type=jnp.float32)
    hidden = (jax.nn.silu(gate_acc) * up_acc).astype(jnp.bfloat16)
    expert_terms = jnp.dot(hidden, expert_down[0], preferred_element_type=jnp.float32)
    expert_terms = jnp.moveaxis(
        expert_terms.astype(jnp.bfloat16).reshape(2 * half, n_tp, feat), 1, 0
    )

    reached = 2 * half + share
    summed = exchange(
        jnp.concatenate(
            [
                expert_terms,
                jnp.broadcast_to(dense_act[None], (n_tp, share, units)),
                jnp.zeros((n_tp, round_up(reached) - reached, feat), jnp.bfloat16),
            ],
            1,
        ),
        "tp",
    )
    expert_out = sum_lead(summed[:, : 2 * half]).astype(jnp.bfloat16)
    acts = summed[:, 2 * half : reached].reshape(total, units)
    dense_term = jnp.dot(acts, dense_down, preferred_element_type=jnp.float32)

    returned = exchange(
        jnp.concatenate(
            [
                dense_term.astype(jnp.bfloat16).reshape(n_ep, seq_count, feat),
                expert_out.reshape(n_ep, cap, feat),
                jnp.zeros((n_ep, both_pad - both, feat), jnp.bfloat16),
            ],
            1,
        ),
        "ep",
    )
    dense = sum_lead(returned[:, :seq_count])
    flat_back = returned[:, seq_count:both].reshape(experts * cap, feat)

    inverse_two = lax.rsqrt(home_sum[:, home_count - 1 :] / width + epsilon)
    logits = home_sum[:, : home_count - 1] * inverse_two
    group_exp = jnp.exp(logits[:, :groups])
    group_iota = lax.broadcasted_iota(jnp.int32, (1, groups), 1)
    own_group = jnp.sum(
        jnp.where(group_iota == routing[:, :1] // per_group, group_exp, 0.0), 1, keepdims=True
    )
    group_prob = own_group / jnp.sum(group_exp, 1, keepdims=True)
    chosen_exp = jnp.exp(logits[:, groups : groups + top])
    route_gate = group_prob * chosen_exp / jnp.sum(chosen_exp, 1, keepdims=True)
    row_iota = lax.broadcasted_iota(jnp.int32, (1, experts * cap), 1)
    moe = jnp.zeros((seq_count, feat), jnp.float32)
    for which in range(top):
        select = (index[:, which : which + 1] == row_iota).astype(jnp.bfloat16)
        moe = moe + route_gate[:, which : which + 1] * jnp.dot(
            select, flat_back, preferred_element_type=jnp.float32
        )
    branch = jax.nn.sigmoid(logits[:, groups + top :])
    mixed = (residual_own + moe + branch * dense).astype(jnp.bfloat16)
    return (mixed, fresh_keys, fresh_values)


def solution(mesh):
    placed = (
        P("ep", None),
        P(),
        P("tp", None),
        P("tp", None),
        P("tp", None),
        P("tp"),
        P("ep", "tp", None),
        P("ep", "tp", None),
        P("ep"),
        P("tp", None),
        P(),
        P(),
        P(),
        P("ep", None),
        P("ep", None, "tp"),
        P("ep", None, "tp"),
        P("ep", "tp", None),
        P(),
        P("tp", "ep"),
        P("tp", "ep"),
        P("ep", "tp"),
    )
    return jax.shard_map(
        local,
        mesh=mesh,
        in_specs=placed,
        out_specs=(P("ep", "tp"), P("ep", "tp"), P("ep", "tp")),
        check_vma=False,
    )
```

time: 212 us -> 152 us (0.72)
  blocking collectives: 67.4 us -> 0 us
  waiting for transfers between devices: 57.4 us -> 80.8 us
  between operations: 15 us -> 1.97 us
  matrix products: 14.9 us -> 8.97 us
  starting transfers between devices: 35.9 us -> 40.8 us
  other arithmetic: 14.8 us -> 11.1 us
  local copies, waits for them, and re-layouts: 4.55 us -> 7.72 us
    all_to_all x2 -> x0, blocking collectives: 46.6 us -> none  [the longest x1 29.9 us: from_everyone(): lax.all_to_all(jnp.broadcast_to(array[None], (length, *array.shape)), axi...]
    all_to_all x5, waiting for transfers between devices: 57.3 us -> 80.8 us  [exchange(): return lax.all_to_all(array, axis, 0, 0, tiled=True)]
    all_gather x1 -> x0, blocking collectives: 20.8 us -> none  [run_experts(): piece = lax.all_gather(flat, 'tp', axis=1, tiled=True)]
    dot_general x11 -> x9, matrix products: 9.87 us -> 4.88 us  [the longest x1 1.99 us: local(): jnp.dot(hidden, expert_down[0], preferred_element_type=jnp.float32)]
    all_to_all x5, starting transfers between devices: 35.9 us -> 40.8 us  [exchange(): return lax.all_to_all(array, axis, 0, 0, tiled=True)]
    reduce_sum x9 -> x12, other arithmetic: 5.76 us -> 2.56 us  [the longest x1 0.83 us: local(): jnp.sum(residual_own * residual_own, 1, keepdims=True)]
    concatenate x1 -> x5, other arithmetic: 0.85 us -> 3.99 us  [the longest x1 1.25 us: local(): jnp.concatenate([dense_terms.reshape(n_tp, share, lanes), jnp.broadcast_t...]
    another operation x2 -> x0, other arithmetic: 2.54 us -> none
  transfers between devices with their start and end apart: 6 -> 5, of which waited for: 5 -> 5; matrix products, arithmetic and copies ran while one was open for 7% -> 5% of each run, Pallas kernels for 0% -> 0%
where the time goes in v1:
time: 152 us; the launch traced here: 151 us
  waiting for transfers between devices  80.8 us (53%)
  starting transfers between devices  40.8 us (27%)
  other arithmetic  11.1 us (7%)
  matrix products  8.97 us (6%)
  local copies, waits for them, and re-layouts  7.72 us (5%)
  between operations  1.97 us (1%)
    all_to_all x5, waiting for transfers between devices, exchange(): return lax.all_to_all(array, axis, 0, 0, tiled=True)  80.8 us
    all_to_all x5, starting transfers between devices, exchange(): return lax.all_to_all(array, axis, 0, 0, tiled=True)  40.8 us
  transfers between devices with their start and end apart: 5, of which 5 were waited for; matrix products, arithmetic and copies ran while one was open for 5% of the time, Pallas kernels for 0%

profile of v1, /device:TPU:1, one launch (start us, length us, event | category | flops | bytes accessed | tf_op | source)
XLA Modules:
  0.0 151.4 jit_solution(11985343682174935683)
XLA Ops:
  1.4 1.0 fusion.32
  2.5 0.7 convert_element_type.178
  3.2 0.6 copy-done.10
  3.8 1.2 fusion.14
  5.1 1.3 fusion.87
  6.4 0.2 fusion.9
  6.6 0.3 fusion.64
  7.1 0.6 copy.118
  7.7 13.8 %all-to-all-start = ((bf16[16,24,128]{2,1,0:T(8,128)(2,1)}), bf16[16,24,128]{2,1,0:T(8,128)(2,1)S(1)}, u32[]{:S(2)}, u32[]{:S(2)}) async-start(bf16[16,24,128]{2,1,0:T(8,128)(2,1)} %bitcast.93), calls=%async_computation | async-start | bytes 196608 | tf_op jit(solution)/shard_map/all_to_all | solution.py:28
  21.6 0.7 constant_dynamic-slice_fusion.1
  23.2 0.7 constant_dynamic-slice_fusion
  24.0 6.0 %all-to-all-done = bf16[16,24,128]{2,1,0:T(8,128)(2,1)S(1)} async-done(((bf16[16,24,128]{2,1,0:T(8,128)(2,1)}), bf16[16,24,128]{2,1,0:T(8,128)(2,1)S(1)}, u32[]{:S(2)}, u32[]{:S(2)}) %all-to-all-start) | async-done | bytes 98336 | tf_op jit(solution)/shard_map/all_to_all | solution.py:28
  30.0 0.8 fusion.73
  30.8 0.2 convolution_convert_fusion.4
  31.1 0.8 maximum_maximum_fusion.1
  31.9 12.8 %all-to-all-start.1 = ((bf16[48,24,128]{2,1,0:T(8,128)(2,1)}), bf16[48,24,128]{2,1,0:T(8,128)(2,1)S(1)}, u32[]{:S(2)}, u32[]{:S(2)}) async-start(bf16[48,24,128]{2,1,0:T(8,128)(2,1)} %maximum_maximum_fusion.1), calls=%async_computation.1 | async-start | bytes 589824 | tf_op jit(solution)/shard_map/all_to_all | solution.py:28
  44.7 0.8 dynamic-slice_bitcast_fusion
  45.5 0.5 fusion.95
  46.2 0.2 select_reduce_fusion.2
  46.9 15.2 %all-to-all-done.1 = bf16[48,24,128]{2,1,0:T(8,128)(2,1)S(1)} async-done(((bf16[48,24,128]{2,1,0:T(8,128)(2,1)}), bf16[48,24,128]{2,1,0:T(8,128)(2,1)S(1)}, u32[]{:S(2)}, u32[]{:S(2)}) %all-to-all-start.1) | async-done | bytes 294944 | tf_op jit(solution)/shard_map/all_to_all | solution.py:28
  62.1 0.2 multiply_reduce_fusion
  62.5 0.5 copy-done.5
  63.1 0.3 convolution_convert_fusion.2
  63.6 1.3 fusion.21
  64.8 5.6 %all-to-all-start.2 = ((bf16[16,112,256]{2,1,0:T(8,128)(2,1)}), bf16[16,112,256]{2,1,0:T(8,128)(2,1)S(1)}, u32[]{:S(2)}, u32[]{:S(2)}) async-start(bf16[16,112,256]{2,1,0:T(8,128)(2,1)} %fusion.21), calls=%async_computation.2 | async-start | bytes 1835008 | tf_op jit(solution)/shard_map/all_to_all | solution.py:28
  70.5 0.6 pad.28.clone
  71.1 24.8 %all-to-all-done.2 = bf16[16,112,256]{2,1,0:T(8,128)(2,1)S(1)} async-done(((bf16[16,112,256]{2,1,0:T(8,128)(2,1)}), bf16[16,112,256]{2,1,0:T(8,128)(2,1)S(1)}, u32[]{:S(2)}, u32[]{:S(2)}) %all-to-all-start.2) | async-done | bytes 917536 | tf_op jit(solution)/shard_map/all_to_all | solution.py:28
  95.9 0.5 add_rsqrt_fusion.1
  96.5 0.4 reshape.206
  97.0 0.6 fusion.22
  97.6 0.5 fusion.24
  98.2 0.3 fusion.18
  98.5 2.0 %fusion.3 = bf16[12,16,8,128]{3,2,1,0:T(8,128)(2,1)S(1)} fusion(bf16[1,256,2048]{2,1,0:T(8,128)(2,1)S(1)} %copy-done, bf16[1,2048,256]{2,1,0:T(8,128)(2,1)} %param.36, bf16[12,8,16,128]{3,2,1,0:T(8,128)(2,1)S(1)} %bitcast.98, f32[96,256]{1,0:T(8,128)S(1)} %fusion.18), kind=kOutput, calls=%fused_computation.9 | convolution fusion | flops 201670656 | bytes 2981888 | tf_op jit(solution)/shard_map/dot_general | solution.py:213
  100.7 0.5 copy-done.17
  101.4 1.0 maximum_maximum_fusion
  102.4 3.6 %all-to-all-start.3 = ((bf16[16,160,128]{2,1,0:T(8,128)(2,1)}), bf16[16,160,128]{2,1,0:T(8,128)(2,1)S(1)}, u32[]{:S(2)}, u32[]{:S(2)}) async-start(bf16[16,160,128]{2,1,0:T(8,128)(2,1)} %maximum_maximum_fusion), calls=%async_computation.3 | async-start | bytes 1310720 | tf_op jit(solution)/shard_map/all_to_all | solution.py:28
  106.1 0.8 convolution_convert_fusion.6
  107.0 0.8 convolution_convert_fusion.5
  107.9 17.8 %all-to-all-done.3 = bf16[16,160,128]{2,1,0:T(8,128)(2,1)S(1)} async-done(((bf16[16,160,128]{2,1,0:T(8,128)(2,1)}), bf16[16,160,128]{2,1,0:T(8,128)(2,1)S(1)}, u32[]{:S(2)}, u32[]{:S(2)}) %all-to-all-start.3) | async-done | bytes 655392 | tf_op jit(solution)/shard_map/all_to_all | solution.py:28
  125.8 0.2 convolution_convert_fusion.3
  126.2 0.2 copy-done.15
  126.4 0.8 maximum_maximum_fusion.2
  127.3 5.0 %all-to-all-start.4 = ((bf16[48,24,128]{2,1,0:T(8,128)(2,1)}), bf16[48,24,128]{2,1,0:T(8,128)(2,1)S(1)}, u32[]{:S(2)}, u32[]{:S(2)}) async-start(bf16[48,24,128]{2,1,0:T(8,128)(2,1)} %maximum_maximum_fusion.2), calls=%async_computation.4 | async-start | bytes 589824 | tf_op jit(solution)/shard_map/all_to_all | solution.py:28
  132.7 0.2 fusion.86
  133.0 0.2 slice_reduce_fusion.1
  133.2 17.1 %all-to-all-done.4 = bf16[48,24,128]{2,1,0:T(8,128)(2,1)S(1)} async-done(((bf16[48,24,128]{2,1,0:T(8,128)(2,1)}), bf16[48,24,128]{2,1,0:T(8,128)(2,1)S(1)}, u32[]{:S(2)}, u32[]{:S(2)}) %all-to-all-start.4) | async-done | bytes 294944 | tf_op jit(solution)/shard_map/all_to_all | solution.py:28
  150.3 0.2 convolution_multiply_fusion.2
  150.6 0.8 fusion.13
  (103 shorter events, 3.9 us)
Async XLA Ops:
  0.6 97.8 %copy-start = (bf16[1,256,2048]{2,1,0:T(8,128)(2,1)S(1)}, bf16[1,256,2048]{2,1,0:T(8,128)(2,1)}, u32[]{:S(2)}) copy-start(bf16[1,256,2048]{2,1,0:T(8,128)(2,1)} %param.37) | copy-start | bytes 3145732
  0.6 5.7 %copy-start.21 = (s32[20]{0:T(128)S(1)}, s32[20]{0:T(128)}, u32[]{:S(2)}) copy-start(s32[20]{0:T(128)} %param.29) | copy-start | bytes 244
  0.7 6.0 %copy-start.18 = (bf16[20,64,256]{2,1,0:T(8,128)(2,1)S(1)}, bf16[20,64,256]{2,1,0:T(8,128)(2,1)}, u32[]{:S(2)}) copy-start(bf16[20,64,256]{2,1,0:T(8,128)(2,1)} %param.28) | copy-start | bytes 1966084
  2.5 4.4 %copy-start.2 = (bf16[64,2048]{1,0:T(8,128)(2,1)S(1)}, bf16[64,2048]{1,0:T(8,128)(2,1)}, u32[]{:S(2)}) copy-start(bf16[64,2048]{1,0:T(8,128)(2,1)} %param.30) | copy-start | bytes 786436
  2.5 0.7 copy-start.22
  3.2 0.6 copy-start.10
  6.3 15.1 %copy-start.12 = (bf16[2048]{0:T(1024)(128)(2,1)S(1)}, bf16[2048]{0:T(1024)(128)(2,1)}, u32[]{:S(2)}) copy-start(bf16[2048]{0:T(1024)(128)(2,1)} %param.31) | copy-start | bytes 12292
  6.3 15.9 %copy-start.7 = (s32[20,2]{0,1:T(2,128)S(1)}, s32[20,2]{0,1:T(2,128)}, u32[]{:S(2)}) copy-start(s32[20,2]{0,1:T(2,128)} %param.34) | copy-start | bytes 484
  7.7 22.3 %all-to-all-start = ((bf16[16,24,128]{2,1,0:T(8,128)(2,1)}), bf16[16,24,128]{2,1,0:T(8,128)(2,1)S(1)}, u32[]{:S(2)}, u32[]{:S(2)}) async-start(bf16[16,24,128]{2,1,0:T(8,128)(2,1)} %bitcast.93), calls=%async_computation | async-start | bytes 196608 | tf_op jit(solution)/shard_map/all_to_all | solution.py:28
  23.0 22.5 %copy-start.8 = (s32[20,2]{0,1:T(2,128)}, s32[20,2]{0,1:T(2,128)S(1)}, u32[]{:S(2)}) copy-start(s32[20,2]{0,1:T(2,128)S(1)} %multiply_add_fusion) | copy-start | bytes 484
  23.2 22.3 %copy-start.14 = (bf16[24]{0:T(256)(128)(2,1)}, bf16[24]{0:T(256)(128)(2,1)S(1)}, u32[]{:S(2)}) copy-start(bf16[24]{0:T(256)(128)(2,1)S(1)} %pad.44.clone) | copy-start | bytes 148
  31.9 30.2 %all-to-all-start.1 = ((bf16[48,24,128]{2,1,0:T(8,128)(2,1)}), bf16[48,24,128]{2,1,0:T(8,128)(2,1)S(1)}, u32[]{:S(2)}, u32[]{:S(2)}) async-start(bf16[48,24,128]{2,1,0:T(8,128)(2,1)} %maximum_maximum_fusion.1), calls=%async_computation.1 | async-start | bytes 589824 | tf_op jit(solution)/shard_map/all_to_all | solution.py:28
  62.3 0.8 copy-start.5
  62.3 0.8 copy-start.6
  64.8 31.0 %all-to-all-start.2 = ((bf16[16,112,256]{2,1,0:T(8,128)(2,1)}), bf16[16,112,256]{2,1,0:T(8,128)(2,1)S(1)}, u32[]{:S(2)}, u32[]{:S(2)}) async-start(bf16[16,112,256]{2,1,0:T(8,128)(2,1)} %fusion.21), calls=%async_computation.2 | async-start | bytes 1835008 | tf_op jit(solution)/shard_map/all_to_all | solution.py:28
  96.9 1.2 copy-start.1
  100.5 0.7 copy-start.17
  100.5 0.8 copy-start.16
  101.3 4.7 %copy-start.9 = (s32[20,2]{0,1:T(2,128)S(1)}, s32[20,2]{0,1:T(2,128)}, u32[]{:S(2)}) copy-start(s32[20,2]{0,1:T(2,128)} %copy-done.8) | copy-start | bytes 484
  101.3 4.7 %copy-start.3 = (bf16[20,2048]{1,0:T(8,128)(2,1)S(1)}, bf16[20,2048]{1,0:T(8,128)(2,1)}, u32[]{:S(2)}) copy-start(bf16[20,2048]{1,0:T(8,128)(2,1)} %param.21) | copy-start | bytes 245764
  101.3 4.7 %copy-start.11 = (f32[2048]{0:T(1024)S(1)}, f32[2048]{0:T(1024)}, u32[]{:S(2)}) copy-start(f32[2048]{0:T(1024)} %copy-done.10) | copy-start | bytes 24580
  101.3 4.7 %copy-start.19 = (bf16[64,2048]{1,0:T(8,128)(2,1)S(1)}, bf16[64,2048]{1,0:T(8,128)(2,1)}, u32[]{:S(2)}) copy-start(bf16[64,2048]{1,0:T(8,128)(2,1)} %param.24) | copy-start | bytes 786436
  101.3 4.7 %copy-start.23 = (f32[20]{0:T(128)S(1)}, f32[20]{0:T(128)}, u32[]{:S(2)}) copy-start(f32[20]{0:T(128)} %copy-done.22) | copy-start | bytes 244
  102.4 4.6 %copy-start.20 = (bf16[64,2048]{1,0:T(8,128)(2,1)S(1)}, bf16[64,2048]{1,0:T(8,128)(2,1)}, u32[]{:S(2)}) copy-start(bf16[64,2048]{1,0:T(8,128)(2,1)} %param.25) | copy-start | bytes 786436
  102.4 23.3 %all-to-all-start.3 = ((bf16[16,160,128]{2,1,0:T(8,128)(2,1)}), bf16[16,160,128]{2,1,0:T(8,128)(2,1)S(1)}, u32[]{:S(2)}, u32[]{:S(2)}) async-start(bf16[16,160,128]{2,1,0:T(8,128)(2,1)} %maximum_maximum_fusion), calls=%async_computation.3 | async-start | bytes 1310720 | tf_op jit(solution)/shard_map/all_to_all | solution.py:28
  106.0 19.8 %copy-start.4 = (bf16[128,128]{1,0:T(8,128)(2,1)S(1)}, bf16[128,128]{1,0:T(8,128)(2,1)}, u32[]{:S(2)}) copy-start(bf16[128,128]{1,0:T(8,128)(2,1)} %param.41) | copy-start | bytes 98308
  125.7 0.7 copy-start.15
  126.0 6.5 %copy-start.13 = (s32[20]{0:T(128)S(1)}, s32[20]{0:T(128)}, u32[]{:S(2)}) copy-start(s32[20]{0:T(128)} %get-tuple-element.17) | copy-start | bytes 244
  127.3 23.0 %all-to-all-start.4 = ((bf16[48,24,128]{2,1,0:T(8,128)(2,1)}), bf16[48,24,128]{2,1,0:T(8,128)(2,1)S(1)}, u32[]{:S(2)}, u32[]{:S(2)}) async-start(bf16[48,24,128]{2,1,0:T(8,128)(2,1)} %maximum_maximum_fusion.2), calls=%async_computation.4 | async-start | bytes 589824 | tf_op jit(solution)/shard_map/all_to_all | solution.py:28

commit v2 on v1

--- a/solution.py
+++ b/solution.py
@@ -2,6 +2,7 @@
 import jax.numpy as jnp
 from jax import lax
 from jax.sharding import PartitionSpec as P
+
 
 epsilon = 1e-06
 
@@ -161,50 +162,34 @@
     squares_high, squares_low = to_pair(jnp.sum(rows * rows, 1).reshape(n_tp, 1, share))
     home_high, home_low = to_pair(home_part.reshape(1, seq_count * home_count))
     lanes = 2 * units
-    half = n_ep * cap // 2
 
     def lane_pad(array):
         return jnp.pad(array, [(0, 0)] * (array.ndim - 1) + [(0, lanes - array.shape[-1])])
 
-    common = jnp.concatenate(
+    leaving = jnp.concatenate(
         [
-            jnp.concatenate([picked[:half], picked[half:]], 1),
-            lane_pad(home_high),
-            lane_pad(home_low),
+            dense_terms.reshape(n_tp, share, lanes),
+            lane_pad(squares_high),
+            lane_pad(squares_low),
+            jnp.broadcast_to(lane_pad(home_high)[None], (n_tp, 1, lanes)),
+            jnp.broadcast_to(lane_pad(home_low)[None], (n_tp, 1, lanes)),
         ],
-        0,
-    )
-    gathered = exchange(
-        jnp.concatenate(
-            [
-                dense_terms.reshape(n_tp, share, lanes),
-                jnp.broadcast_to(common[None], (n_tp, *common.shape)),
-                lane_pad(squares_high),
-                lane_pad(squares_low),
-            ],
-            1,
-        ),
-        "tp",
-    )
-    at_home = share + half
-    at_squares = at_home + 2
+        1,
+    )
+    gathered = exchange(leaving, "tp")
+    whole = lax.all_gather(picked, "tp", axis=1, tiled=True)
+    whole = whole.astype(jnp.float32)
+    at_home = share + 2
     dense_both = sum_lead(gathered[:, :share])
     home_sum = jnp.sum(
-        gathered[:, at_home:at_squares, : seq_count * home_count].astype(jnp.float32), (0, 1)
+        gathered[:, at_home:, : seq_count * home_count].astype(jnp.float32), (0, 1)
     ).reshape(seq_count, home_count)
-    squares = jnp.sum(gathered[:, at_squares:, :share].astype(jnp.float32), (0, 1))
+    squares = jnp.sum(gathered[:, share:at_home, :share].astype(jnp.float32), (0, 1))
     scale = lax.rsqrt(squares / width + epsilon)[:, None]
     dense_act = (
         jax.nn.silu(dense_both[:, :units] * scale) * (dense_both[:, units:] * scale)
     ).astype(jnp.bfloat16)
 
-    whole = (
-        gathered[:, share:at_home]
-        .reshape(n_tp, half, 2, feat)
-        .transpose(2, 1, 0, 3)
-        .reshape(2 * half, width)
-        .astype(jnp.float32)
-    )
     inverse_rows = lax.rsqrt(jnp.mean(whole * whole, -1, keepdims=True) + epsilon)
     hidden_in = (whole * inverse_rows * gain_ffn).astype(jnp.bfloat16)
     gate_acc = jnp.dot(hidden_in, expert_gate[0], preferred_element_type=jnp.float32)
@@ -212,23 +197,12 @@
     hidden = (jax.nn.silu(gate_acc) * up_acc).astype(jnp.bfloat16)
     expert_terms = jnp.dot(hidden, expert_down[0], preferred_element_type=jnp.float32)
     expert_terms = jnp.moveaxis(
-        expert_terms.astype(jnp.bfloat16).reshape(2 * half, n_tp, feat), 1, 0
-    )
-
-    reached = 2 * half + share
-    summed = exchange(
-        jnp.concatenate(
-            [
-                expert_terms,
-                jnp.broadcast_to(dense_act[None], (n_tp, share, units)),
-                jnp.zeros((n_tp, round_up(reached) - reached, feat), jnp.bfloat16),
-            ],
-            1,
-        ),
-        "tp",
-    )
-    expert_out = sum_lead(summed[:, : 2 * half]).astype(jnp.bfloat16)
-    acts = summed[:, 2 * half : reached].reshape(total, units)
+        expert_terms.astype(jnp.bfloat16).reshape(n_ep * cap, n_tp, feat), 1, 0
+    )
+
+    summed = exchange(expert_terms, "tp")
+    acts = lax.all_gather(dense_act, "tp", axis=0, tiled=True)
+    expert_out = sum_lead(summed).astype(jnp.bfloat16)
     dense_term = jnp.dot(acts, dense_down, preferred_element_type=jnp.float32)
 
     returned = exchange(

time: 152 us -> 163 us (1.072)
  blocking collectives: 0 us -> 32.7 us
  waiting for transfers between devices: 80.8 us -> 61.9 us
  other arithmetic: 11.1 us -> 5.27 us
  local copies, waits for them, and re-layouts: 7.72 us -> 12.1 us
    all_gather x0 -> x2, blocking collectives: none -> 32.7 us  [the longest x1 17.6 us: local(): whole = lax.all_gather(picked, 'tp', axis=1, tiled=True)]
    all_to_all x5, waiting for transfers between devices: 80.8 us -> 61.9 us  [exchange(): return lax.all_to_all(array, axis, 0, 0, tiled=True)]
    concatenate x1, local copies, waits for them, and re-layouts: 0.62 us -> 2.97 us  [local(): jnp.concatenate([dense_terms.reshape(n_tp, share, lanes), lane_pad(square...]
    concatenate x3 -> x0, other arithmetic: 2.31 us -> none  [the longest x1 1.25 us: local(): jnp.concatenate([dense_terms.reshape(n_tp, share, lanes), jnp.broadcast_t...]
    unnamed x51 -> x32, local copies, waits for them, and re-layouts: 2.16 us -> 3.7 us
  transfers between devices with their start and end apart: 5 -> 5, of which waited for: 5 -> 5; matrix products, arithmetic and copies ran while one was open for 5% -> 7% of each run, Pallas kernels for 0% -> 0%
where the time goes in v2:
time: 163 us; the launch traced here: 162 us
  waiting for transfers between devices  61.9 us (38%)
  starting transfers between devices  39.4 us (24%)
  blocking collectives  32.7 us (20%)
  local copies, waits for them, and re-layouts  12.1 us (7%)
  matrix products  9.14 us (6%)
  other arithmetic  5.27 us (3%)
  between operations  1.8 us (1%)
    all_to_all x5, waiting for transfers between devices, exchange(): return lax.all_to_all(array, axis, 0, 0, tiled=True)  61.9 us
    all_to_all x5, starting transfers between devices, exchange(): return lax.all_to_all(array, axis, 0, 0, tiled=True)  39.4 us
    all_gather x1, blocking collectives, local(): whole = lax.all_gather(picked, 'tp', axis=1, tiled=True)  17.6 us
    all_gather x1, blocking collectives, local(): acts = lax.all_gather(dense_act, 'tp', axis=0, tiled=True)  15.2 us
    unnamed x32, local copies, waits for them, and re-layouts  3.7 us
  transfers between devices with their start and end apart: 5, of which 5 were waited for; matrix products, arithmetic and copies ran while one was open for 7% of the time, Pallas kernels for 0%

profile of v2, /device:TPU:1, one launch (start us, length us, event | category | flops | bytes accessed | tf_op | source)
XLA Modules:
  0.0 162.4 jit_solution(16508866388599746461)
XLA Ops:
  1.4 1.0 fusion.21
  2.5 1.3 fusion.11
  3.7 1.3 fusion.75
  5.0 0.7 copy-done.13
  5.7 0.2 fusion.6
  6.0 0.3 fusion.51
  6.2 0.7 copy-done.2
  7.1 0.6 copy.99
  7.7 13.8 %all-to-all-start = ((bf16[16,24,128]{2,1,0:T(8,128)(2,1)}), bf16[16,24,128]{2,1,0:T(8,128)(2,1)S(1)}, u32[]{:S(2)}, u32[]{:S(2)}) async-start(bf16[16,24,128]{2,1,0:T(8,128)(2,1)} %bitcast.75), calls=%async_computation | async-start | bytes 196608 | tf_op jit(solution)/shard_map/all_to_all | solution.py:29
  21.5 0.7 copy-done.9
  22.2 0.7 constant_dynamic-slice_fusion.1
  23.3 0.2 select_reduce_fusion
  23.9 0.7 constant_dynamic-slice_fusion
  24.7 5.3 %all-to-all-done = bf16[16,24,128]{2,1,0:T(8,128)(2,1)S(1)} async-done(((bf16[16,24,128]{2,1,0:T(8,128)(2,1)}), bf16[16,24,128]{2,1,0:T(8,128)(2,1)S(1)}, u32[]{:S(2)}, u32[]{:S(2)}) %all-to-all-start) | async-done | bytes 98336 | tf_op jit(solution)/shard_map/all_to_all | solution.py:29
  30.1 0.2 convolution_convert_fusion.4
  30.4 0.8 maximum_maximum_fusion
  31.2 12.8 %all-to-all-start.1 = ((bf16[48,24,128]{2,1,0:T(8,128)(2,1)}), bf16[48,24,128]{2,1,0:T(8,128)(2,1)S(1)}, u32[]{:S(2)}, u32[]{:S(2)}) async-start(bf16[48,24,128]{2,1,0:T(8,128)(2,1)} %maximum_maximum_fusion), calls=%async_computation.1 | async-start | bytes 589824 | tf_op jit(solution)/shard_map/all_to_all | solution.py:29
  44.0 0.8 dynamic-slice_bitcast_fusion
  45.0 0.2 select_reduce_fusion.2
  45.7 15.6 %all-to-all-done.1 = bf16[48,24,128]{2,1,0:T(8,128)(2,1)S(1)} async-done(((bf16[48,24,128]{2,1,0:T(8,128)(2,1)}), bf16[48,24,128]{2,1,0:T(8,128)(2,1)S(1)}, u32[]{:S(2)}, u32[]{:S(2)}) %all-to-all-start.1) | async-done | bytes 294944 | tf_op jit(solution)/shard_map/all_to_all | solution.py:29
  61.4 17.6 %all_gather.7 = bf16[96,2048]{1,0:T(8,128)(2,1)S(1)} all-gather(bf16[96,128]{1,0:T(8,128)(2,1)S(1)} %bitcast.82), channel_id=1, replica_groups=mesh['ep'=48,'tp'=16] {'tp'}, dimensions={1}, use_global_device_ids=true | all-gather | bytes 417792 | tf_op jit(solution)/shard_map/all_gather | solution.py:180
  79.0 0.2 fusion.17
  79.1 1.7 %fusion.15 = f32[96,256]{1,0:T(8,128)S(1)} fusion(bf16[1,2048,256]{2,1,0:T(8,128)(2,1)} %param.35, bf16[96,2048]{1,0:T(8,128)(2,1)S(1)} %all_gather.7, f32[2048]{0:T(1024)S(1)} %convert_element_type.181, f32[96]{0:T(128)S(1)} %add_rsqrt_fusion), kind=kOutput, calls=%fused_computation.26 | convolution fusion | flops 101449728 | bytes 1548672 | tf_op jit(solution)/shard_map/dot_general | solution.py:195
  80.8 0.8 fusion
  81.6 0.8 copy.98
  82.5 4.6 %all-to-all-start.3 = ((bf16[16,96,128]{2,1,0:T(8,128)(2,1)}), bf16[16,96,128]{2,1,0:T(8,128)(2,1)S(1)}, u32[]{:S(2)}, u32[]{:S(2)}) async-start(bf16[16,96,128]{2,1,0:T(8,128)(2,1)} %bitcast.73), calls=%async_computation.3 | async-start | bytes 786432 | tf_op jit(solution)/shard_map/all_to_all | solution.py:29
  87.0 0.2 multiply_reduce_fusion
  87.5 0.7 copy-done.5
  88.3 0.3 convolution_convert_fusion.2
  88.7 3.0 %concatenate.22 = bf16[16,64,256]{2,1,0:T(8,128)(2,1)} concatenate(bf16[16,60,256]{2,1,0:T(8,128)(2,1)S(1)} %reshape.169, bf16[16,1,256]{2,1,0:T(2,128)(2,1)S(1)} %pad.19.clone, bf16[16,1,256]{2,1,0:T(2,128)(2,1)S(1)} %pad.20.clone, bf16[16,1,256]{2,1,0:T(2,128)(2,1)S(1)} %broadcast_in_dim.63, bf16[16,1,256]{2,1,0:T(2,128)(2,1)S(1)} %broadcast_in_dim.65), dimensions={1} | concatenate | bytes 1048576 | tf_op jit(solution)/shard_map/concatenate | solution.py:169
  91.6 9.9 %all-to-all-done.3 = bf16[16,96,128]{2,1,0:T(8,128)(2,1)S(1)} async-done(((bf16[16,96,128]{2,1,0:T(8,128)(2,1)}), bf16[16,96,128]{2,1,0:T(8,128)(2,1)S(1)}, u32[]{:S(2)}, u32[]{:S(2)}) %all-to-all-start.3) | async-done | bytes 393248 | tf_op jit(solution)/shard_map/all_to_all | solution.py:29
  101.5 3.5 %all-to-all-start.2 = ((bf16[16,64,256]{2,1,0:T(8,128)(2,1)}), bf16[16,64,256]{2,1,0:T(8,128)(2,1)S(1)}, u32[]{:S(2)}, u32[]{:S(2)}) async-start(bf16[16,64,256]{2,1,0:T(8,128)(2,1)} %concatenate.22), calls=%async_computation.2 | async-start | bytes 1048576 | tf_op jit(solution)/shard_map/all_to_all | solution.py:29
  105.0 0.8 convolution_convert_fusion.6
  106.0 0.8 convolution_convert_fusion.5
  106.9 14.8 %all-to-all-done.2 = bf16[16,64,256]{2,1,0:T(8,128)(2,1)S(1)} async-done(((bf16[16,64,256]{2,1,0:T(8,128)(2,1)}), bf16[16,64,256]{2,1,0:T(8,128)(2,1)S(1)}, u32[]{:S(2)}, u32[]{:S(2)}) %all-to-all-start.2) | async-done | bytes 524320 | tf_op jit(solution)/shard_map/all_to_all | solution.py:29
  121.8 0.2 fusion.67
  122.2 15.2 %all-gather = bf16[16,60,128]{2,1,0:T(8,128)(2,1)S(1)} all-gather(bf16[1,60,128]{2,1,0:T(8,128)(2,1)S(1)} %fusion.54), channel_id=1, replica_groups=mesh['ep'=48,'tp'=16] {'tp'}, dimensions={0}, use_global_device_ids=true | all-gather | bytes 261120 | tf_op jit(solution)/shard_map/all_gather | solution.py:204
  137.4 0.7 copy-done.4
  138.1 0.2 convolution_convert_fusion.3
  138.4 0.8 maximum_maximum_fusion.1
  139.2 4.8 %all-to-all-start.4 = ((bf16[48,24,128]{2,1,0:T(8,128)(2,1)}), bf16[48,24,128]{2,1,0:T(8,128)(2,1)S(1)}, u32[]{:S(2)}, u32[]{:S(2)}) async-start(bf16[48,24,128]{2,1,0:T(8,128)(2,1)} %maximum_maximum_fusion.1), calls=%async_computation.4 | async-start | bytes 589824 | tf_op jit(solution)/shard_map/all_to_all | solution.py:29
  144.1 0.2 fusion.73
  144.3 0.2 fusion.74
  144.6 0.2 slice_reduce_fusion
  144.8 0.2 fusion.72
  145.0 16.3 %all-to-all-done.4 = bf16[48,24,128]{2,1,0:T(8,128)(2,1)S(1)} async-done(((bf16[48,24,128]{2,1,0:T(8,128)(2,1)}), bf16[48,24,128]{2,1,0:T(8,128)(2,1)S(1)}, u32[]{:S(2)}, u32[]{:S(2)}) %all-to-all-start.4) | async-done | bytes 294944 | tf_op jit(solution)/shard_map/all_to_all | solution.py:29
  161.4 0.2 convolution_multiply_fusion.2
  161.6 0.8 fusion.10
  (81 shorter events, 3.2 us)
Async XLA Ops:
  0.6 80.2 %copy-start = (bf16[1,256,2048]{2,1,0:T(8,128)(2,1)S(1)}, bf16[1,256,2048]{2,1,0:T(8,128)(2,1)}, u32[]{:S(2)}) copy-start(bf16[1,256,2048]{2,1,0:T(8,128)(2,1)} %param.37) | copy-start | bytes 3145732
  0.6 1.8 %copy-start.3 = (bf16[20,2048]{1,0:T(8,128)(2,1)S(1)}, bf16[20,2048]{1,0:T(8,128)(2,1)}, u32[]{:S(2)}) copy-start(bf16[20,2048]{1,0:T(8,128)(2,1)} %param.21) | copy-start | bytes 245764
  1.4 1.1 copy-start.8
  2.5 3.5 %copy-start.10 = (bf16[20,64,256]{2,1,0:T(8,128)(2,1)S(1)}, bf16[20,64,256]{2,1,0:T(8,128)(2,1)}, u32[]{:S(2)}) copy-start(bf16[20,64,256]{2,1,0:T(8,128)(2,1)} %param.28) | copy-start | bytes 1966084
  5.0 0.7 copy-start.13
  5.9 1.0 copy-start.2
  7.7 22.3 %all-to-all-start = ((bf16[16,24,128]{2,1,0:T(8,128)(2,1)}), bf16[16,24,128]{2,1,0:T(8,128)(2,1)S(1)}, u32[]{:S(2)}, u32[]{:S(2)}) async-start(bf16[16,24,128]{2,1,0:T(8,128)(2,1)} %bitcast.75), calls=%async_computation | async-start | bytes 196608 | tf_op jit(solution)/shard_map/all_to_all | solution.py:29
  21.5 0.7 copy-start.9
  22.2 0.7 copy-start.7
  31.2 30.2 %all-to-all-start.1 = ((bf16[48,24,128]{2,1,0:T(8,128)(2,1)}), bf16[48,24,128]{2,1,0:T(8,128)(2,1)S(1)}, u32[]{:S(2)}, u32[]{:S(2)}) async-start(bf16[48,24,128]{2,1,0:T(8,128)(2,1)} %maximum_maximum_fusion), calls=%async_computation.1 | async-start | bytes 589824 | tf_op jit(solution)/shard_map/all_to_all | solution.py:29
  79.0 1.9 %copy-start.1 = (bf16[1,2048,256]{2,1,0:T(8,128)(2,1)S(1)}, bf16[1,2048,256]{2,1,0:T(8,128)(2,1)}, u32[]{:S(2)}) copy-start(bf16[1,2048,256]{2,1,0:T(8,128)(2,1)} %param.36) | copy-start | bytes 3145732
  82.5 19.1 %all-to-all-start.3 = ((bf16[16,96,128]{2,1,0:T(8,128)(2,1)}), bf16[16,96,128]{2,1,0:T(8,128)(2,1)S(1)}, u32[]{:S(2)}, u32[]{:S(2)}) async-start(bf16[16,96,128]{2,1,0:T(8,128)(2,1)} %bitcast.73), calls=%async_computation.3 | async-start | bytes 786432 | tf_op jit(solution)/shard_map/all_to_all | solution.py:29
  87.5 0.8 copy-start.5
  87.5 0.8 copy-start.6
  91.6 13.4 %copy-start.11 = (bf16[64,2048]{1,0:T(8,128)(2,1)S(1)}, bf16[64,2048]{1,0:T(8,128)(2,1)}, u32[]{:S(2)}) copy-start(bf16[64,2048]{1,0:T(8,128)(2,1)} %param.24) | copy-start | bytes 786436
  101.5 20.1 %all-to-all-start.2 = ((bf16[16,64,256]{2,1,0:T(8,128)(2,1)}), bf16[16,64,256]{2,1,0:T(8,128)(2,1)S(1)}, u32[]{:S(2)}, u32[]{:S(2)}) async-start(bf16[16,64,256]{2,1,0:T(8,128)(2,1)} %concatenate.22), calls=%async_computation.2 | async-start | bytes 1048576 | tf_op jit(solution)/shard_map/all_to_all | solution.py:29
  105.0 1.0 copy-start.12
  137.4 0.8 copy-start.4
  139.2 22.1 %all-to-all-start.4 = ((bf16[48,24,128]{2,1,0:T(8,128)(2,1)}), bf16[48,24,128]{2,1,0:T(8,128)(2,1)S(1)}, u32[]{:S(2)}, u32[]{:S(2)}) async-start(bf16[48,24,128]{2,1,0:T(8,128)(2,1)} %maximum_maximum_fusion.1), calls=%async_computation.4 | async-start | bytes 589824 | tf_op jit(solution)/shard_map/all_to_all | solution.py:29

commit v3 on v1

v3 whole, which is shorter than its diff:
```python
import jax
import jax.numpy as jnp
from jax import lax
from jax.sharding import Mesh, PartitionSpec as P

epsilon = 1e-06
TP = ("y", "core")


def project_rows(normed, weight):
    return lax.dot_general(
        normed, weight, (((1,), (1,)), ((), ())), preferred_element_type=jnp.float32
    )


def stick_weights(scores, inside):
    positions = scores.shape[1]
    log_keep = jnp.where(inside, jax.nn.log_sigmoid(-scores), 0.0)
    rows = lax.broadcasted_iota(jnp.int32, (positions, positions), 0)
    columns = lax.broadcasted_iota(jnp.int32, (positions, positions), 1)
    after = (rows > columns).astype(jnp.float32)
    remain = jnp.dot(
        log_keep, after, precision=lax.Precision.HIGHEST, preferred_element_type=jnp.float32
    )
    return jnp.where(inside, jnp.exp(jax.nn.log_sigmoid(scores) + remain), 0.0)


def exchange(array, axis):
    return lax.all_to_all(array, axis, 0, 0, tiled=True)


def to_pair(value):
    high = lax.reduce_precision(value, 8, 7)
    return high.astype(jnp.bfloat16), (value - high).astype(jnp.bfloat16)


def round_up(count, unit=8):
    return -(-count // unit) * unit


def sum_lead(array):
    return jnp.sum(array.astype(jnp.float32), axis=0)


def local(
    stream,
    norm_gain_mix,
    query_weight,
    key_weight,
    value_weight,
    score_offset,
    cache_keys,
    cache_values,
    lengths,
    out_weight,
    norm_gain_ffn,
    group_weight,
    router_weight,
    routing,
    expert_gate,
    expert_up,
    expert_down,
    branch_gate,
    dense_gate,
    dense_up,
    dense_down,
):
    seq_count = stream.shape[0]
    width = stream.shape[1]
    n_tp = lax.axis_size(TP)
    n_ep = lax.axis_size("ep")
    n_y = lax.axis_size("y")
    n_core = lax.axis_size("core")
    core = lax.axis_index("core")
    feat = width // n_tp
    offset = lax.axis_index(TP) * feat
    wide = n_core * feat
    wide_offset = lax.axis_index("y") * wide

    swap = [(0, 1), (1, 0)]
    with jax.named_scope("swap_gate"):
        other_gate = lax.ppermute(expert_gate[0], "core", swap)
    with jax.named_scope("swap_up"):
        other_up = lax.ppermute(expert_up[0], "core", swap)
    with jax.named_scope("swap_down"):
        other_down = lax.ppermute(expert_down[0], "core", swap)
    with jax.named_scope("dense_gather"):
        dense_pair = lax.all_gather(
            jnp.concatenate([dense_gate, dense_up, dense_down], 1), "core"
        )
    units = dense_gate.shape[1]
    dense_in = dense_pair[:, :, : 2 * units]
    dense_out = dense_pair[:, :, 2 * units :]
    rows_pad = round_up(seq_count)

    stream_f = stream.astype(jnp.float32)
    inverse = lax.rsqrt(jnp.mean(stream_f * stream_f, -1, keepdims=True) + epsilon)
    normed = (stream_f * inverse * norm_gain_mix.astype(jnp.float32)).astype(jnp.bfloat16)
    queries = project_rows(normed, query_weight).astype(jnp.bfloat16)
    fresh_keys = project_rows(normed, key_weight).astype(jnp.bfloat16)
    fresh_values = project_rows(normed, value_weight).astype(jnp.bfloat16)
    head_size = queries.shape[1]
    cache_len = cache_keys.shape[2]
    scores = jnp.einsum("sd,sdl->sl", queries, cache_keys, preferred_element_type=jnp.float32)
    scores = scores * head_size ** (-0.5) + score_offset[0]
    inside = lax.broadcasted_iota(jnp.int32, (1, cache_len), 1) < lengths[:, None]
    weights = stick_weights(scores, inside).astype(jnp.bfloat16)
    heads_out = jnp.einsum("sl,sdl->sd", weights, cache_values, preferred_element_type=jnp.float32)
    heads_out = jnp.pad(heads_out.astype(jnp.bfloat16), ((0, rows_pad - seq_count), (0, 0)))
    partial_value = jnp.dot(heads_out, out_weight, preferred_element_type=jnp.float32)
    terms = partial_value.astype(jnp.bfloat16).reshape(rows_pad, n_tp, feat)
    attn = sum_lead(exchange(jnp.moveaxis(terms, 1, 0), TP))[:seq_count]

    residual = (
        lax.dynamic_slice_in_dim(stream, offset, feat, 1).astype(jnp.float32)
        + attn.astype(jnp.bfloat16).astype(jnp.float32)
    ).astype(jnp.bfloat16)
    residual_own = residual.astype(jnp.float32)
    pair = lax.all_gather(residual, "core", axis=1, tiled=True)

    experts = router_weight.shape[1]
    groups = group_weight.shape[1]
    per_group = experts // groups
    top = routing.shape[1]
    cap = 2 * ((seq_count + experts - 1) // experts)
    expert_iota = lax.broadcasted_iota(jnp.int32, (1, experts), 1)
    pair_expert = routing.reshape(seq_count * top)
    onehot = (pair_expert[:, None] == expert_iota).astype(jnp.int32)
    before = jnp.cumsum(onehot, 0) - onehot
    slot = jnp.sum(before * onehot, 1)
    index = (pair_expert * cap + slot).reshape(seq_count, top)
    slot_iota = n_core * lax.broadcasted_iota(jnp.int32, (experts, 1, 1), 0) + core
    dispatch = jnp.sum((index[None, :, :] == slot_iota).astype(jnp.int32), 2).astype(jnp.bfloat16)
    send = jnp.dot(dispatch, pair, preferred_element_type=jnp.float32).astype(jnp.bfloat16)

    part = seq_count // n_core
    own_rows = lax.dynamic_slice_in_dim(pair, core * part, part, 0)
    both = seq_count + n_core
    both_pad = round_up(both)
    arrived = exchange(
        jnp.concatenate(
            [
                jnp.broadcast_to(own_rows[None, :, :feat], (n_ep, part, feat)),
                jnp.broadcast_to(own_rows[None, :, feat:], (n_ep, part, feat)),
                send.reshape(n_ep, n_core, feat),
                jnp.zeros((n_ep, both_pad - both, feat), jnp.bfloat16),
            ],
            1,
        ),
        "ep",
    )
    total = n_ep * part
    rows = [
        arrived[:, :part].reshape(total, feat).astype(jnp.float32),
        arrived[:, part:seq_count].reshape(total, feat).astype(jnp.float32),
    ]
    picked = arrived[:, seq_count:both].reshape(n_ep, wide)

    home_weights = jnp.concatenate(
        [
            lax.dynamic_slice_in_dim(group_weight, wide_offset, wide, 0),
            lax.dynamic_slice_in_dim(router_weight, wide_offset, wide, 0),
            lax.dynamic_slice_in_dim(branch_gate, wide_offset, wide, 0)[:, None],
        ],
        1,
    )
    products = jnp.dot(pair, home_weights, preferred_element_type=jnp.float32)
    expert_part = products[:, groups : groups + experts]
    home_part = jnp.concatenate(
        [products[:, :groups]]
        + [
            jnp.sum(jnp.where(expert_iota == routing[:, k : k + 1], expert_part, 0.0), 1, keepdims=True)
            for k in range(top)
        ]
        + [products[:, groups + experts :], jnp.sum(jnp.square(pair.astype(jnp.float32)), 1, keepdims=True)],
        1,
    )
    home_count = home_part.shape[1]

    gain_ffn = norm_gain_ffn.astype(jnp.float32)
    gain_wide = lax.dynamic_slice_in_dim(gain_ffn, wide_offset, wide, 0)
    share = total // n_y
    dense_terms = jnp.zeros((total, 2 * units), jnp.float32)
    for k in range(n_core):
        scaled = (rows[k] * gain_wide[k * feat : (k + 1) * feat]).astype(jnp.bfloat16)
        dense_terms += jnp.dot(scaled, dense_in[k], preferred_element_type=jnp.float32)
    dense_terms = dense_terms.astype(jnp.bfloat16)
    squares_part = sum(jnp.sum(r * r, 1) for r in rows)
    squares_high, squares_low = to_pair(squares_part.reshape(n_y, 1, share))
    home_high, home_low = to_pair(home_part.reshape(1, seq_count * home_count))
    lanes = 2 * units

    def lane_pad(array):
        return jnp.pad(array, [(0, 0)] * (array.ndim - 1) + [(0, lanes - array.shape[-1])])

    common = jnp.concatenate(
        [
            picked,
            lane_pad(home_high),
            lane_pad(home_low),
        ],
        0,
    )
    gathered = exchange(
        jnp.concatenate(
            [
                dense_terms.reshape(n_y, share, lanes),
                jnp.broadcast_to(common[None], (n_y, *common.shape)),
                lane_pad(squares_high),
                lane_pad(squares_low),
            ],
            1,
        ),
        "y",
    )
    at_home = share + n_ep
    at_squares = at_home + 2
    dense_both = sum_lead(gathered[:, :share])
    home_sum = jnp.sum(
        gathered[:, at_home:at_squares, : seq_count * home_count].astype(jnp.float32), (0, 1)
    ).reshape(seq_count, home_count)
    squares = jnp.sum(gathered[:, at_squares:, :share].astype(jnp.float32), (0, 1))
    scale = lax.rsqrt(squares / width + epsilon)[:, None]
    dense_act = (
        jax.nn.silu(dense_both[:, :units] * scale) * (dense_both[:, units:] * scale)
    ).astype(jnp.bfloat16)

    whole = (
        jnp.moveaxis(gathered[:, share:at_home], 0, 1).reshape(n_ep, width).astype(jnp.float32)
    )
    inverse_rows = lax.rsqrt(jnp.mean(whole * whole, -1, keepdims=True) + epsilon)
    hidden_in = (whole * inverse_rows * gain_ffn).astype(jnp.bfloat16)
    expert_terms = jnp.zeros((n_ep, width), jnp.float32)
    for gate_w, up_w, down_w in (
        (expert_gate[0], expert_up[0], expert_down[0]),
        (other_gate, other_up, other_down),
    ):
        gate_acc = jnp.dot(hidden_in, gate_w, preferred_element_type=jnp.float32)
        up_acc = jnp.dot(hidden_in, up_w, preferred_element_type=jnp.float32)
        hidden = (jax.nn.silu(gate_acc) * up_acc).astype(jnp.bfloat16)
        expert_terms += jnp.dot(hidden, down_w, preferred_element_type=jnp.float32)
    expert_terms = jnp.moveaxis(
        expert_terms.astype(jnp.bfloat16).reshape(n_ep, n_tp, feat), 1, 0
    ).reshape(n_y, n_core * n_ep, feat)

    at_act = n_core * n_ep
    reached = at_act + share
    summed = exchange(
        jnp.concatenate(
            [
                expert_terms,
                jnp.broadcast_to(dense_act[None], (n_y, share, units)),
                jnp.zeros((n_y, round_up(reached) - reached, feat), jnp.bfloat16),
            ],
            1,
        ),
        "y",
    )
    expert_out = sum_lead(summed[:, :at_act]).astype(jnp.bfloat16)
    acts = summed[:, at_act:reached].reshape(total, units)
    dense_terms_out = [
        jnp.dot(acts, dense_out[k], preferred_element_type=jnp.float32)
        .astype(jnp.bfloat16)
        .reshape(n_ep, part, feat)
        for k in range(n_core)
    ]

    returned = exchange(
        jnp.concatenate(
            dense_terms_out
            + [
                jnp.moveaxis(expert_out.reshape(n_core, n_ep, feat), 0, 1),
                jnp.zeros((n_ep, both_pad - both, feat), jnp.bfloat16),
            ],
            1,
        ),
        "ep",
    )
    dense = sum_lead(returned[:, :seq_count])
    dense = jnp.concatenate([dense[:part], dense[part:]], 1)
    back = returned[:, seq_count:both].reshape(n_ep, wide)

    inverse_two = lax.rsqrt(home_sum[:, home_count - 1 :] / width + epsilon)
    logits = home_sum[:, : home_count - 1] * inverse_two
    group_exp = jnp.exp(logits[:, :groups])
    group_iota = lax.broadcasted_iota(jnp.int32, (1, groups), 1)
    own_group = jnp.sum(
        jnp.where(group_iota == routing[:, :1] // per_group, group_exp, 0.0), 1, keepdims=True
    )
    group_prob = own_group / jnp.sum(group_exp, 1, keepdims=True)
    chosen_exp = jnp.exp(logits[:, groups : groups + top])
    route_gate = group_prob * chosen_exp / jnp.sum(chosen_exp, 1, keepdims=True)
    row_iota = n_core * lax.broadcasted_iota(jnp.int32, (1, experts), 1) + core
    mixture = jnp.zeros((seq_count, wide), jnp.float32)
    for which in range(top):
        select = (index[:, which : which + 1] == row_iota).astype(jnp.bfloat16)
        mixture = mixture + route_gate[:, which : which + 1] * jnp.dot(
            select, back, preferred_element_type=jnp.float32
        )
    branch = jax.nn.sigmoid(logits[:, groups + top :])
    mine = lax.broadcasted_iota(jnp.int32, (seq_count, 1), 0) // part == core
    mixture = mixture + branch * jnp.where(mine, jnp.concatenate([dense] * n_core, 0), 0.0)
    mixture = jnp.sum(lax.all_gather(mixture, "core"), 0)
    mixed = (residual_own + lax.dynamic_slice_in_dim(mixture, core * feat, feat, 1)).astype(
        jnp.bfloat16
    )
    return (mixed, fresh_keys, fresh_values)


def solution(mesh):
    n_ep, n_tp = mesh.devices.shape
    split = Mesh(mesh.devices.reshape(n_ep, n_tp // 2, 2), ("ep", "y", "core"))
    placed = (
        P("ep", None),
        P(),
        P(TP, None),
        P(TP, None),
        P(TP, None),
        P(TP),
        P("ep", TP, None),
        P("ep", TP, None),
        P("ep"),
        P(TP, None),
        P(),
        P(),
        P(),
        P("ep", None),
        P("ep", None, TP),
        P("ep", None, TP),
        P("ep", TP, None),
        P(),
        P(TP, "ep"),
        P(TP, "ep"),
        P("ep", TP),
    )
    return jax.shard_map(
        local,
        mesh=split,
        in_specs=placed,
        out_specs=(P("ep", TP), P("ep", TP), P("ep", TP)),
        check_vma=False,
    )
```

time: 152 us -> 141 us (0.928)
  waiting for transfers between devices: 80.8 us -> 41.7 us
  starting transfers between devices: 40.8 us -> 52.5 us
  blocking collectives: 0 us -> 10.6 us
  local copies, waits for them, and re-layouts: 7.72 us -> 12.4 us
  matrix products: 8.97 us -> 11.7 us
  other arithmetic: 11.1 us -> 9.34 us
    all_to_all x5, waiting for transfers between devices: 80.8 us -> 41.7 us  [exchange(): return lax.all_to_all(array, axis, 0, 0, tiled=True)]
    all_gather x0 -> x3, blocking collectives: none -> 10.6 us  [the longest x1 6.78 us: local(): mixture = jnp.sum(lax.all_gather(mixture, 'core'), 0)]
    ppermute x0 -> x3, starting transfers between devices: none -> 8.72 us  [the longest x1 4.39 us: local(): other_down = lax.ppermute(expert_down[0], 'core', swap)]
    unnamed x51 -> x62, local copies, waits for them, and re-layouts: 2.16 us -> 7.03 us
    dot_general x8 -> x12, matrix products: 4.05 us -> 7.91 us  [the longest x2 4.62 us: local(): expert_terms += jnp.dot(hidden, down_w, preferred_element_type=jnp.float32)]
    all_to_all x5, starting transfers between devices: 40.8 us -> 43.8 us  [exchange(): return lax.all_to_all(array, axis, 0, 0, tiled=True)]
    concatenate x5 -> x6, other arithmetic: 3.99 us -> 3.53 us  [the longest x1 0.9 us: local(): jnp.concatenate([jnp.broadcast_to(own_rows[None, :, :feat], (n_ep, part,...]
  transfers between devices with their start and end apart: 5 -> 8, of which waited for: 5 -> 5; matrix products, arithmetic and copies ran while one was open for 5% -> 10% of each run, Pallas kernels for 0% -> 0%
where the time goes in v3:
time: 141 us; the launch traced here: 140 us
  starting transfers between devices  52.5 us (37%)
  waiting for transfers between devices  41.7 us (30%)
  local copies, waits for them, and re-layouts  12.4 us (9%)
  matrix products  11.7 us (8%)
  blocking collectives  10.6 us (8%)
  other arithmetic  9.34 us (7%)
  between operations  2.03 us (1%)
    all_to_all x5, starting transfers between devices, exchange(): return lax.all_to_all(array, axis, 0, 0, tiled=True)  43.8 us
    all_to_all x5, waiting for transfers between devices, exchange(): return lax.all_to_all(array, axis, 0, 0, tiled=True)  41.7 us
    unnamed x62, local copies, waits for them, and re-layouts  7.03 us
    all_gather x1, blocking collectives, local(): mixture = jnp.sum(lax.all_gather(mixture, 'core'), 0)  6.78 us
    dot_general x2, matrix products, local(): expert_terms += jnp.dot(hidden, down_w, preferred_element_type=jnp.float32)  4.62 us
    ppermute x1, starting transfers between devices, local(): other_down = lax.ppermute(expert_down[0], 'core', swap)  4.39 us
    dot_general x3, matrix products, project_rows(): lax.dot_general(normed, weight, (((1,), (1,)), ((), ())), preferred_eleme...  2.95 us
  transfers between devices with their start and end apart: 8, of which 5 were waited for; matrix products, arithmetic and copies ran while one was open for 10% of the time, Pallas kernels for 0%

profile of v3, /device:TPU:1, one launch (start us, length us, event | category | flops | bytes accessed | tf_op | source)
XLA Modules:
  0.0 140.4 jit_solution(4282785436029683127)
XLA Ops:
  1.4 1.0 fusion.26
  2.5 1.3 fusion.13
  4.0 0.7 copy-done.25
  5.2 0.7 copy-done.2
  6.0 0.6 copy.130
  6.6 13.8 %all-to-all-start = ((bf16[16,24,128]{2,1,0:T(8,128)(2,1)}), bf16[16,24,128]{2,1,0:T(8,128)(2,1)S(1)}, u32[]{:S(2)}, u32[]{:S(2)}) async-start(bf16[16,24,128]{2,1,0:T(8,128)(2,1)} %bitcast.107), calls=%async_computation | async-start | bytes 196608 | tf_op jit(solution)/shard_map/all_to_all | solution.py:29
  20.4 0.8 dynamic_slice.26
  21.3 0.7 constant_dynamic-slice_fusion.1
  22.8 0.5 copy-done.9
  23.3 0.7 constant_dynamic-slice_fusion
  24.0 1.9 %all-gather = bf16[256,384]{1,0:T(8,128)(2,1)S(1)} all-gather(bf16[128,384]{1,0:T(8,128)(2,1)S(1)} %pad_maximum_fusion), channel_id=2, replica_groups=mesh['ep'=48,'y'=8,'core'=2] {'core'}, dimensions={0}, use_global_device_ids=true | all-gather | bytes 294912 | tf_op jit(solution)/shard_map/dense_gather/all_gather | solution.py:88
  26.2 0.5 fusion.98
  26.7 2.2 %all-to-all-done = bf16[16,24,128]{2,1,0:T(8,128)(2,1)S(1)} async-done(((bf16[16,24,128]{2,1,0:T(8,128)(2,1)}), bf16[16,24,128]{2,1,0:T(8,128)(2,1)S(1)}, u32[]{:S(2)}, u32[]{:S(2)}) %all-to-all-start) | async-done | bytes 98336 | tf_op jit(solution)/shard_map/all_to_all | solution.py:29
  28.9 1.8 %all_gather.15 = bf16[20,256]{1,0:T(8,128)(2,1)S(1)} all-gather(bf16[20,128]{1,0:T(8,128)(2,1)S(1)} %add_convert_fusion.1), channel_id=1, replica_groups=mesh['ep'=48,'y'=8,'core'=2] {'core'}, dimensions={1}, use_global_device_ids=true | all-gather | bytes 15360 | tf_op jit(solution)/shard_map/all_gather | solution.py:119
  31.2 0.9 maximum_maximum_fusion.1
  32.0 12.8 %all-to-all-start.1 = ((bf16[48,24,128]{2,1,0:T(8,128)(2,1)}), bf16[48,24,128]{2,1,0:T(8,128)(2,1)S(1)}, u32[]{:S(2)}, u32[]{:S(2)}) async-start(bf16[48,24,128]{2,1,0:T(8,128)(2,1)} %maximum_maximum_fusion.1), calls=%async_computation.1 | async-start | bytes 589824 | tf_op jit(solution)/shard_map/all_to_all | solution.py:29
  45.9 16.2 %all-to-all-done.1 = bf16[48,24,128]{2,1,0:T(8,128)(2,1)S(1)} async-done(((bf16[48,24,128]{2,1,0:T(8,128)(2,1)}), bf16[48,24,128]{2,1,0:T(8,128)(2,1)S(1)}, u32[]{:S(2)}, u32[]{:S(2)}) %all-to-all-start.1) | async-done | bytes 294944 | tf_op jit(solution)/shard_map/all_to_all | solution.py:29
  63.2 0.9 fusion.18
  64.1 4.8 %all-to-all-start.2 = ((bf16[8,112,256]{2,1,0:T(8,128)(2,1)}), bf16[8,112,256]{2,1,0:T(8,128)(2,1)S(1)}, u32[]{:S(2)}, u32[]{:S(2)}) async-start(bf16[8,112,256]{2,1,0:T(8,128)(2,1)} %fusion.18), calls=%async_computation.2 | async-start | bytes 917504 | tf_op jit(solution)/shard_map/all_to_all | solution.py:29
  68.9 4.4 %collective-permute-start.2 = (bf16[256,2048]{1,0:T(8,128)(2,1)}, bf16[256,2048]{1,0:T(8,128)(2,1)}, u32[]{:S(2)}, u32[]{:S(2)}) collective-permute-start(bf16[256,2048]{1,0:T(8,128)(2,1)} %bitcast.19), channel_id=1, source_target_pairs={{0,1},{1,0},{2,3},{3,2},{4,5},{5,4},{6,7},{7,6},{8,9},{9,8},{10,11... | collective-permute-start | bytes 3145736 | tf_op jit(solution)/shard_map/swap_down/ppermute | solution.py:86
  73.3 1.9 %collective-permute-start.1 = (bf16[2048,256]{1,0:T(8,128)(2,1)}, bf16[2048,256]{1,0:T(8,128)(2,1)}, u32[]{:S(2)}, u32[]{:S(2)}) collective-permute-start(bf16[2048,256]{1,0:T(8,128)(2,1)} %bitcast.18), channel_id=1, source_target_pairs={{0,1},{1,0},{2,3},{3,2},{4,5},{5,4},{6,7},{7,6},{8,9},{9,8},{10,11... | collective-permute-start | bytes 3145736 | tf_op jit(solution)/shard_map/swap_up/ppermute | solution.py:84
  75.2 2.4 %collective-permute-start = (bf16[2048,256]{1,0:T(8,128)(2,1)S(1)}, bf16[2048,256]{1,0:T(8,128)(2,1)}, u32[]{:S(2)}, u32[]{:S(2)}) collective-permute-start(bf16[2048,256]{1,0:T(8,128)(2,1)S(1)} %bitcast.117), channel_id=1, source_target_pairs={{0,1},{1,0},{2,3},{3,2},{4,5},{5,4},{6,7},{7,6},{8,9},{9,8},{10,11... | collective-permute-start | bytes 3145736 | tf_op jit(solution)/shard_map/swap_gate/ppermute | solution.py:82
  77.7 0.7 pad.33.clone
  78.4 0.5 fusion.97
  78.9 0.8 convolution_convert_fusion.5
  79.7 2.5 %all-to-all-done.2 = bf16[8,112,256]{2,1,0:T(8,128)(2,1)S(1)} async-done(((bf16[8,112,256]{2,1,0:T(8,128)(2,1)}), bf16[8,112,256]{2,1,0:T(8,128)(2,1)S(1)}, u32[]{:S(2)}, u32[]{:S(2)}) %all-to-all-start.2) | async-done | bytes 458784 | tf_op jit(solution)/shard_map/all_to_all | solution.py:29
  82.7 0.5 add_rsqrt_fusion
  83.2 0.3 fusion.103
  83.5 1.6 %fusion.110 = f32[48,256]{1,0:T(8,128)S(1)} fusion(bf16[2048,256]{1,0:T(8,128)(2,1)} %collective-permute-done.1, f32[48,2048]{1,0:T(8,128)S(1)} %bitcast.113, f32[2048]{0:T(1024)S(1)} %convert_element_type.215, f32[48]{0:T(128)S(1)} %add_rsqrt_fusion.1), kind=kOutput, calls=%fused_computation.205 | convolution fusion | flops 50626560 | bytes 1499328 | tf_op jit(solution)/shard_map/dot_general | solution.py:239
  85.1 2.3 %fusion.10 = f32[48,2048]{1,0:T(8,128)S(1)} fusion(bf16[48,2048]{1,0:T(8,128)(2,1)S(1)} %bitcast.116, f32[48,256]{1,0:T(8,128)S(1)} %fusion.103, bf16[1,256,2048]{2,1,0:T(8,128)(2,1)} %param.37, bf16[1,2048,256]{2,1,0:T(8,128)(2,1)} %param.36), kind=kOutput, calls=%fused_computation.22 | convolution fusion | flops 100737024 | bytes 2736128 | tf_op jit(solution)/shard_map/dot_general | solution.py:241
  87.4 2.3 %fusion.2 = bf16[6,16,8,128]{3,2,1,0:T(8,128)(2,1)S(1)} fusion(f32[48,2048]{1,0:T(8,128)S(1)} %fusion.10, bf16[256,2048]{1,0:T(8,128)(2,1)} %collective-permute-done.2, f32[48,256]{1,0:T(8,128)S(1)} %fusion.110, bf16[2048,256]{1,0:T(8,128)(2,1)} %collective-permute-done, f32[48,2048]{1,0:T(8,128)S(1)} %bitcast.114, f32[2048]{0:T(1024)S(1)} %convert_element_type.215, ...), kind=kOutput, calls=%fused_computation.7 | convolution fusion | flops 101228544 | bytes 3137728 | tf_op jit(solution)/shard_map/dot_general | solution.py:241
  89.9 0.5 copy-done.18
  90.5 0.7 copy-done.21
  91.2 0.8 maximum_maximum_fusion
  92.0 4.5 %all-to-all-start.3 = ((bf16[8,160,128]{2,1,0:T(8,128)(2,1)}), bf16[8,160,128]{2,1,0:T(8,128)(2,1)S(1)}, u32[]{:S(2)}, u32[]{:S(2)}) async-start(bf16[8,160,128]{2,1,0:T(8,128)(2,1)} %maximum_maximum_fusion), calls=%async_computation.3 | async-start | bytes 655360 | tf_op jit(solution)/shard_map/all_to_all | solution.py:29
  96.5 0.7 copy-done.10
  97.2 0.6 copy-done.27
  97.8 0.8 convolution_convert_fusion.4
  98.8 8.0 %all-to-all-done.3 = bf16[8,160,128]{2,1,0:T(8,128)(2,1)S(1)} async-done(((bf16[8,160,128]{2,1,0:T(8,128)(2,1)}), bf16[8,160,128]{2,1,0:T(8,128)(2,1)S(1)}, u32[]{:S(2)}, u32[]{:S(2)}) %all-to-all-start.3) | async-done | bytes 327712 | tf_op jit(solution)/shard_map/all_to_all | solution.py:29
  107.4 0.7 copy-done.16
  108.0 0.9 maximum_maximum_fusion.2
  108.9 7.9 %all-to-all-start.4 = ((bf16[48,24,128]{2,1,0:T(8,128)(2,1)}), bf16[48,24,128]{2,1,0:T(8,128)(2,1)S(1)}, u32[]{:S(2)}, u32[]{:S(2)}) async-start(bf16[48,24,128]{2,1,0:T(8,128)(2,1)} %maximum_maximum_fusion.2), calls=%async_computation.4 | async-start | bytes 589824 | tf_op jit(solution)/shard_map/all_to_all | solution.py:29
  117.1 0.7 copy-done.17
  118.5 12.7 %all-to-all-done.4 = bf16[48,24,128]{2,1,0:T(8,128)(2,1)S(1)} async-done(((bf16[48,24,128]{2,1,0:T(8,128)(2,1)}), bf16[48,24,128]{2,1,0:T(8,128)(2,1)S(1)}, u32[]{:S(2)}, u32[]{:S(2)}) %all-to-all-start.4) | async-done | bytes 294944 | tf_op jit(solution)/shard_map/all_to_all | solution.py:29
  131.3 0.7 copy-done.20
  132.2 0.6 copy-done.28
  133.0 6.8 %all-gather.2 = f32[2,20,256]{2,1,0:T(8,128)S(1)} all-gather(f32[1,20,256]{2,1,0:T(8,128)S(1)} %fusion.9), channel_id=3, replica_groups=mesh['ep'=48,'y'=8,'core'=2] {'core'}, dimensions={0}, use_global_device_ids=true | all-gather | bytes 61440 | tf_op jit(solution)/shard_map/all_gather | solution.py:303
  139.8 0.6 add_convert_fusion
  (144 shorter events, 7.1 us)
Async XLA Ops:
  0.6 3.1 %copy-start = (bf16[20,64,256]{2,1,0:T(8,128)(2,1)S(1)}, bf16[20,64,256]{2,1,0:T(8,128)(2,1)}, u32[]{:S(2)}) copy-start(bf16[20,64,256]{2,1,0:T(8,128)(2,1)} %param.27) | copy-start | bytes 1966084
  0.6 1.8 %copy-start.3 = (bf16[20,2048]{1,0:T(8,128)(2,1)S(1)}, bf16[20,2048]{1,0:T(8,128)(2,1)}, u32[]{:S(2)}) copy-start(bf16[20,2048]{1,0:T(8,128)(2,1)} %param.21) | copy-start | bytes 245764
  1.4 1.1 copy-start.14
  2.4 76.5 %copy-start.26 = (f32[20]{0:T(128)}, f32[20]{0:T(128)S(1)}, u32[]{:S(2)}) copy-start(f32[20]{0:T(128)S(1)} %add_rsqrt_fusion.2) | copy-start | bytes 244
  2.5 76.4 %copy-start.11 = (f32[2048]{0:T(1024)}, f32[2048]{0:T(1024)S(1)}, u32[]{:S(2)}) copy-start(f32[2048]{0:T(1024)S(1)} %convert_element_type.200) | copy-start | bytes 24580
  2.5 2.4 %copy-start.22 = (bf16[20,64,256]{2,1,0:T(8,128)(2,1)S(1)}, bf16[20,64,256]{2,1,0:T(8,128)(2,1)}, u32[]{:S(2)}) copy-start(bf16[20,64,256]{2,1,0:T(8,128)(2,1)} %param.28) | copy-start | bytes 1966084
  4.0 0.7 copy-start.25
  4.9 1.0 copy-start.2
  6.6 22.3 %all-to-all-start = ((bf16[16,24,128]{2,1,0:T(8,128)(2,1)}), bf16[16,24,128]{2,1,0:T(8,128)(2,1)S(1)}, u32[]{:S(2)}, u32[]{:S(2)}) async-start(bf16[16,24,128]{2,1,0:T(8,128)(2,1)} %bitcast.107), calls=%async_computation | async-start | bytes 196608 | tf_op jit(solution)/shard_map/all_to_all | solution.py:29
  20.4 5.7 %copy-start.19 = (s32[48]{0:T(128)}, s32[48]{0:T(128)S(1)}, u32[]{:S(2)}) copy-start(s32[48]{0:T(128)S(1)} %multiply_add_fusion.1) | copy-start | bytes 580
  20.4 0.8 copy-start.7
  21.3 0.7 copy-start.8
  22.2 1.8 %copy-start.6 = (bf16[128,128]{1,0:T(8,128)(2,1)S(1)}, bf16[128,128]{1,0:T(8,128)(2,1)}, u32[]{:S(2)}) copy-start(bf16[128,128]{1,0:T(8,128)(2,1)} %param.39) | copy-start | bytes 98308
  22.7 1.3 copy-start.4
  22.7 1.3 copy-start.5
  22.7 0.6 copy-start.9
  26.1 5.1 %copy-start.15 = (bf16[24]{0:T(256)(128)(2,1)}, bf16[24]{0:T(256)(128)(2,1)S(1)}, u32[]{:S(2)}) copy-start(bf16[24]{0:T(256)(128)(2,1)S(1)} %pad.50.clone) | copy-start | bytes 148
  32.0 30.1 %all-to-all-start.1 = ((bf16[48,24,128]{2,1,0:T(8,128)(2,1)}), bf16[48,24,128]{2,1,0:T(8,128)(2,1)S(1)}, u32[]{:S(2)}, u32[]{:S(2)}) async-start(bf16[48,24,128]{2,1,0:T(8,128)(2,1)} %maximum_maximum_fusion.1), calls=%async_computation.1 | async-start | bytes 589824 | tf_op jit(solution)/shard_map/all_to_all | solution.py:29
  63.2 12.0 %copy-start.1 = (bf16[1,2048,256]{2,1,0:T(8,128)(2,1)S(1)}, bf16[1,2048,256]{2,1,0:T(8,128)(2,1)}, u32[]{:S(2)}) copy-start(bf16[1,2048,256]{2,1,0:T(8,128)(2,1)} %param.35) | copy-start | bytes 3145732
  64.1 14.8 %copy-start.23 = (bf16[64,2048]{1,0:T(8,128)(2,1)S(1)}, bf16[64,2048]{1,0:T(8,128)(2,1)}, u32[]{:S(2)}) copy-start(bf16[64,2048]{1,0:T(8,128)(2,1)} %param.24) | copy-start | bytes 786436
  64.1 18.2 %all-to-all-start.2 = ((bf16[8,112,256]{2,1,0:T(8,128)(2,1)}), bf16[8,112,256]{2,1,0:T(8,128)(2,1)S(1)}, u32[]{:S(2)}, u32[]{:S(2)}) async-start(bf16[8,112,256]{2,1,0:T(8,128)(2,1)} %fusion.18), calls=%async_computation.2 | async-start | bytes 917504 | tf_op jit(solution)/shard_map/all_to_all | solution.py:29
  68.9 18.5 %collective-permute-start.2 = (bf16[256,2048]{1,0:T(8,128)(2,1)}, bf16[256,2048]{1,0:T(8,128)(2,1)}, u32[]{:S(2)}, u32[]{:S(2)}) collective-permute-start(bf16[256,2048]{1,0:T(8,128)(2,1)} %bitcast.19), channel_id=1, source_target_pairs={{0,1},{1,0},{2,3},{3,2},{4,5},{5,4},{6,7},{7,6},{8,9},{9,8},{10,11... | collective-permute-start | bytes 3145736 | tf_op jit(solution)/shard_map/swap_down/ppermute | solution.py:86
  73.3 10.2 %collective-permute-start.1 = (bf16[2048,256]{1,0:T(8,128)(2,1)}, bf16[2048,256]{1,0:T(8,128)(2,1)}, u32[]{:S(2)}, u32[]{:S(2)}) collective-permute-start(bf16[2048,256]{1,0:T(8,128)(2,1)} %bitcast.18), channel_id=1, source_target_pairs={{0,1},{1,0},{2,3},{3,2},{4,5},{5,4},{6,7},{7,6},{8,9},{9,8},{10,11... | collective-permute-start | bytes 3145736 | tf_op jit(solution)/shard_map/swap_up/ppermute | solution.py:84
  75.2 12.2 %collective-permute-start = (bf16[2048,256]{1,0:T(8,128)(2,1)S(1)}, bf16[2048,256]{1,0:T(8,128)(2,1)}, u32[]{:S(2)}, u32[]{:S(2)}) collective-permute-start(bf16[2048,256]{1,0:T(8,128)(2,1)S(1)} %bitcast.117), channel_id=1, source_target_pairs={{0,1},{1,0},{2,3},{3,2},{4,5},{5,4},{6,7},{7,6},{8,9},{9,8},{10,11... | collective-permute-start | bytes 3145736 | tf_op jit(solution)/shard_map/swap_gate/ppermute | solution.py:82
  82.5 1.1 copy-start.13
  89.8 0.6 copy-start.18
  90.5 0.7 copy-start.21
  92.0 5.2 %copy-start.12 = (f32[2048]{0:T(1024)S(1)}, f32[2048]{0:T(1024)}, u32[]{:S(2)}) copy-start(f32[2048]{0:T(1024)} %copy-done.11) | copy-start | bytes 24580
  92.0 5.2 %copy-start.24 = (bf16[64,2048]{1,0:T(8,128)(2,1)S(1)}, bf16[64,2048]{1,0:T(8,128)(2,1)}, u32[]{:S(2)}) copy-start(bf16[64,2048]{1,0:T(8,128)(2,1)} %param.25) | copy-start | bytes 786436
  92.0 14.7 %all-to-all-start.3 = ((bf16[8,160,128]{2,1,0:T(8,128)(2,1)}), bf16[8,160,128]{2,1,0:T(8,128)(2,1)S(1)}, u32[]{:S(2)}, u32[]{:S(2)}) async-start(bf16[8,160,128]{2,1,0:T(8,128)(2,1)} %maximum_maximum_fusion), calls=%async_computation.3 | async-start | bytes 655360 | tf_op jit(solution)/shard_map/all_to_all | solution.py:29
  96.5 0.7 copy-start.10
  97.2 0.6 copy-start.27
  107.3 0.7 copy-start.16
  108.9 22.3 %all-to-all-start.4 = ((bf16[48,24,128]{2,1,0:T(8,128)(2,1)}), bf16[48,24,128]{2,1,0:T(8,128)(2,1)S(1)}, u32[]{:S(2)}, u32[]{:S(2)}) async-start(bf16[48,24,128]{2,1,0:T(8,128)(2,1)} %maximum_maximum_fusion.2), calls=%async_computation.4 | async-start | bytes 589824 | tf_op jit(solution)/shard_map/all_to_all | solution.py:29
  117.1 0.7 copy-start.17
  131.3 0.7 copy-start.20
  132.2 0.6 copy-start.28

commit v4 on v3

v4 whole, which is shorter than its diff:
```python
import jax
import jax.numpy as jnp
from jax import lax
from jax.experimental import pallas as pl
from jax.experimental.pallas import tpu as pltpu
from jax.sharding import Mesh, PartitionSpec as P

epsilon = 1e-06
TP = ("y", "core")


def across(left, right):
    return lax.dot_general(
        left, right, (((1,), (1,)), ((), ())), preferred_element_type=jnp.float32
    )


def attend_kernel(
    offset_ref,
    lengths_ref,
    stream_ref,
    gain_ref,
    query_ref,
    key_ref,
    value_ref,
    keys_ref,
    values_ref,
    out_weight_ref,
    terms_ref,
    fresh_keys_ref,
    fresh_values_ref,
):
    count, width = stream_ref.shape
    head_size, cache_len = keys_ref.shape[1:]
    n_blocks, rows, feat = terms_ref.shape
    stream_f = stream_ref[...].astype(jnp.float32)
    inverse = lax.rsqrt(jnp.mean(stream_f * stream_f, -1, keepdims=True) + epsilon)
    normed = (stream_f * inverse * gain_ref[...].astype(jnp.float32)[None]).astype(jnp.bfloat16)
    queries = across(normed, query_ref[...])
    queries = jnp.concatenate([queries, jnp.zeros((rows - count, head_size), jnp.float32)], 0)
    queries = queries.astype(jnp.bfloat16)
    row = lax.broadcasted_iota(jnp.int32, (rows, 1), 0)
    scores = jnp.zeros((rows, cache_len), jnp.float32)
    for s in range(count):
        each = jnp.dot(queries, keys_ref[s], preferred_element_type=jnp.float32)
        scores = jnp.where(row == s, each, scores)
    scores = scores * head_size ** (-0.5) + offset_ref[0]
    filled = jnp.zeros((rows, 1), jnp.int32)
    for s in range(count):
        filled = jnp.where(row == s, lengths_ref[s], filled)
    inside = lax.broadcasted_iota(jnp.int32, (rows, cache_len), 1) < filled
    tail = jnp.log1p(jnp.exp(-jnp.abs(scores)))
    log_keep = jnp.where(inside, jnp.minimum(-scores, 0.0) - tail, 0.0)
    after = (
        lax.broadcasted_iota(jnp.int32, (cache_len, cache_len), 0)
        > lax.broadcasted_iota(jnp.int32, (cache_len, cache_len), 1)
    ).astype(jnp.float32)
    remain = jnp.dot(
        log_keep, after, precision=lax.Precision.HIGHEST, preferred_element_type=jnp.float32
    )
    weights = jnp.where(inside, jnp.exp(jnp.minimum(scores, 0.0) - tail + remain), 0.0)
    weights = weights.astype(jnp.bfloat16)
    heads_out = jnp.zeros((rows, head_size), jnp.float32)
    for s in range(count):
        heads_out = jnp.where(row == s, across(weights, values_ref[s]), heads_out)
    terms = jnp.dot(
        heads_out.astype(jnp.bfloat16), out_weight_ref[...], preferred_element_type=jnp.float32
    ).astype(jnp.bfloat16)
    for k in range(n_blocks):
        terms_ref[k] = terms[:, k * feat : (k + 1) * feat]
    fresh_keys_ref[...] = across(normed, key_ref[...]).astype(jnp.bfloat16)
    fresh_values_ref[...] = across(normed, value_ref[...]).astype(jnp.bfloat16)


def attend(
    stream, gain, query_w, key_w, value_w, offset, keys, values, lengths, out_weight, n_tp, rows
):
    count, width = stream.shape
    whole = pl.BlockSpec(memory_space=pltpu.VMEM)
    fresh = jax.ShapeDtypeStruct((count, key_w.shape[0]), jnp.bfloat16)
    return pl.pallas_call(
        attend_kernel,
        out_shape=(
            jax.ShapeDtypeStruct((n_tp, rows, width // n_tp), jnp.bfloat16),
            fresh,
            fresh,
        ),
        in_specs=[pl.BlockSpec(memory_space=pltpu.SMEM)] * 2 + [whole] * 8,
        out_specs=(whole, whole, whole),
        name="attend",
    )(offset, lengths, stream, gain, query_w, key_w, value_w, keys, values, out_weight)


def silu(value):
    return value * jax.nn.sigmoid(value)


def expert_kernel(
    gathered_ref,
    gain_ref,
    gate_hbm,
    up_hbm,
    down_hbm,
    other_gate_hbm,
    other_up_hbm,
    other_down_hbm,
    out_ref,
    home_ref,
    hidden_ref,
    gate_ref,
    up_ref,
    down_ref,
    other_gate_ref,
    other_up_ref,
    other_down_ref,
    sems,
):
    copies = [
        pltpu.make_async_copy(source, target, sems.at[k])
        for k, (source, target) in enumerate(
            (
                (gate_hbm, gate_ref),
                (up_hbm, up_ref),
                (other_gate_hbm, other_gate_ref),
                (other_up_hbm, other_up_ref),
                (down_hbm, down_ref),
                (other_down_hbm, other_down_ref),
            )
        )
    ]
    for copy in copies:
        copy.start()
    n_y, rows_in, lanes = gathered_ref.shape
    n_rows, width = hidden_ref.shape
    feat = out_ref.shape[2]
    units = lanes // 2
    at_expert = rows_in - n_rows
    share = at_expert - 4

    both = gathered_ref[0, :at_expert].astype(jnp.float32)
    for k in range(1, n_y):
        both = both + gathered_ref[k, :at_expert].astype(jnp.float32)
    home_ref[...] = both[share:]
    squares = both[share + 2 : share + 3] + both[share + 3 : share + 4]
    diagonal = lax.broadcasted_iota(jnp.int32, (at_expert, lanes), 0) == lax.broadcasted_iota(
        jnp.int32, (at_expert, lanes), 1
    )
    column = jnp.sum(jnp.where(diagonal, squares, 0.0), 1, keepdims=True)
    both = both * lax.rsqrt(column / width + epsilon)
    act = (silu(both[:, :units]) * both[:, units:]).astype(jnp.bfloat16)
    for k in range(n_y):
        out_ref[k, 2 * n_rows :] = act

    squares = jnp.zeros((n_rows, 1), jnp.float32)
    for k in range(n_y):
        rows = gathered_ref[k, at_expert:].astype(jnp.float32)
        squares = squares + jnp.sum(rows * rows, 1, keepdims=True)
    inverse = lax.rsqrt(squares / width + epsilon)
    for k in range(n_y):
        rows = gathered_ref[k, at_expert:].astype(jnp.float32)
        gain = gain_ref[pl.ds(k * lanes, lanes)].astype(jnp.float32)[None]
        hidden_ref[:, k * lanes : (k + 1) * lanes] = (rows * inverse * gain).astype(jnp.bfloat16)
    hidden_in = hidden_ref[...]
    acts = []
    for k, (gate_w, up_w) in enumerate(((gate_ref, up_ref), (other_gate_ref, other_up_ref))):
        copies[2 * k].wait()
        gate = jnp.dot(hidden_in, gate_w[...], preferred_element_type=jnp.float32)
        copies[2 * k + 1].wait()
        up = jnp.dot(hidden_in, up_w[...], preferred_element_type=jnp.float32)
        acts.append((silu(gate) * up).astype(jnp.bfloat16))
    copies[4].wait()
    copies[5].wait()
    for k in range(n_y):
        columns = slice(k * lanes, (k + 1) * lanes)
        terms = jnp.dot(acts[0], down_ref[:, columns], preferred_element_type=jnp.float32)
        terms = terms + jnp.dot(
            acts[1], other_down_ref[:, columns], preferred_element_type=jnp.float32
        )
        terms = terms.astype(jnp.bfloat16)
        out_ref[k, :n_rows] = terms[:, :feat]
        out_ref[k, n_rows : 2 * n_rows] = terms[:, feat:]


def run_expert(gathered, gain, weights, n_rows, feat):
    n_y, rows_in, lanes = gathered.shape
    at_expert = rows_in - n_rows
    whole = pl.BlockSpec(memory_space=pltpu.VMEM)
    return pl.pallas_call(
        expert_kernel,
        out_shape=(
            jax.ShapeDtypeStruct((n_y, 2 * n_rows + at_expert, feat), jnp.bfloat16),
            jax.ShapeDtypeStruct((4, lanes), jnp.float32),
        ),
        in_specs=[whole, whole] + [pl.BlockSpec(memory_space=pltpu.HBM)] * 6,
        out_specs=(whole, whole),
        scratch_shapes=[pltpu.VMEM((n_rows, gain.shape[0]), jnp.bfloat16)]
        + [pltpu.VMEM(weights[k].shape, jnp.bfloat16) for k in range(6)]
        + [pltpu.SemaphoreType.DMA((6,))],
        compiler_params=pltpu.CompilerParams(vmem_limit_bytes=52 * 2**20),
        name="expert",
    )(gathered, gain, *weights)


def exchange(array, axis):
    return lax.all_to_all(array, axis, 0, 0, tiled=True)


def to_pair(value):
    high = lax.reduce_precision(value, 8, 7)
    return high.astype(jnp.bfloat16), (value - high).astype(jnp.bfloat16)


def round_up(count, unit=8):
    return -(-count // unit) * unit


def sum_lead(array):
    return jnp.sum(array.astype(jnp.float32), axis=0)


def local(
    stream,
    norm_gain_mix,
    query_weight,
    key_weight,
    value_weight,
    score_offset,
    cache_keys,
    cache_values,
    lengths,
    out_weight,
    norm_gain_ffn,
    group_weight,
    router_weight,
    routing,
    expert_gate,
    expert_up,
    expert_down,
    branch_gate,
    dense_gate,
    dense_up,
    dense_down,
):
    seq_count = stream.shape[0]
    width = stream.shape[1]
    n_tp = lax.axis_size(TP)
    n_ep = lax.axis_size("ep")
    n_y = lax.axis_size("y")
    n_core = lax.axis_size("core")
    core = lax.axis_index("core")
    feat = width // n_tp
    offset = lax.axis_index(TP) * feat
    wide = n_core * feat
    wide_offset = lax.axis_index("y") * wide

    swap = [(0, 1), (1, 0)]
    with jax.named_scope("swap_gate"):
        other_gate = lax.ppermute(expert_gate[0], "core", swap)
    with jax.named_scope("swap_up"):
        other_up = lax.ppermute(expert_up[0], "core", swap)
    with jax.named_scope("swap_down"):
        other_down = lax.ppermute(expert_down[0], "core", swap)
    with jax.named_scope("dense_gather"):
        dense_pair = lax.all_gather(
            jnp.concatenate([dense_gate, dense_up, dense_down], 1), "core"
        )
    units = dense_gate.shape[1]
    dense_in = dense_pair[:, :, : 2 * units]
    dense_out = dense_pair[:, :, 2 * units :]
    rows_pad = round_up(seq_count)

    terms, fresh_keys, fresh_values = attend(
        stream,
        norm_gain_mix,
        query_weight,
        key_weight,
        value_weight,
        score_offset,
        cache_keys,
        cache_values,
        lengths,
        out_weight,
        n_tp,
        rows_pad,
    )
    attn = sum_lead(exchange(terms, TP))[:seq_count]

    residual = (
        lax.dynamic_slice_in_dim(stream, offset, feat, 1).astype(jnp.float32)
        + attn.astype(jnp.bfloat16).astype(jnp.float32)
    ).astype(jnp.bfloat16)
    residual_own = residual.astype(jnp.float32)
    pair = lax.all_gather(residual, "core", axis=1, tiled=True)

    experts = router_weight.shape[1]
    groups = group_weight.shape[1]
    per_group = experts // groups
    top = routing.shape[1]
    cap = 2 * ((seq_count + experts - 1) // experts)
    expert_iota = lax.broadcasted_iota(jnp.int32, (1, experts), 1)
    pair_expert = routing.reshape(seq_count * top)
    onehot = (pair_expert[:, None] == expert_iota).astype(jnp.int32)
    before = jnp.cumsum(onehot, 0) - onehot
    slot = jnp.sum(before * onehot, 1)
    index = (pair_expert * cap + slot).reshape(seq_count, top)
    slot_iota = n_core * lax.broadcasted_iota(jnp.int32, (experts, 1, 1), 0) + core
    dispatch = jnp.sum((index[None, :, :] == slot_iota).astype(jnp.int32), 2).astype(jnp.bfloat16)
    send = jnp.dot(dispatch, pair, preferred_element_type=jnp.float32).astype(jnp.bfloat16)

    part = seq_count // n_core
    own_rows = lax.dynamic_slice_in_dim(pair, core * part, part, 0)
    both = seq_count + n_core
    spare = (round_up(both) - seq_count) // n_core
    arrived = exchange(
        jnp.concatenate(
            [
                jnp.broadcast_to(own_rows[None, :, :feat], (n_ep, part, feat)),
                jnp.broadcast_to(own_rows[None, :, feat:], (n_ep, part, feat)),
                jnp.tile(send.reshape(n_ep, n_core, feat), (1, spare, 1)),
            ],
            1,
        ),
        "ep",
    )
    arrived, other_gate, other_up, other_down = lax.optimization_barrier(
        (arrived, other_gate, other_up, other_down)
    )
    total = n_ep * part
    rows = [
        arrived[:, :part].reshape(total, feat).astype(jnp.float32),
        arrived[:, part:seq_count].reshape(total, feat).astype(jnp.float32),
    ]
    picked = arrived[:, seq_count:both].reshape(n_ep, wide)

    home_weights = jnp.concatenate(
        [
            lax.dynamic_slice_in_dim(group_weight, wide_offset, wide, 0),
            lax.dynamic_slice_in_dim(router_weight, wide_offset, wide, 0),
            lax.dynamic_slice_in_dim(branch_gate, wide_offset, wide, 0)[:, None],
        ],
        1,
    )
    products = jnp.dot(pair, home_weights, preferred_element_type=jnp.float32)
    expert_part = products[:, groups : groups + experts]
    home_part = jnp.concatenate(
        [products[:, :groups]]
        + [
            jnp.sum(jnp.where(expert_iota == routing[:, k : k + 1], expert_part, 0.0), 1, keepdims=True)
            for k in range(top)
        ]
        + [products[:, groups + experts :], jnp.sum(jnp.square(pair.astype(jnp.float32)), 1, keepdims=True)],
        1,
    )
    home_count = home_part.shape[1]

    gain_ffn = norm_gain_ffn.astype(jnp.float32)
    gain_wide = lax.dynamic_slice_in_dim(gain_ffn, wide_offset, wide, 0)
    share = total // n_y
    dense_terms = jnp.zeros((total, 2 * units), jnp.float32)
    for k in range(n_core):
        scaled = (rows[k] * gain_wide[k * feat : (k + 1) * feat]).astype(jnp.bfloat16)
        dense_terms += jnp.dot(scaled, dense_in[k], preferred_element_type=jnp.float32)
    dense_terms = dense_terms.astype(jnp.bfloat16)
    squares_part = sum(jnp.sum(r * r, 1) for r in rows)
    squares_high, squares_low = to_pair(squares_part.reshape(n_y, 1, share))
    home_high, home_low = to_pair(home_part.reshape(1, seq_count * home_count))
    lanes = 2 * units

    def lane_pad(array):
        return jnp.pad(array, [(0, 0)] * (array.ndim - 1) + [(0, lanes - array.shape[-1])])

    home_rows = jnp.concatenate([lane_pad(home_high), lane_pad(home_low)], 0)
    gathered = exchange(
        jnp.concatenate(
            [
                dense_terms.reshape(n_y, share, lanes),
                jnp.broadcast_to(home_rows[None], (n_y, *home_rows.shape)),
                lane_pad(squares_high),
                lane_pad(squares_low),
                jnp.broadcast_to(picked[None], (n_y, *picked.shape)),
            ],
            1,
        ),
        "y",
    )

    leaving, sums = run_expert(
        gathered,
        norm_gain_ffn,
        (expert_gate[0], expert_up[0], expert_down[0], other_gate, other_up, other_down),
        n_ep,
        feat,
    )
    home_sum = (sums[0] + sums[1])[: seq_count * home_count].reshape(seq_count, home_count)

    summed = exchange(leaving, "y")
    at_act = n_core * n_ep
    expert_out = sum_lead(summed[:, :at_act]).astype(jnp.bfloat16)
    acts = summed[:, at_act : at_act + share].reshape(total, units)
    dense_terms_out = [
        jnp.dot(acts, dense_out[k], preferred_element_type=jnp.float32)
        .astype(jnp.bfloat16)
        .reshape(n_ep, part, feat)
        for k in range(n_core)
    ]

    returned = exchange(
        jnp.concatenate(
            dense_terms_out
            + [jnp.moveaxis(expert_out.reshape(n_core, n_ep, feat), 0, 1)] * spare,
            1,
        ),
        "ep",
    )
    inverse_two = lax.rsqrt(home_sum[:, home_count - 1 :] / width + epsilon)
    logits = home_sum[:, : home_count - 1] * inverse_two
    group_exp = jnp.exp(logits[:, :groups])
    group_iota = lax.broadcasted_iota(jnp.int32, (1, groups), 1)
    own_group = jnp.sum(
        jnp.where(group_iota == routing[:, :1] // per_group, group_exp, 0.0), 1, keepdims=True
    )
    group_prob = own_group / jnp.sum(group_exp, 1, keepdims=True)
    chosen_exp = jnp.exp(logits[:, groups : groups + top])
    route_gate = group_prob * chosen_exp / jnp.sum(chosen_exp, 1, keepdims=True)
    branch = jax.nn.sigmoid(logits[:, groups + top :])

    stride = returned.shape[1]
    place = lax.broadcasted_iota(jnp.int32, (1, n_ep * stride), 1)
    block, row = place // stride, place % stride
    sequence = lax.broadcasted_iota(jnp.int32, (rows_pad, 1), 0)
    wanted = jnp.where(
        (sequence < seq_count) & (sequence // part == core), sequence % part, -seq_count
    )
    padded = jnp.pad(index, ((0, rows_pad - seq_count), (0, 0)), constant_values=-1)
    taken = [row == wanted + k * part for k in range(n_core)]
    for which in range(top):
        here = block * n_core + core == padded[:, which : which + 1]
        taken += [here & (row == seq_count + k) for k in range(n_core)]
    taken = lax.optimization_barrier(jnp.concatenate(taken, 0).astype(jnp.bfloat16))
    found = jnp.dot(
        taken, returned.reshape(n_ep * stride, feat), preferred_element_type=jnp.float32
    ).reshape(1 + top, n_core, rows_pad, feat)[:, :, :seq_count]
    mixture = [
        branch * found[0, k]
        + sum(route_gate[:, j : j + 1] * found[1 + j, k] for j in range(top))
        for k in range(n_core)
    ]
    mixture = jnp.sum(lax.all_gather(jnp.concatenate(mixture, 1), "core"), 0)
    mixed = (residual_own + lax.dynamic_slice_in_dim(mixture, core * feat, feat, 1)).astype(
        jnp.bfloat16
    )
    return (mixed, fresh_keys, fresh_values)


def solution(mesh):
    n_ep, n_tp = mesh.devices.shape
    split = Mesh(mesh.devices.reshape(n_ep, n_tp // 2, 2), ("ep", "y", "core"))
    placed = (
        P("ep", None),
        P(),
        P(TP, None),
        P(TP, None),
        P(TP, None),
        P(TP),
        P("ep", TP, None),
        P("ep", TP, None),
        P("ep"),
        P(TP, None),
        P(),
        P(),
        P(),
        P("ep", None),
        P("ep", None, TP),
        P("ep", None, TP),
        P("ep", TP, None),
        P(),
        P(TP, "ep"),
        P(TP, "ep"),
        P("ep", TP),
    )
    return jax.shard_map(
        local,
        mesh=split,
        in_specs=placed,
        out_specs=(P("ep", TP), P("ep", TP), P("ep", TP)),
        check_vma=False,
    )
```

time: 141 us -> 139 us (0.986)
  matrix products: 11.7 us -> 1.31 us
  Pallas kernels: 0 us -> 7.81 us
  waiting for transfers between devices: 41.7 us -> 49.4 us
  local copies, waits for them, and re-layouts: 12.4 us -> 7.97 us
  other arithmetic: 9.34 us -> 5.96 us
    dot_general x13 -> x1, matrix products: 10.7 us -> 0.25 us  [local(): jnp.dot(taken, returned.reshape(n_ep * stride, feat), preferred_element_t...]
    pallas_call x0 -> x2, Pallas kernels: none -> 7.81 us  [the longest x1 3.97 us: attend(): pl.pallas_call(attend_kernel, out_shape=(jax.ShapeDtypeStruct((n_tp, rows...]
    all_to_all x5, waiting for transfers between devices: 41.7 us -> 49.4 us  [exchange(): return lax.all_to_all(array, axis, 0, 0, tiled=True)]
    unnamed x62 -> x18, local copies, waits for them, and re-layouts: 7.03 us -> 1.97 us
    all_to_all x5, starting transfers between devices: 43.8 us -> 46.2 us  [exchange(): return lax.all_to_all(array, axis, 0, 0, tiled=True)]
    ppermute x1, starting transfers between devices: 4.39 us -> 2.14 us  [local(): other_down = lax.ppermute(expert_down[0], 'core', swap)]
    concatenate x2 -> x1, local copies, waits for them, and re-layouts: 0.75 us -> 2.89 us  [local(): jnp.concatenate([dense_terms.reshape(n_y, share, lanes), jnp.broadcast_to...]
    concatenate x3 -> x2, other arithmetic: 1.72 us -> 0.11 us  [the longest x1 0.1 us: local(): jnp.concatenate(taken, 0).astype(jnp.bfloat16)]
  transfers between devices with their start and end apart: 8 -> 8, of which waited for: 5 -> 4; matrix products, arithmetic and copies ran while one was open for 10% -> 5% of each run, Pallas kernels for 0% -> 0%
where the time goes in v4:
time: 139 us; the launch traced here: 138 us
  starting transfers between devices  52.6 us (38%)
  waiting for transfers between devices  49.4 us (36%)
  blocking collectives  10.8 us (8%)
  local copies, waits for them, and re-layouts  7.97 us (6%)
  Pallas kernels  7.81 us (6%)
  other arithmetic  5.96 us (4%)
  between operations  1.83 us (1%)
    all_to_all x5, waiting for transfers between devices, exchange(): return lax.all_to_all(array, axis, 0, 0, tiled=True)  49.4 us
    all_to_all x5, starting transfers between devices, exchange(): return lax.all_to_all(array, axis, 0, 0, tiled=True)  46.2 us
    all_gather x1, blocking collectives, local(): mixture = jnp.sum(lax.all_gather(jnp.concatenate(mixture, 1), 'core'), 0)  6.8 us
    pallas_call x1, Pallas kernels, attend(): pl.pallas_call(attend_kernel, out_shape=(jax.ShapeDtypeStruct((n_tp, rows...  3.97 us
    pallas_call x1, Pallas kernels, run_expert(): pl.pallas_call(expert_kernel, out_shape=(jax.ShapeDtypeStruct((n_y, 2 * n...  3.84 us
    concatenate x1, local copies, waits for them, and re-layouts, local(): jnp.concatenate([dense_terms.reshape(n_y, share, lanes), jnp.broadcast_to...  2.89 us
  transfers between devices with their start and end apart: 8, of which 4 were waited for; matrix products, arithmetic and copies ran while one was open for 5% of the time, Pallas kernels for 0%

profile of v4, /device:TPU:1, one launch (start us, length us, event | category | flops | bytes accessed | tf_op | source)
XLA Modules:
  0.0 137.7 jit_solution(11377398534077766621)
XLA Ops:
  1.4 4.0 %attend.1 = (bf16[16,24,128]{2,1,0:T(8,128)(2,1)}, bf16[20,64]{1,0:T(8,128)(2,1)}, bf16[20,64]{1,0:T(8,128)(2,1)}) custom-call(f32[1]{0:T(128)S(6)} %copy.89.offset_ref, s32[20]{0:T(128)} %lengths_ref.1, bf16[20,2048]{1,0:T(8,128)(2,1)} %stream_ref.1, bf16[2048]{0:T(1024)(128)(2,1)} %gain_ref.2, bf16[64,2048]{1,0:T(8,128)(2,1)} %query_ref.1, ...), custom_call_target="tpu_custom_call" | custom-call | tf_op jit(solution)/shard_map/attend/pallas_call | solution.py:81
  5.3 13.8 %all-to-all-start = ((bf16[16,24,128]{2,1,0:T(8,128)(2,1)}), bf16[16,24,128]{2,1,0:T(8,128)(2,1)S(1)}, u32[]{:S(2)}, u32[]{:S(2)}) async-start(bf16[16,24,128]{2,1,0:T(8,128)(2,1)} %get-tuple-element.12), calls=%async_computation | async-start | bytes 196608 | tf_op jit(solution)/shard_map/all_to_all | solution.py:205
  19.1 2.1 %collective-permute-start = (bf16[2048,256]{1,0:T(8,128)(2,1)S(1)}, bf16[2048,256]{1,0:T(8,128)(2,1)}, u32[]{:S(2)}, u32[]{:S(2)}) collective-permute-start(bf16[2048,256]{1,0:T(8,128)(2,1)S(1)} %bitcast.98), channel_id=1, source_target_pairs={{0,1},{1,0},{2,3},{3,2},{4,5},{5,4},{6,7},{7,6},{8,9},{9,8},{10,11... | collective-permute-start | bytes 3145736 | tf_op jit(solution)/shard_map/swap_gate/ppermute | solution.py:258
  21.3 2.2 %collective-permute-start.1 = (bf16[2048,256]{1,0:T(8,128)(2,1)S(1)}, bf16[2048,256]{1,0:T(8,128)(2,1)}, u32[]{:S(2)}, u32[]{:S(2)}) collective-permute-start(bf16[2048,256]{1,0:T(8,128)(2,1)S(1)} %bitcast.103), channel_id=1, source_target_pairs={{0,1},{1,0},{2,3},{3,2},{4,5},{5,4},{6,7},{7,6},{8,9},{9,8},{10,11... | collective-permute-start | bytes 3145736 | tf_op jit(solution)/shard_map/swap_up/ppermute | solution.py:260
  23.5 2.1 %collective-permute-start.2 = (bf16[256,2048]{1,0:T(8,128)(2,1)}, bf16[256,2048]{1,0:T(8,128)(2,1)}, u32[]{:S(2)}, u32[]{:S(2)}) collective-permute-start(bf16[256,2048]{1,0:T(8,128)(2,1)} %bitcast.104), channel_id=1, source_target_pairs={{0,1},{1,0},{2,3},{3,2},{4,5},{5,4},{6,7},{7,6},{8,9},{9,8},{10,11... | collective-permute-start | bytes 3145736 | tf_op jit(solution)/shard_map/swap_down/ppermute | solution.py:262
  25.6 0.7 copy-done.7
  26.7 0.2 select_reduce_fusion
  27.2 0.6 copy-done.2
  27.9 0.7 constant_dynamic-slice_fusion.1
  28.6 0.1 fusion.16
  28.9 0.4 copy-done.6
  29.3 0.1 copy-done.4
  29.5 0.7 add_convert_fusion.1
  30.3 1.8 %all_gather.15 = bf16[20,256]{1,0:T(8,128)(2,1)S(1)} all-gather(bf16[20,128]{1,0:T(8,128)(2,1)S(1)} %add_convert_fusion.1), channel_id=1, replica_groups=mesh['ep'=48,'y'=8,'core'=2] {'core'}, dimensions={1}, use_global_device_ids=true | all-gather | bytes 15360 | tf_op jit(solution)/shard_map/all_gather | solution.py:293
  32.1 0.2 convolution_convert_fusion.2
  32.5 0.9 pad_maximum_fusion
  33.3 12.8 %all-to-all-start.1 = ((bf16[48,24,128]{2,1,0:T(8,128)(2,1)}), bf16[48,24,128]{2,1,0:T(8,128)(2,1)S(1)}, u32[]{:S(2)}, u32[]{:S(2)}) async-start(bf16[48,24,128]{2,1,0:T(8,128)(2,1)} %pad_maximum_fusion), calls=%async_computation.1 | async-start | bytes 589824 | tf_op jit(solution)/shard_map/all_to_all | solution.py:205
  46.2 0.8 dynamic_slice.26
  46.9 2.2 %all-gather = bf16[256,384]{1,0:T(8,128)(2,1)S(1)} all-gather(bf16[128,384]{1,0:T(8,128)(2,1)S(1)} %pad_maximum_fusion.2), channel_id=2, replica_groups=mesh['ep'=48,'y'=8,'core'=2] {'core'}, dimensions={0}, use_global_device_ids=true | all-gather | bytes 294912 | tf_op jit(solution)/shard_map/dense_gather/all_gather | solution.py:264
  49.1 0.1 fusion.10
  49.3 0.2 select_reduce_fusion.2
  49.7 0.1 multiply_reduce_fusion
  50.0 0.1 reshape.270
  50.2 13.4 %all-to-all-done.1 = bf16[48,24,128]{2,1,0:T(8,128)(2,1)S(1)} async-done(((bf16[48,24,128]{2,1,0:T(8,128)(2,1)}), bf16[48,24,128]{2,1,0:T(8,128)(2,1)S(1)}, u32[]{:S(2)}, u32[]{:S(2)}) %all-to-all-start.1) | async-done | bytes 294944 | tf_op jit(solution)/shard_map/all_to_all | solution.py:205
  63.7 0.3 fusion.4
  64.2 0.2 fusion.9
  64.4 0.2 fusion
  64.7 2.9 %concatenate.32 = bf16[8,112,256]{2,1,0:T(8,128)(2,1)} concatenate(bf16[8,60,256]{2,1,0:T(8,128)(2,1)S(1)} %reshape.269, bf16[8,2,256]{2,1,0:T(2,128)(2,1)S(1)} %broadcast_in_dim.62, bf16[8,1,256]{2,1,0:T(2,128)(2,1)S(1)} %pad.20, bf16[8,1,256]{2,1,0:T(2,128)(2,1)S(1)} %pad.21, bf16[8,48,256]{2,1,0:T(8,128)(2,1)S(1)} %broadcast_in_dim.64), dimensions={1} | concatenate | bytes 917504 | tf_op jit(solution)/shard_map/concatenate | solution.py:374
  67.6 6.5 %all-to-all-start.2 = ((bf16[8,112,256]{2,1,0:T(8,128)(2,1)}), bf16[8,112,256]{2,1,0:T(8,128)(2,1)S(1)}, u32[]{:S(2)}, u32[]{:S(2)}) async-start(bf16[8,112,256]{2,1,0:T(8,128)(2,1)} %concatenate.32), calls=%async_computation.2 | async-start | bytes 917504 | tf_op jit(solution)/shard_map/all_to_all | solution.py:205
  74.2 0.1 fusion.5
  74.4 12.8 %all-to-all-done.2.gathered_ref = bf16[8,112,256]{2,1,0:T(8,128)(2,1)S(1)} async-done(((bf16[8,112,256]{2,1,0:T(8,128)(2,1)}), bf16[8,112,256]{2,1,0:T(8,128)(2,1)S(1)}, u32[]{:S(2)}, u32[]{:S(2)}) %all-to-all-start.2) | async-done | bytes 458784 | tf_op jit(solution)/shard_map/all_to_all | solution.py:205
  87.2 3.8 %expert.1 = (bf16[8,160,128]{2,1,0:T(8,128)(2,1)}, f32[4,256]{1,0:T(4,128)S(1)}) custom-call(bf16[8,112,256]{2,1,0:T(8,128)(2,1)S(1)} %all-to-all-done.2.gathered_ref, bf16[2048]{0:T(1024)(128)(2,1)S(1)} %copy-done.2, bf16[2048,256]{1,0:T(8,128)(2,1)S(1)} %bitcast.99, bf16[2048,256]{1,0:T(8,128)(2,1)} %bitcast.102, bf16[256,2048]{1,0:T(8,128)(2,1)} %bitcast.105, ...), custom_call_target="tpu_custom_call" | custom-call | tf_op jit(solution)/shard_map/expert/pallas_call | solution.py:188
  91.0 3.9 %all-to-all-start.3 = ((bf16[8,160,128]{2,1,0:T(8,128)(2,1)}), bf16[8,160,128]{2,1,0:T(8,128)(2,1)S(1)}, u32[]{:S(2)}, u32[]{:S(2)}) async-start(bf16[8,160,128]{2,1,0:T(8,128)(2,1)} %get-tuple-element.18), calls=%async_computation.3 | async-start | bytes 655360 | tf_op jit(solution)/shard_map/all_to_all | solution.py:205
  94.9 0.1 fusion.7
  95.0 0.1 fusion.8
  95.2 9.7 %all-to-all-done.3 = bf16[8,160,128]{2,1,0:T(8,128)(2,1)S(1)} async-done(((bf16[8,160,128]{2,1,0:T(8,128)(2,1)}), bf16[8,160,128]{2,1,0:T(8,128)(2,1)S(1)}, u32[]{:S(2)}, u32[]{:S(2)}) %all-to-all-start.3) | async-done | bytes 327712 | tf_op jit(solution)/shard_map/all_to_all | solution.py:205
  105.0 0.2 convolution_convert_fusion.1
  105.2 0.2 convolution_convert_fusion
  105.5 0.9 pad_maximum_fusion.1
  106.4 9.2 %all-to-all-start.4 = ((bf16[48,24,128]{2,1,0:T(8,128)(2,1)}), bf16[48,24,128]{2,1,0:T(8,128)(2,1)S(1)}, u32[]{:S(2)}, u32[]{:S(2)}) async-start(bf16[48,24,128]{2,1,0:T(8,128)(2,1)} %pad_maximum_fusion.1), calls=%async_computation.4 | async-start | bytes 589824 | tf_op jit(solution)/shard_map/all_to_all | solution.py:205
  115.6 0.2 fusion.33
  115.9 0.2 fusion.35
  116.1 0.2 fusion.36
  116.4 0.2 slice_reduce_fusion.2
  116.6 13.4 %all-to-all-done.4 = bf16[48,24,128]{2,1,0:T(8,128)(2,1)S(1)} async-done(((bf16[48,24,128]{2,1,0:T(8,128)(2,1)}), bf16[48,24,128]{2,1,0:T(8,128)(2,1)S(1)}, u32[]{:S(2)}, u32[]{:S(2)}) %all-to-all-start.4) | async-done | bytes 294944 | tf_op jit(solution)/shard_map/all_to_all | solution.py:205
  130.0 0.3 fusion.52
  130.3 6.8 %all-gather.2 = f32[2,20,256]{2,1,0:T(8,128)S(1)} all-gather(f32[1,20,256]{2,1,0:T(8,128)S(1)} %maximum_bitcast_fusion), channel_id=3, replica_groups=mesh['ep'=48,'y'=8,'core'=2] {'core'}, dimensions={0}, use_global_device_ids=true | all-gather | bytes 61440 | tf_op jit(solution)/shard_map/all_gather | solution.py:448
  137.1 0.6 add_convert_fusion
  (82 shorter events, 2.7 us)
Async XLA Ops:
  0.6 27.3 %copy-start = (bf16[2048,48]{0,1:T(8,128)(2,1)S(1)}, bf16[2048,48]{0,1:T(8,128)(2,1)}, u32[]{:S(2)}) copy-start(bf16[2048,48]{0,1:T(8,128)(2,1)} %param.33) | copy-start | bytes 589828
  1.3 17.8 %copy-start.1 = (bf16[1,2048,256]{2,1,0:T(8,128)(2,1)S(1)}, bf16[1,2048,256]{2,1,0:T(8,128)(2,1)}, u32[]{:S(2)}) copy-start(bf16[1,2048,256]{2,1,0:T(8,128)(2,1)} %param.35) | copy-start | bytes 3145732
  1.3 19.9 %copy-start.3 = (bf16[1,2048,256]{2,1,0:T(8,128)(2,1)S(1)}, bf16[1,2048,256]{2,1,0:T(8,128)(2,1)}, u32[]{:S(2)}) copy-start(bf16[1,2048,256]{2,1,0:T(8,128)(2,1)} %param.36) | copy-start | bytes 3145732
  5.3 24.2 %all-to-all-start = ((bf16[16,24,128]{2,1,0:T(8,128)(2,1)}), bf16[16,24,128]{2,1,0:T(8,128)(2,1)S(1)}, u32[]{:S(2)}, u32[]{:S(2)}) async-start(bf16[16,24,128]{2,1,0:T(8,128)(2,1)} %get-tuple-element.12), calls=%async_computation | async-start | bytes 196608 | tf_op jit(solution)/shard_map/all_to_all | solution.py:205
  19.1 31.1 %collective-permute-start = (bf16[2048,256]{1,0:T(8,128)(2,1)S(1)}, bf16[2048,256]{1,0:T(8,128)(2,1)}, u32[]{:S(2)}, u32[]{:S(2)}) collective-permute-start(bf16[2048,256]{1,0:T(8,128)(2,1)S(1)} %bitcast.98), channel_id=1, source_target_pairs={{0,1},{1,0},{2,3},{3,2},{4,5},{5,4},{6,7},{7,6},{8,9},{9,8},{10,11... | collective-permute-start | bytes 3145736 | tf_op jit(solution)/shard_map/swap_gate/ppermute | solution.py:258
  21.3 28.9 %collective-permute-start.1 = (bf16[2048,256]{1,0:T(8,128)(2,1)S(1)}, bf16[2048,256]{1,0:T(8,128)(2,1)}, u32[]{:S(2)}, u32[]{:S(2)}) collective-permute-start(bf16[2048,256]{1,0:T(8,128)(2,1)S(1)} %bitcast.103), channel_id=1, source_target_pairs={{0,1},{1,0},{2,3},{3,2},{4,5},{5,4},{6,7},{7,6},{8,9},{9,8},{10,11... | collective-permute-start | bytes 3145736 | tf_op jit(solution)/shard_map/swap_up/ppermute | solution.py:260
  23.5 26.7 %collective-permute-start.2 = (bf16[256,2048]{1,0:T(8,128)(2,1)}, bf16[256,2048]{1,0:T(8,128)(2,1)}, u32[]{:S(2)}, u32[]{:S(2)}) collective-permute-start(bf16[256,2048]{1,0:T(8,128)(2,1)} %bitcast.104), channel_id=1, source_target_pairs={{0,1},{1,0},{2,3},{3,2},{4,5},{5,4},{6,7},{7,6},{8,9},{9,8},{10,11... | collective-permute-start | bytes 3145736 | tf_op jit(solution)/shard_map/swap_down/ppermute | solution.py:262
  25.6 0.7 copy-start.7
  27.1 0.7 copy-start.2
  28.6 0.8 copy-start.6
  28.7 0.8 copy-start.4
  28.7 0.8 copy-start.5
  33.3 30.3 %all-to-all-start.1 = ((bf16[48,24,128]{2,1,0:T(8,128)(2,1)}), bf16[48,24,128]{2,1,0:T(8,128)(2,1)S(1)}, u32[]{:S(2)}, u32[]{:S(2)}) async-start(bf16[48,24,128]{2,1,0:T(8,128)(2,1)} %pad_maximum_fusion), calls=%async_computation.1 | async-start | bytes 589824 | tf_op jit(solution)/shard_map/all_to_all | solution.py:205
  67.6 19.5 %all-to-all-start.2 = ((bf16[8,112,256]{2,1,0:T(8,128)(2,1)}), bf16[8,112,256]{2,1,0:T(8,128)(2,1)S(1)}, u32[]{:S(2)}, u32[]{:S(2)}) async-start(bf16[8,112,256]{2,1,0:T(8,128)(2,1)} %concatenate.32), calls=%async_computation.2 | async-start | bytes 917504 | tf_op jit(solution)/shard_map/all_to_all | solution.py:205
  91.0 13.9 %all-to-all-start.3 = ((bf16[8,160,128]{2,1,0:T(8,128)(2,1)}), bf16[8,160,128]{2,1,0:T(8,128)(2,1)S(1)}, u32[]{:S(2)}, u32[]{:S(2)}) async-start(bf16[8,160,128]{2,1,0:T(8,128)(2,1)} %get-tuple-element.18), calls=%async_computation.3 | async-start | bytes 655360 | tf_op jit(solution)/shard_map/all_to_all | solution.py:205
  106.4 23.6 %all-to-all-start.4 = ((bf16[48,24,128]{2,1,0:T(8,128)(2,1)}), bf16[48,24,128]{2,1,0:T(8,128)(2,1)S(1)}, u32[]{:S(2)}, u32[]{:S(2)}) async-start(bf16[48,24,128]{2,1,0:T(8,128)(2,1)} %pad_maximum_fusion.1), calls=%async_computation.4 | async-start | bytes 589824 | tf_op jit(solution)/shard_map/all_to_all | solution.py:205

commit v5 on v4

--- a/solution.py
+++ b/solution.py
@@ -4,6 +4,7 @@
 from jax.experimental import pallas as pl
 from jax.experimental.pallas import tpu as pltpu
 from jax.sharding import Mesh, PartitionSpec as P
+
 
 epsilon = 1e-06
 TP = ("y", "core")
@@ -30,7 +31,7 @@
     fresh_keys_ref,
     fresh_values_ref,
 ):
-    count, width = stream_ref.shape
+    count, _ = stream_ref.shape
     head_size, cache_len = keys_ref.shape[1:]
     n_blocks, rows, feat = terms_ref.shape
     stream_f = stream_ref[...].astype(jnp.float32)
@@ -89,6 +90,65 @@
         out_specs=(whole, whole, whole),
         name="attend",
     )(offset, lengths, stream, gain, query_w, key_w, value_w, keys, values, out_weight)
+
+
+def spread_kernel(arrived_ref, gain_ref, dense_in_ref, home_ref, out_ref, wide_ref, rows_ref, block_ref):
+    n_ep, _, feat = arrived_ref.shape
+    n_y, rows_out, lanes = out_ref.shape
+    at_expert = rows_out - n_ep
+    share = at_expert - 4
+    total = n_y * share
+    part = total // n_ep
+    wide_ref[...] = arrived_ref[...].astype(jnp.float32)
+    for b in range(n_ep):
+        for k in range(2):
+            rows_ref[k, pl.ds(b * part, part)] = wide_ref[b, pl.ds(k * part, part)]
+            rows_ref[k, pl.ds(total + b, 1)] = wide_ref[b, pl.ds(2 * part + k, 1)]
+    products = jnp.zeros((total, lanes), jnp.float32)
+    squares = jnp.zeros((total, 1), jnp.float32)
+    for k in range(2):
+        rows = rows_ref[k, :total]
+        squares = squares + jnp.sum(rows * rows, 1, keepdims=True)
+        gain = gain_ref[:, k * feat : (k + 1) * feat].astype(jnp.float32)
+        products = products + jnp.dot(
+            (rows * gain).astype(jnp.bfloat16),
+            dense_in_ref[k, :, :lanes],
+            preferred_element_type=jnp.float32,
+        )
+        picked = rows_ref[k, pl.ds(total, n_ep)].astype(jnp.bfloat16)
+        for y in range(n_y):
+            out_ref[y, at_expert:, k * feat : (k + 1) * feat] = picked
+    diagonal = lax.broadcasted_iota(jnp.int32, (share, lanes), 0) == lax.broadcasted_iota(
+        jnp.int32, (share, lanes), 1
+    )
+    for y in range(n_y):
+        part_squares = squares[y * share : (y + 1) * share]
+        line = jnp.sum(jnp.where(diagonal, part_squares, 0.0), 0, keepdims=True)
+        high = line.astype(jnp.bfloat16).astype(jnp.float32)
+        block_ref[y, pl.ds(0, share)] = products[y * share : (y + 1) * share]
+        block_ref[y, pl.ds(share, 2)] = home_ref[...]
+        block_ref[y, pl.ds(share + 2, 1)] = high
+        block_ref[y, pl.ds(share + 3, 1)] = line - high
+        out_ref[y, :at_expert] = block_ref[y].astype(jnp.bfloat16)
+
+
+def spread(arrived, gain, dense_in, home, n_y, share):
+    n_ep, _, feat = arrived.shape
+    lanes = home.shape[1]
+    whole = pl.BlockSpec(memory_space=pltpu.VMEM)
+    return pl.pallas_call(
+        spread_kernel,
+        out_shape=jax.ShapeDtypeStruct((n_y, share + 4 + n_ep, lanes), jnp.bfloat16),
+        in_specs=[whole] * 4,
+        out_specs=whole,
+        scratch_shapes=[
+            pltpu.VMEM(arrived.shape, jnp.float32),
+            pltpu.VMEM((2, n_y * share + n_ep, feat), jnp.float32),
+            pltpu.VMEM((n_y, share + 4, lanes), jnp.float32),
+        ],
+        compiler_params=pltpu.CompilerParams(vmem_limit_bytes=52 * 2**20),
+        name="spread",
+    )(arrived, gain, dense_in, home)
 
 
 def silu(value):
@@ -205,11 +265,6 @@
     return lax.all_to_all(array, axis, 0, 0, tiled=True)
 
 
-def to_pair(value):
-    high = lax.reduce_precision(value, 8, 7)
-    return high.astype(jnp.bfloat16), (value - high).astype(jnp.bfloat16)
-
-
 def round_up(count, unit=8):
     return -(-count // unit) * unit
 
@@ -254,18 +309,13 @@
     wide_offset = lax.axis_index("y") * wide
 
     swap = [(0, 1), (1, 0)]
-    with jax.named_scope("swap_gate"):
-        other_gate = lax.ppermute(expert_gate[0], "core", swap)
-    with jax.named_scope("swap_up"):
-        other_up = lax.ppermute(expert_up[0], "core", swap)
-    with jax.named_scope("swap_down"):
-        other_down = lax.ppermute(expert_down[0], "core", swap)
-    with jax.named_scope("dense_gather"):
-        dense_pair = lax.all_gather(
-            jnp.concatenate([dense_gate, dense_up, dense_down], 1), "core"
-        )
+    other_gate = lax.ppermute(expert_gate[0], "core", swap)
+    other_up = lax.ppermute(expert_up[0], "core", swap)
+    other_down = lax.ppermute(expert_down[0], "core", swap)
+    dense_pair = lax.all_gather(
+        jnp.concatenate([dense_gate, dense_up, dense_down], 1), "core"
+    )
     units = dense_gate.shape[1]
-    dense_in = dense_pair[:, :, : 2 * units]
     dense_out = dense_pair[:, :, 2 * units :]
     rows_pad = round_up(seq_count)
 
@@ -311,27 +361,19 @@
     own_rows = lax.dynamic_slice_in_dim(pair, core * part, part, 0)
     both = seq_count + n_core
     spare = (round_up(both) - seq_count) // n_core
-    arrived = exchange(
-        jnp.concatenate(
-            [
-                jnp.broadcast_to(own_rows[None, :, :feat], (n_ep, part, feat)),
-                jnp.broadcast_to(own_rows[None, :, feat:], (n_ep, part, feat)),
-                jnp.tile(send.reshape(n_ep, n_core, feat), (1, spare, 1)),
-            ],
-            1,
-        ),
-        "ep",
-    )
+    leaving = jnp.concatenate(
+        [
+            jnp.broadcast_to(own_rows[None, :, :feat], (n_ep, part, feat)),
+            jnp.broadcast_to(own_rows[None, :, feat:], (n_ep, part, feat)),
+            jnp.tile(send.reshape(n_ep, n_core, feat), (1, spare, 1)),
+        ],
+        1,
+    )
+    arrived = exchange(leaving, "ep")
     arrived, other_gate, other_up, other_down = lax.optimization_barrier(
         (arrived, other_gate, other_up, other_down)
     )
     total = n_ep * part
-    rows = [
-        arrived[:, :part].reshape(total, feat).astype(jnp.float32),
-        arrived[:, part:seq_count].reshape(total, feat).astype(jnp.float32),
-    ]
-    picked = arrived[:, seq_count:both].reshape(n_ep, wide)
-
     home_weights = jnp.concatenate(
         [
             lax.dynamic_slice_in_dim(group_weight, wide_offset, wide, 0),
@@ -353,36 +395,16 @@
     )
     home_count = home_part.shape[1]
 
-    gain_ffn = norm_gain_ffn.astype(jnp.float32)
-    gain_wide = lax.dynamic_slice_in_dim(gain_ffn, wide_offset, wide, 0)
+    gain_wide = lax.dynamic_slice_in_dim(norm_gain_ffn, wide_offset, wide, 0)[None]
     share = total // n_y
-    dense_terms = jnp.zeros((total, 2 * units), jnp.float32)
-    for k in range(n_core):
-        scaled = (rows[k] * gain_wide[k * feat : (k + 1) * feat]).astype(jnp.bfloat16)
-        dense_terms += jnp.dot(scaled, dense_in[k], preferred_element_type=jnp.float32)
-    dense_terms = dense_terms.astype(jnp.bfloat16)
-    squares_part = sum(jnp.sum(r * r, 1) for r in rows)
-    squares_high, squares_low = to_pair(squares_part.reshape(n_y, 1, share))
-    home_high, home_low = to_pair(home_part.reshape(1, seq_count * home_count))
     lanes = 2 * units
-
-    def lane_pad(array):
-        return jnp.pad(array, [(0, 0)] * (array.ndim - 1) + [(0, lanes - array.shape[-1])])
-
-    home_rows = jnp.concatenate([lane_pad(home_high), lane_pad(home_low)], 0)
-    gathered = exchange(
-        jnp.concatenate(
-            [
-                dense_terms.reshape(n_y, share, lanes),
-                jnp.broadcast_to(home_rows[None], (n_y, *home_rows.shape)),
-                lane_pad(squares_high),
-                lane_pad(squares_low),
-                jnp.broadcast_to(picked[None], (n_y, *picked.shape)),
-            ],
-            1,
-        ),
-        "y",
-    )
+    flat = jnp.pad(
+        home_part.reshape(1, seq_count * home_count), ((0, 0), (0, lanes - seq_count * home_count))
+    )
+    high = lax.reduce_precision(flat, 8, 7)
+    home_rows = jnp.concatenate([high, flat - high], 0)
+    leaving = spread(arrived, gain_wide, dense_pair, home_rows, n_y, share)
+    gathered = exchange(leaving, "y")
 
     leaving, sums = run_expert(
         gathered,

time: 139 us -> 138 us (level)
  local copies, waits for them, and re-layouts: 7.97 us -> 4.27 us
  waiting for transfers between devices: 49.4 us -> 52.4 us
    all_to_all x5, waiting for transfers between devices: 49.4 us -> 52.4 us  [exchange(): return lax.all_to_all(array, axis, 0, 0, tiled=True)]
    concatenate x1 -> x0, local copies, waits for them, and re-layouts: 2.89 us -> none  [local(): jnp.concatenate([dense_terms.reshape(n_y, share, lanes), jnp.broadcast_to...]
where the time goes in v5:
time: 138 us; the launch traced here: 137 us
  starting transfers between devices  52.6 us (38%)
  waiting for transfers between devices  52.4 us (38%)
  blocking collectives  10.5 us (8%)
  Pallas kernels  8.94 us (6%)
  other arithmetic  5.58 us (4%)
  local copies, waits for them, and re-layouts  4.27 us (3%)
  between operations  1.75 us (1%)
    all_to_all x5, waiting for transfers between devices, exchange(): return lax.all_to_all(array, axis, 0, 0, tiled=True)  52.4 us
    all_to_all x5, starting transfers between devices, exchange(): return lax.all_to_all(array, axis, 0, 0, tiled=True)  46.1 us
    all_gather x1, blocking collectives, local(): mixture = jnp.sum(lax.all_gather(jnp.concatenate(mixture, 1), 'core'), 0)  6.78 us
    pallas_call x1, Pallas kernels, attend(): pl.pallas_call(attend_kernel, out_shape=(jax.ShapeDtypeStruct((n_tp, rows...  3.97 us
    pallas_call x1, Pallas kernels, run_expert(): pl.pallas_call(expert_kernel, out_shape=(jax.ShapeDtypeStruct((n_y, 2 * n...  3.84 us
  transfers between devices with their start and end apart: 8, of which 4 were waited for; matrix products, arithmetic and copies ran while one was open for 5% of the time, Pallas kernels for 0%

profile of v5, /device:TPU:1, one launch (start us, length us, event | category | flops | bytes accessed | tf_op | source)
XLA Modules:
  0.0 137.0 jit_solution(8756892586308945576)
XLA Ops:
  1.4 4.0 %attend.1 = (bf16[16,24,128]{2,1,0:T(8,128)(2,1)}, bf16[20,64]{1,0:T(8,128)(2,1)}, bf16[20,64]{1,0:T(8,128)(2,1)}) custom-call(f32[1]{0:T(128)S(6)} %copy.75.offset_ref, s32[20]{0:T(128)} %lengths_ref.1, bf16[20,2048]{1,0:T(8,128)(2,1)} %stream_ref.1, bf16[2048]{0:T(1024)(128)(2,1)} %gain_ref.2, bf16[64,2048]{1,0:T(8,128)(2,1)} %query_ref.1, ...), custom_call_target="tpu_custom_call" | custom-call | tf_op jit(solution)/shard_map/attend/pallas_call | solution.py:82
  5.3 13.8 %all-to-all-start = ((bf16[16,24,128]{2,1,0:T(8,128)(2,1)}), bf16[16,24,128]{2,1,0:T(8,128)(2,1)S(1)}, u32[]{:S(2)}, u32[]{:S(2)}) async-start(bf16[16,24,128]{2,1,0:T(8,128)(2,1)} %get-tuple-element.12), calls=%async_computation | async-start | bytes 196608 | tf_op jit(solution)/shard_map/all_to_all | solution.py:265
  19.1 2.1 %collective-permute-start = (bf16[2048,256]{1,0:T(8,128)(2,1)S(1)}, bf16[2048,256]{1,0:T(8,128)(2,1)}, u32[]{:S(2)}, u32[]{:S(2)}) collective-permute-start(bf16[2048,256]{1,0:T(8,128)(2,1)S(1)} %bitcast.86), channel_id=1, source_target_pairs={{0,1},{1,0},{2,3},{3,2},{4,5},{5,4},{6,7},{7,6},{8,9},{9,8},{10,11... | collective-permute-start | bytes 3145736 | tf_op jit(solution)/shard_map/ppermute | solution.py:312
  21.3 2.2 %collective-permute-start.1 = (bf16[2048,256]{1,0:T(8,128)(2,1)S(1)}, bf16[2048,256]{1,0:T(8,128)(2,1)}, u32[]{:S(2)}, u32[]{:S(2)}) collective-permute-start(bf16[2048,256]{1,0:T(8,128)(2,1)S(1)} %bitcast.91), channel_id=1, source_target_pairs={{0,1},{1,0},{2,3},{3,2},{4,5},{5,4},{6,7},{7,6},{8,9},{9,8},{10,11... | collective-permute-start | bytes 3145736 | tf_op jit(solution)/shard_map/ppermute | solution.py:313
  23.5 2.1 %collective-permute-start.2 = (bf16[256,2048]{1,0:T(8,128)(2,1)}, bf16[256,2048]{1,0:T(8,128)(2,1)}, u32[]{:S(2)}, u32[]{:S(2)}) collective-permute-start(bf16[256,2048]{1,0:T(8,128)(2,1)} %bitcast.92), channel_id=1, source_target_pairs={{0,1},{1,0},{2,3},{3,2},{4,5},{5,4},{6,7},{7,6},{8,9},{9,8},{10,11... | collective-permute-start | bytes 3145736 | tf_op jit(solution)/shard_map/ppermute | solution.py:314
  25.7 0.7 constant_dynamic-slice_fusion.1
  26.8 0.2 select_reduce_fusion
  27.4 0.2 copy-done.6
  27.5 0.4 copy-done.4
  28.0 0.1 copy.62
  28.1 0.8 dynamic_slice.26
  28.8 0.7 copy-done.2
  29.6 1.9 %all-gather = bf16[256,384]{1,0:T(8,128)(2,1)S(1)} all-gather(bf16[128,384]{1,0:T(8,128)(2,1)S(1)} %pad_maximum_fusion.2), channel_id=2, replica_groups=mesh['ep'=48,'y'=8,'core'=2] {'core'}, dimensions={0}, use_global_device_ids=true | all-gather | bytes 294912 | tf_op jit(solution)/shard_map/all_gather | solution.py:315
  31.5 0.1 fusion.10
  31.7 0.7 add_convert_fusion.1
  32.4 1.8 %all_gather.15 = bf16[20,256]{1,0:T(8,128)(2,1)S(1)} all-gather(bf16[20,128]{1,0:T(8,128)(2,1)S(1)} %add_convert_fusion.1), channel_id=1, replica_groups=mesh['ep'=48,'y'=8,'core'=2] {'core'}, dimensions={1}, use_global_device_ids=true | all-gather | bytes 15360 | tf_op jit(solution)/shard_map/all_gather | solution.py:343
  34.2 0.2 convolution_convert_fusion.2
  34.6 0.9 pad_maximum_fusion
  35.5 12.8 %all-to-all-start.1 = ((bf16[48,24,128]{2,1,0:T(8,128)(2,1)}), bf16[48,24,128]{2,1,0:T(8,128)(2,1)S(1)}, u32[]{:S(2)}, u32[]{:S(2)}) async-start(bf16[48,24,128]{2,1,0:T(8,128)(2,1)} %pad_maximum_fusion), calls=%async_computation.1 | async-start | bytes 589824 | tf_op jit(solution)/shard_map/all_to_all | solution.py:265
  48.3 0.1 fusion.4
  48.5 0.2 select_reduce_fusion.2
  48.7 0.1 copy.63
  48.9 0.1 multiply_reduce_fusion
  49.0 0.1 copy.65
  49.2 0.1 reshape.153
  49.4 16.4 %all-to-all-done.1.arrived_ref = bf16[48,24,128]{2,1,0:T(8,128)(2,1)S(1)} async-done(((bf16[48,24,128]{2,1,0:T(8,128)(2,1)}), bf16[48,24,128]{2,1,0:T(8,128)(2,1)S(1)}, u32[]{:S(2)}, u32[]{:S(2)}) %all-to-all-start.1) | async-done | bytes 294944 | tf_op jit(solution)/shard_map/all_to_all | solution.py:265
  65.8 1.1 spread.1
  66.9 6.5 %all-to-all-start.2 = ((bf16[8,112,256]{2,1,0:T(8,128)(2,1)}), bf16[8,112,256]{2,1,0:T(8,128)(2,1)S(1)}, u32[]{:S(2)}, u32[]{:S(2)}) async-start(bf16[8,112,256]{2,1,0:T(8,128)(2,1)} %spread.1), calls=%async_computation.2 | async-start | bytes 917504 | tf_op jit(solution)/shard_map/all_to_all | solution.py:265
  73.5 0.1 fusion
  73.6 0.1 fusion.1
  73.7 12.8 %all-to-all-done.2.gathered_ref = bf16[8,112,256]{2,1,0:T(8,128)(2,1)S(1)} async-done(((bf16[8,112,256]{2,1,0:T(8,128)(2,1)}), bf16[8,112,256]{2,1,0:T(8,128)(2,1)S(1)}, u32[]{:S(2)}, u32[]{:S(2)}) %all-to-all-start.2) | async-done | bytes 458784 | tf_op jit(solution)/shard_map/all_to_all | solution.py:265
  86.5 3.8 %expert.1 = (bf16[8,160,128]{2,1,0:T(8,128)(2,1)}, f32[4,256]{1,0:T(4,128)S(1)}) custom-call(bf16[8,112,256]{2,1,0:T(8,128)(2,1)S(1)} %all-to-all-done.2.gathered_ref, bf16[2048]{0:T(1024)(128)(2,1)S(1)} %copy-done.2, bf16[2048,256]{1,0:T(8,128)(2,1)S(1)} %bitcast.87, bf16[2048,256]{1,0:T(8,128)(2,1)} %bitcast.90, bf16[256,2048]{1,0:T(8,128)(2,1)} %bitcast.93, ...), custom_call_target="tpu_custom_call" | custom-call | tf_op jit(solution)/shard_map/expert/pallas_call | solution.py:248
  90.3 3.9 %all-to-all-start.3 = ((bf16[8,160,128]{2,1,0:T(8,128)(2,1)}), bf16[8,160,128]{2,1,0:T(8,128)(2,1)S(1)}, u32[]{:S(2)}, u32[]{:S(2)}) async-start(bf16[8,160,128]{2,1,0:T(8,128)(2,1)} %get-tuple-element.18), calls=%async_computation.3 | async-start | bytes 655360 | tf_op jit(solution)/shard_map/all_to_all | solution.py:265
  94.2 0.1 fusion.2
  94.3 0.1 fusion.3
  94.5 9.7 %all-to-all-done.3 = bf16[8,160,128]{2,1,0:T(8,128)(2,1)S(1)} async-done(((bf16[8,160,128]{2,1,0:T(8,128)(2,1)}), bf16[8,160,128]{2,1,0:T(8,128)(2,1)S(1)}, u32[]{:S(2)}, u32[]{:S(2)}) %all-to-all-start.3) | async-done | bytes 327712 | tf_op jit(solution)/shard_map/all_to_all | solution.py:265
  104.3 0.2 convolution_convert_fusion.1
  104.5 0.2 convolution_convert_fusion
  104.8 0.9 pad_maximum_fusion.1
  105.7 9.2 %all-to-all-start.4 = ((bf16[48,24,128]{2,1,0:T(8,128)(2,1)}), bf16[48,24,128]{2,1,0:T(8,128)(2,1)S(1)}, u32[]{:S(2)}, u32[]{:S(2)}) async-start(bf16[48,24,128]{2,1,0:T(8,128)(2,1)} %pad_maximum_fusion.1), calls=%async_computation.4 | async-start | bytes 589824 | tf_op jit(solution)/shard_map/all_to_all | solution.py:265
  114.9 0.2 fusion.27
  115.1 0.2 fusion.29
  115.3 0.2 fusion.30
  115.6 0.2 slice_reduce_fusion.2
  115.8 13.4 %all-to-all-done.4 = bf16[48,24,128]{2,1,0:T(8,128)(2,1)S(1)} async-done(((bf16[48,24,128]{2,1,0:T(8,128)(2,1)}), bf16[48,24,128]{2,1,0:T(8,128)(2,1)S(1)}, u32[]{:S(2)}, u32[]{:S(2)}) %all-to-all-start.4) | async-done | bytes 294944 | tf_op jit(solution)/shard_map/all_to_all | solution.py:265
  129.2 0.3 fusion.43
  129.6 6.8 %all-gather.2 = f32[2,20,256]{2,1,0:T(8,128)S(1)} all-gather(f32[1,20,256]{2,1,0:T(8,128)S(1)} %maximum_bitcast_fusion), channel_id=3, replica_groups=mesh['ep'=48,'y'=8,'core'=2] {'core'}, dimensions={0}, use_global_device_ids=true | all-gather | bytes 61440 | tf_op jit(solution)/shard_map/all_gather | solution.py:470
  136.4 0.6 add_convert_fusion
  (65 shorter events, 2.0 us)
Async XLA Ops:
  0.6 25.1 %copy-start = (bf16[2048,48]{0,1:T(8,128)(2,1)S(1)}, bf16[2048,48]{0,1:T(8,128)(2,1)}, u32[]{:S(2)}) copy-start(bf16[2048,48]{0,1:T(8,128)(2,1)} %param.33) | copy-start | bytes 589828
  1.3 17.8 %copy-start.1 = (bf16[1,2048,256]{2,1,0:T(8,128)(2,1)S(1)}, bf16[1,2048,256]{2,1,0:T(8,128)(2,1)}, u32[]{:S(2)}) copy-start(bf16[1,2048,256]{2,1,0:T(8,128)(2,1)} %param.35) | copy-start | bytes 3145732
  1.3 19.9 %copy-start.3 = (bf16[1,2048,256]{2,1,0:T(8,128)(2,1)S(1)}, bf16[1,2048,256]{2,1,0:T(8,128)(2,1)}, u32[]{:S(2)}) copy-start(bf16[1,2048,256]{2,1,0:T(8,128)(2,1)} %param.36) | copy-start | bytes 3145732
  5.3 26.3 %all-to-all-start = ((bf16[16,24,128]{2,1,0:T(8,128)(2,1)}), bf16[16,24,128]{2,1,0:T(8,128)(2,1)S(1)}, u32[]{:S(2)}, u32[]{:S(2)}) async-start(bf16[16,24,128]{2,1,0:T(8,128)(2,1)} %get-tuple-element.12), calls=%async_computation | async-start | bytes 196608 | tf_op jit(solution)/shard_map/all_to_all | solution.py:265
  19.1 30.2 %collective-permute-start = (bf16[2048,256]{1,0:T(8,128)(2,1)S(1)}, bf16[2048,256]{1,0:T(8,128)(2,1)}, u32[]{:S(2)}, u32[]{:S(2)}) collective-permute-start(bf16[2048,256]{1,0:T(8,128)(2,1)S(1)} %bitcast.86), channel_id=1, source_target_pairs={{0,1},{1,0},{2,3},{3,2},{4,5},{5,4},{6,7},{7,6},{8,9},{9,8},{10,11... | collective-permute-start | bytes 3145736 | tf_op jit(solution)/shard_map/ppermute | solution.py:312
  21.3 28.1 %collective-permute-start.1 = (bf16[2048,256]{1,0:T(8,128)(2,1)S(1)}, bf16[2048,256]{1,0:T(8,128)(2,1)}, u32[]{:S(2)}, u32[]{:S(2)}) collective-permute-start(bf16[2048,256]{1,0:T(8,128)(2,1)S(1)} %bitcast.91), channel_id=1, source_target_pairs={{0,1},{1,0},{2,3},{3,2},{4,5},{5,4},{6,7},{7,6},{8,9},{9,8},{10,11... | collective-permute-start | bytes 3145736 | tf_op jit(solution)/shard_map/ppermute | solution.py:313
  23.5 25.9 %collective-permute-start.2 = (bf16[256,2048]{1,0:T(8,128)(2,1)}, bf16[256,2048]{1,0:T(8,128)(2,1)}, u32[]{:S(2)}, u32[]{:S(2)}) collective-permute-start(bf16[256,2048]{1,0:T(8,128)(2,1)} %bitcast.92), channel_id=1, source_target_pairs={{0,1},{1,0},{2,3},{3,2},{4,5},{5,4},{6,7},{7,6},{8,9},{9,8},{10,11... | collective-permute-start | bytes 3145736 | tf_op jit(solution)/shard_map/ppermute | solution.py:314
  25.7 0.7 copy-start.7
  26.8 0.8 copy-start.6
  27.2 0.8 copy-start.4
  27.2 0.8 copy-start.5
  28.8 0.7 copy-start.2
  35.5 30.3 %all-to-all-start.1 = ((bf16[48,24,128]{2,1,0:T(8,128)(2,1)}), bf16[48,24,128]{2,1,0:T(8,128)(2,1)S(1)}, u32[]{:S(2)}, u32[]{:S(2)}) async-start(bf16[48,24,128]{2,1,0:T(8,128)(2,1)} %pad_maximum_fusion), calls=%async_computation.1 | async-start | bytes 589824 | tf_op jit(solution)/shard_map/all_to_all | solution.py:265
  66.9 19.5 %all-to-all-start.2 = ((bf16[8,112,256]{2,1,0:T(8,128)(2,1)}), bf16[8,112,256]{2,1,0:T(8,128)(2,1)S(1)}, u32[]{:S(2)}, u32[]{:S(2)}) async-start(bf16[8,112,256]{2,1,0:T(8,128)(2,1)} %spread.1), calls=%async_computation.2 | async-start | bytes 917504 | tf_op jit(solution)/shard_map/all_to_all | solution.py:265
  90.3 13.9 %all-to-all-start.3 = ((bf16[8,160,128]{2,1,0:T(8,128)(2,1)}), bf16[8,160,128]{2,1,0:T(8,128)(2,1)S(1)}, u32[]{:S(2)}, u32[]{:S(2)}) async-start(bf16[8,160,128]{2,1,0:T(8,128)(2,1)} %get-tuple-element.18), calls=%async_computation.3 | async-start | bytes 655360 | tf_op jit(solution)/shard_map/all_to_all | solution.py:265
  105.7 23.5 %all-to-all-start.4 = ((bf16[48,24,128]{2,1,0:T(8,128)(2,1)}), bf16[48,24,128]{2,1,0:T(8,128)(2,1)S(1)}, u32[]{:S(2)}, u32[]{:S(2)}) async-start(bf16[48,24,128]{2,1,0:T(8,128)(2,1)} %pad_maximum_fusion.1), calls=%async_computation.4 | async-start | bytes 589824 | tf_op jit(solution)/shard_map/all_to_all | solution.py:265

commit v6 on v5

--- a/solution.py
+++ b/solution.py
@@ -22,25 +22,44 @@
     stream_ref,
     gain_ref,
     query_ref,
-    key_ref,
-    value_ref,
+    keys_hbm,
+    values_hbm,
+    out_weight_hbm,
+    terms_ref,
+    normed_ref,
     keys_ref,
     values_ref,
     out_weight_ref,
-    terms_ref,
-    fresh_keys_ref,
-    fresh_values_ref,
+    sems,
 ):
+    copies = [
+        pltpu.make_async_copy(source, target, sems.at[k])
+        for k, (source, target) in enumerate(
+            (
+                (keys_hbm, keys_ref),
+                (values_hbm, values_ref),
+                (out_weight_hbm, out_weight_ref),
+            )
+        )
+    ]
+    for copy in copies:
+        copy.start()
     count, _ = stream_ref.shape
     head_size, cache_len = keys_ref.shape[1:]
     n_blocks, rows, feat = terms_ref.shape
     stream_f = stream_ref[...].astype(jnp.float32)
     inverse = lax.rsqrt(jnp.mean(stream_f * stream_f, -1, keepdims=True) + epsilon)
     normed = (stream_f * inverse * gain_ref[...].astype(jnp.float32)[None]).astype(jnp.bfloat16)
+    normed_ref[...] = normed
     queries = across(normed, query_ref[...])
     queries = jnp.concatenate([queries, jnp.zeros((rows - count, head_size), jnp.float32)], 0)
     queries = queries.astype(jnp.bfloat16)
     row = lax.broadcasted_iota(jnp.int32, (rows, 1), 0)
+    after = (
+        lax.broadcasted_iota(jnp.int32, (cache_len, cache_len), 0)
+        > lax.broadcasted_iota(jnp.int32, (cache_len, cache_len), 1)
+    ).astype(jnp.float32)
+    copies[0].wait()
     scores = jnp.zeros((rows, cache_len), jnp.float32)
     for s in range(count):
         each = jnp.dot(queries, keys_ref[s], preferred_element_type=jnp.float32)
@@ -52,54 +71,128 @@
     inside = lax.broadcasted_iota(jnp.int32, (rows, cache_len), 1) < filled
     tail = jnp.log1p(jnp.exp(-jnp.abs(scores)))
     log_keep = jnp.where(inside, jnp.minimum(-scores, 0.0) - tail, 0.0)
-    after = (
-        lax.broadcasted_iota(jnp.int32, (cache_len, cache_len), 0)
-        > lax.broadcasted_iota(jnp.int32, (cache_len, cache_len), 1)
-    ).astype(jnp.float32)
     remain = jnp.dot(
         log_keep, after, precision=lax.Precision.HIGHEST, preferred_element_type=jnp.float32
     )
     weights = jnp.where(inside, jnp.exp(jnp.minimum(scores, 0.0) - tail + remain), 0.0)
     weights = weights.astype(jnp.bfloat16)
+    copies[1].wait()
     heads_out = jnp.zeros((rows, head_size), jnp.float32)
     for s in range(count):
         heads_out = jnp.where(row == s, across(weights, values_ref[s]), heads_out)
+    copies[2].wait()
     terms = jnp.dot(
         heads_out.astype(jnp.bfloat16), out_weight_ref[...], preferred_element_type=jnp.float32
     ).astype(jnp.bfloat16)
     for k in range(n_blocks):
         terms_ref[k] = terms[:, k * feat : (k + 1) * feat]
-    fresh_keys_ref[...] = across(normed, key_ref[...]).astype(jnp.bfloat16)
-    fresh_values_ref[...] = across(normed, value_ref[...]).astype(jnp.bfloat16)
-
-
-def attend(
-    stream, gain, query_w, key_w, value_w, offset, keys, values, lengths, out_weight, n_tp, rows
-):
+
+
+def attend(stream, gain, query_w, offset, keys, values, lengths, out_weight, n_tp, rows):
     count, width = stream.shape
     whole = pl.BlockSpec(memory_space=pltpu.VMEM)
-    fresh = jax.ShapeDtypeStruct((count, key_w.shape[0]), jnp.bfloat16)
     return pl.pallas_call(
         attend_kernel,
         out_shape=(
             jax.ShapeDtypeStruct((n_tp, rows, width // n_tp), jnp.bfloat16),
-            fresh,
-            fresh,
+            jax.ShapeDtypeStruct((count, width), jnp.bfloat16),
         ),
-        in_specs=[pl.BlockSpec(memory_space=pltpu.SMEM)] * 2 + [whole] * 8,
-        out_specs=(whole, whole, whole),
+        in_specs=[pl.BlockSpec(memory_space=pltpu.SMEM)] * 2
+        + [whole] * 3
+        + [pl.BlockSpec(memory_space=pltpu.HBM)] * 3,
+        out_specs=(whole, whole),
+        scratch_shapes=[
+            pltpu.VMEM(each.shape, jnp.bfloat16) for each in (keys, values, out_weight)
+        ]
+        + [pltpu.SemaphoreType.DMA((3,))],
         name="attend",
-    )(offset, lengths, stream, gain, query_w, key_w, value_w, keys, values, out_weight)
+    )(offset, lengths, stream, gain, query_w, keys, values, out_weight)
+
+
+def pack_kernel(core_ref, pair_ref, dispatch_ref, out_ref, send_ref):
+    n_ep, stride, feat = out_ref.shape
+    part = pair_ref.shape[0] // 2
+    pair = pair_ref[...]
+    send_ref[:n_ep] = jnp.dot(dispatch_ref[...], pair, preferred_element_type=jnp.float32)
+    pair = pair.astype(jnp.float32)
+    mine = jnp.where(core_ref[0] == 0, pair[:part], pair[part:])
+    rest = jnp.zeros((stride - 2 * part, feat), jnp.float32)
+    base = jnp.concatenate([mine[:, :feat], mine[:, feat:], rest], 0)
+    row = lax.broadcasted_iota(jnp.int32, (stride, 1), 0)
+    for b in range(n_ep):
+        block = jnp.where(row == 2 * part, send_ref[pl.ds(b, 1), :feat], base)
+        block = jnp.where(row == 2 * part + 1, send_ref[pl.ds(b, 1), feat:], block)
+        out_ref[b] = block.astype(jnp.bfloat16)
+
+
+def pack(core, pair, dispatch, stride):
+    n_ep = dispatch.shape[0]
+    wide = pair.shape[1]
+    whole = pl.BlockSpec(memory_space=pltpu.VMEM)
+    return pl.pallas_call(
+        pack_kernel,
+        out_shape=jax.ShapeDtypeStruct((n_ep, stride, wide // 2), jnp.bfloat16),
+        in_specs=[pl.BlockSpec(memory_space=pltpu.SMEM), whole, whole],
+        out_specs=whole,
+        scratch_shapes=[pltpu.VMEM((n_ep + guard, wide), jnp.float32)],
+        compiler_params=pltpu.CompilerParams(vmem_limit_bytes=52 * 2**20),
+        name="pack",
+    )(core, pair, dispatch)
+
+
+def merge_kernel(summed_ref, dense_out_ref, out_ref, act_ref, dense_ref, expert_ref, block_ref):
+    n_ep, stride, feat = out_ref.shape
+    n_y, _, _ = summed_ref.shape
+    at_act = 2 * n_ep
+    total = act_ref.shape[0] - guard
+    share = total // n_y
+    part = total // n_ep
+    expert = jnp.zeros((at_act, feat), jnp.float32)
+    for y in range(n_y):
+        expert = expert + summed_ref[y, :at_act].astype(jnp.float32)
+        act_ref[pl.ds(y * share, share)] = summed_ref[y, at_act:].astype(jnp.float32)[:share]
+    expert_ref[:at_act] = expert
+    acts = act_ref[:total].astype(jnp.bfloat16)
+    for k in range(2):
+        dense_ref[k, :total] = jnp.dot(
+            acts, dense_out_ref[k, :, 2 * feat :], preferred_element_type=jnp.float32
+        )
+    block_ref[...] = jnp.zeros_like(block_ref)
+    for b in range(n_ep):
+        for k in range(2):
+            block_ref[b, pl.ds(k * part, part)] = dense_ref[k, pl.ds(b * part, part)]
+            block_ref[b, pl.ds(2 * part + k, 1)] = expert_ref[pl.ds(k * n_ep + b, 1)]
+    out_ref[...] = block_ref[:, :stride].astype(jnp.bfloat16)
+
+
+def merge(summed, dense_pair, n_ep, stride, part):
+    feat = summed.shape[2]
+    total = n_ep * part
+    whole = pl.BlockSpec(memory_space=pltpu.VMEM)
+    return pl.pallas_call(
+        merge_kernel,
+        out_shape=jax.ShapeDtypeStruct((n_ep, stride, feat), jnp.bfloat16),
+        in_specs=[whole, whole],
+        out_specs=whole,
+        scratch_shapes=[
+            pltpu.VMEM((total + guard, feat), jnp.float32),
+            pltpu.VMEM((2, total + guard, feat), jnp.float32),
+            pltpu.VMEM((2 * n_ep + guard, feat), jnp.float32),
+            pltpu.VMEM((n_ep, stride + guard, feat), jnp.float32),
+        ],
+        compiler_params=pltpu.CompilerParams(vmem_limit_bytes=52 * 2**20),
+        name="merge",
+    )(summed, dense_pair)
 
 
 def spread_kernel(arrived_ref, gain_ref, dense_in_ref, home_ref, out_ref, wide_ref, rows_ref, block_ref):
-    n_ep, _, feat = arrived_ref.shape
+    n_ep, stride, feat = arrived_ref.shape
     n_y, rows_out, lanes = out_ref.shape
     at_expert = rows_out - n_ep
     share = at_expert - 4
     total = n_y * share
     part = total // n_ep
-    wide_ref[...] = arrived_ref[...].astype(jnp.float32)
+    wide_ref[:, :stride] = arrived_ref[...].astype(jnp.float32)
     for b in range(n_ep):
         for k in range(2):
             rows_ref[k, pl.ds(b * part, part)] = wide_ref[b, pl.ds(k * part, part)]
@@ -129,11 +222,11 @@
         block_ref[y, pl.ds(share, 2)] = home_ref[...]
         block_ref[y, pl.ds(share + 2, 1)] = high
         block_ref[y, pl.ds(share + 3, 1)] = line - high
-        out_ref[y, :at_expert] = block_ref[y].astype(jnp.bfloat16)
+        out_ref[y, :at_expert] = block_ref[y, :at_expert].astype(jnp.bfloat16)
 
 
 def spread(arrived, gain, dense_in, home, n_y, share):
-    n_ep, _, feat = arrived.shape
+    n_ep, stride, feat = arrived.shape
     lanes = home.shape[1]
     whole = pl.BlockSpec(memory_space=pltpu.VMEM)
     return pl.pallas_call(
@@ -142,13 +235,16 @@
         in_specs=[whole] * 4,
         out_specs=whole,
         scratch_shapes=[
-            pltpu.VMEM(arrived.shape, jnp.float32),
-            pltpu.VMEM((2, n_y * share + n_ep, feat), jnp.float32),
-            pltpu.VMEM((n_y, share + 4, lanes), jnp.float32),
+            pltpu.VMEM((n_ep, stride + guard, feat), jnp.float32),
+            pltpu.VMEM((2, n_y * share + n_ep + guard, feat), jnp.float32),
+            pltpu.VMEM((n_y, share + 4 + guard, lanes), jnp.float32),
         ],
         compiler_params=pltpu.CompilerParams(vmem_limit_bytes=52 * 2**20),
         name="spread",
     )(arrived, gain, dense_in, home)
+
+
+guard = 8
 
 
 def silu(value):
@@ -316,15 +412,15 @@
         jnp.concatenate([dense_gate, dense_up, dense_down], 1), "core"
     )
     units = dense_gate.shape[1]
-    dense_out = dense_pair[:, :, 2 * units :]
     rows_pad = round_up(seq_count)
 
-    terms, fresh_keys, fresh_values = attend(
+    stream_own = lax.optimization_barrier(
+        lax.dynamic_slice_in_dim(stream, offset, feat, 1).astype(jnp.float32)
+    )
+    terms, normed = attend(
         stream,
         norm_gain_mix,
         query_weight,
-        key_weight,
-        value_weight,
         score_offset,
         cache_keys,
         cache_values,
@@ -336,7 +432,7 @@
     attn = sum_lead(exchange(terms, TP))[:seq_count]
 
     residual = (
-        lax.dynamic_slice_in_dim(stream, offset, feat, 1).astype(jnp.float32)
+        stream_own
         + attn.astype(jnp.bfloat16).astype(jnp.float32)
     ).astype(jnp.bfloat16)
     residual_own = residual.astype(jnp.float32)
@@ -355,20 +451,10 @@
     index = (pair_expert * cap + slot).reshape(seq_count, top)
     slot_iota = n_core * lax.broadcasted_iota(jnp.int32, (experts, 1, 1), 0) + core
     dispatch = jnp.sum((index[None, :, :] == slot_iota).astype(jnp.int32), 2).astype(jnp.bfloat16)
-    send = jnp.dot(dispatch, pair, preferred_element_type=jnp.float32).astype(jnp.bfloat16)
 
     part = seq_count // n_core
-    own_rows = lax.dynamic_slice_in_dim(pair, core * part, part, 0)
-    both = seq_count + n_core
-    spare = (round_up(both) - seq_count) // n_core
-    leaving = jnp.concatenate(
-        [
-            jnp.broadcast_to(own_rows[None, :, :feat], (n_ep, part, feat)),
-            jnp.broadcast_to(own_rows[None, :, feat:], (n_ep, part, feat)),
-            jnp.tile(send.reshape(n_ep, n_core, feat), (1, spare, 1)),
-        ],
-        1,
-    )
+    stride = round_up(seq_count + n_core)
+    leaving = pack(core[None].astype(jnp.int32), pair, dispatch, stride)
     arrived = exchange(leaving, "ep")
     arrived, other_gate, other_up, other_down = lax.optimization_barrier(
         (arrived, other_gate, other_up, other_down)
@@ -405,6 +491,8 @@
     home_rows = jnp.concatenate([high, flat - high], 0)
     leaving = spread(arrived, gain_wide, dense_pair, home_rows, n_y, share)
     gathered = exchange(leaving, "y")
+    fresh_keys = across(normed, key_weight).astype(jnp.bfloat16)
+    fresh_values = across(normed, value_weight).astype(jnp.bfloat16)
 
     leaving, sums = run_expert(
         gathered,
@@ -416,24 +504,8 @@
     home_sum = (sums[0] + sums[1])[: seq_count * home_count].reshape(seq_count, home_count)
 
     summed = exchange(leaving, "y")
-    at_act = n_core * n_ep
-    expert_out = sum_lead(summed[:, :at_act]).astype(jnp.bfloat16)
-    acts = summed[:, at_act : at_act + share].reshape(total, units)
-    dense_terms_out = [
-        jnp.dot(acts, dense_out[k], preferred_element_type=jnp.float32)
-        .astype(jnp.bfloat16)
-        .reshape(n_ep, part, feat)
-        for k in range(n_core)
-    ]
-
-    returned = exchange(
-        jnp.concatenate(
-            dense_terms_out
-            + [jnp.moveaxis(expert_out.reshape(n_core, n_ep, feat), 0, 1)] * spare,
-            1,
-        ),
-        "ep",
-    )
+
+    returned = exchange(merge(summed, dense_pair, n_ep, stride, part), "ep")
     inverse_two = lax.rsqrt(home_sum[:, home_count - 1 :] / width + epsilon)
     logits = home_sum[:, : home_count - 1] * inverse_two
     group_exp = jnp.exp(logits[:, :groups])
@@ -446,7 +518,6 @@
     route_gate = group_prob * chosen_exp / jnp.sum(chosen_exp, 1, keepdims=True)
     branch = jax.nn.sigmoid(logits[:, groups + top :])
 
-    stride = returned.shape[1]
     place = lax.broadcasted_iota(jnp.int32, (1, n_ep * stride), 1)
     block, row = place // stride, place % stride
     sequence = lax.broadcasted_iota(jnp.int32, (rows_pad, 1), 0)

time: 138 us -> 139 us (level)
  Pallas kernels: 8.94 us -> 10.9 us
  other arithmetic: 5.58 us -> 3.81 us
  waiting for transfers between devices: 52.4 us -> 50.8 us
    pallas_call x0 -> x2, Pallas kernels: none -> 1.85 us  [the longest x1 0.98 us: merge(): pl.pallas_call(merge_kernel, out_shape=jax.ShapeDtypeStruct((n_ep, stride...]
    concatenate x2 -> x0, other arithmetic: 1.74 us -> none  [the longest x1 0.87 us: local(): jnp.concatenate(dense_terms_out + [jnp.moveaxis(expert_out.reshape(n_core...]
    all_to_all x5, waiting for transfers between devices: 52.4 us -> 50.8 us  [exchange(): return lax.all_to_all(array, axis, 0, 0, tiled=True)]
  transfers between devices with their start and end apart: 8 -> 8, of which waited for: 4 -> 4; matrix products, arithmetic and copies ran while one was open for 5% -> 6% of each run, Pallas kernels for 0% -> 1%
where the time goes in v6:
time: 139 us; the launch traced here: 138 us
  starting transfers between devices  52.8 us (38%)
  waiting for transfers between devices  50.8 us (37%)
  Pallas kernels  10.9 us (8%)
  blocking collectives  10.6 us (8%)
  local copies, waits for them, and re-layouts  5.45 us (4%)
  other arithmetic  3.81 us (3%)
  matrix products  1.96 us (1%)
  between operations  1.68 us (1%)
    all_to_all x5, waiting for transfers between devices, exchange(): return lax.all_to_all(array, axis, 0, 0, tiled=True)  50.8 us
    all_to_all x5, starting transfers between devices, exchange(): return lax.all_to_all(array, axis, 0, 0, tiled=True)  46.3 us
    all_gather x1, blocking collectives, local(): mixture = jnp.sum(lax.all_gather(jnp.concatenate(mixture, 1), 'core'), 0)  6.8 us
    pallas_call x1, Pallas kernels, attend(): pl.pallas_call(attend_kernel, out_shape=(jax.ShapeDtypeStruct((n_tp, rows...  4.05 us
    pallas_call x1, Pallas kernels, run_expert(): pl.pallas_call(expert_kernel, out_shape=(jax.ShapeDtypeStruct((n_y, 2 * n...  3.84 us
  transfers between devices with their start and end apart: 8, of which 4 were waited for; matrix products, arithmetic and copies ran while one was open for 6% of the time, Pallas kernels for 1%

profile of v6, /device:TPU:1, one launch (start us, length us, event | category | flops | bytes accessed | tf_op | source)
XLA Modules:
  0.0 137.9 jit_solution(17112292572407745517)
XLA Ops:
  1.4 4.1 %attend.1 = (bf16[16,24,128]{2,1,0:T(8,128)(2,1)}, bf16[20,2048]{1,0:T(8,128)(2,1)}) custom-call(f32[1]{0:T(128)S(6)} %copy.70.offset_ref, s32[20]{0:T(128)} %lengths_ref.1, bf16[20,2048]{1,0:T(8,128)(2,1)} %stream_ref.1, bf16[2048]{0:T(1024)(128)(2,1)} %gain_ref.2, bf16[64,2048]{1,0:T(8,128)(2,1)} %query_ref.1, bf16[20,64,256]{2,1,0:T(8,128)(2,1)} %keys_hbm.1, ...), custom_call_target="tpu_custom_call" | custom-call | tf_op jit(solution)/shard_map/attend/pallas_call | solution.py:94
  5.4 13.8 %all-to-all-start = ((bf16[16,24,128]{2,1,0:T(8,128)(2,1)}), bf16[16,24,128]{2,1,0:T(8,128)(2,1)S(1)}, u32[]{:S(2)}, u32[]{:S(2)}) async-start(bf16[16,24,128]{2,1,0:T(8,128)(2,1)} %get-tuple-element.11), calls=%async_computation | async-start | bytes 196608 | tf_op jit(solution)/shard_map/all_to_all | solution.py:361
  19.2 2.1 %collective-permute-start = (bf16[2048,256]{1,0:T(8,128)(2,1)S(1)}, bf16[2048,256]{1,0:T(8,128)(2,1)}, u32[]{:S(2)}, u32[]{:S(2)}) collective-permute-start(bf16[2048,256]{1,0:T(8,128)(2,1)S(1)} %bitcast.76), channel_id=1, source_target_pairs={{0,1},{1,0},{2,3},{3,2},{4,5},{5,4},{6,7},{7,6},{8,9},{9,8},{10,11... | collective-permute-start | bytes 3145736 | tf_op jit(solution)/shard_map/ppermute | solution.py:408
  21.4 2.2 %collective-permute-start.1 = (bf16[2048,256]{1,0:T(8,128)(2,1)S(1)}, bf16[2048,256]{1,0:T(8,128)(2,1)}, u32[]{:S(2)}, u32[]{:S(2)}) collective-permute-start(bf16[2048,256]{1,0:T(8,128)(2,1)S(1)} %bitcast.81), channel_id=1, source_target_pairs={{0,1},{1,0},{2,3},{3,2},{4,5},{5,4},{6,7},{7,6},{8,9},{9,8},{10,11... | collective-permute-start | bytes 3145736 | tf_op jit(solution)/shard_map/ppermute | solution.py:409
  23.6 2.1 %collective-permute-start.2 = (bf16[256,2048]{1,0:T(8,128)(2,1)}, bf16[256,2048]{1,0:T(8,128)(2,1)}, u32[]{:S(2)}, u32[]{:S(2)}) collective-permute-start(bf16[256,2048]{1,0:T(8,128)(2,1)} %bitcast.82), channel_id=1, source_target_pairs={{0,1},{1,0},{2,3},{3,2},{4,5},{5,4},{6,7},{7,6},{8,9},{9,8},{10,11... | collective-permute-start | bytes 3145736 | tf_op jit(solution)/shard_map/ppermute | solution.py:410
  25.8 0.7 copy-done.9
  26.8 0.2 select_reduce_fusion
  27.2 0.1 copy.59
  27.3 0.7 dynamic-slice_convert_fusion
  28.0 0.1 fusion.10
  28.3 0.1 fusion
  28.4 0.1 fusion.1
  28.5 0.4 copy-done.8
  29.0 0.1 copy-done.6
  29.1 0.7 constant_dynamic-slice_fusion.1
  29.8 0.8 dynamic_slice.22
  30.6 0.1 copy.60.dispatch_ref
  30.7 0.6 copy-done.2
  31.3 1.9 %all-gather = bf16[256,384]{1,0:T(8,128)(2,1)S(1)} all-gather(bf16[128,384]{1,0:T(8,128)(2,1)S(1)} %pad_maximum_fusion), channel_id=2, replica_groups=mesh['ep'=48,'y'=8,'core'=2] {'core'}, dimensions={0}, use_global_device_ids=true | all-gather | bytes 294912 | tf_op jit(solution)/shard_map/all_gather | solution.py:411
  33.3 0.7 constant_dynamic-slice_fusion
  34.1 1.8 %all_gather.15.pair_ref = bf16[20,256]{1,0:T(8,128)(2,1)S(1)} all-gather(bf16[20,128]{1,0:T(8,128)(2,1)S(1)} %add_convert_fusion.1), channel_id=1, replica_groups=mesh['ep'=48,'y'=8,'core'=2] {'core'}, dimensions={1}, use_global_device_ids=true | all-gather | bytes 15360 | tf_op jit(solution)/shard_map/all_gather | solution.py:439
  35.9 0.9 pack.1
  36.8 12.8 %all-to-all-start.1 = ((bf16[48,24,128]{2,1,0:T(8,128)(2,1)}), bf16[48,24,128]{2,1,0:T(8,128)(2,1)S(1)}, u32[]{:S(2)}, u32[]{:S(2)}) async-start(bf16[48,24,128]{2,1,0:T(8,128)(2,1)} %pack.1), calls=%async_computation.1 | async-start | bytes 589824 | tf_op jit(solution)/shard_map/all_to_all | solution.py:361
  49.6 0.1 fusion.4
  49.8 0.2 select_reduce_fusion.2
  50.2 0.1 multiply_reduce_fusion
  50.5 0.1 reshape.135
  50.7 16.4 %all-to-all-done.1.arrived_ref = bf16[48,24,128]{2,1,0:T(8,128)(2,1)S(1)} async-done(((bf16[48,24,128]{2,1,0:T(8,128)(2,1)}), bf16[48,24,128]{2,1,0:T(8,128)(2,1)S(1)}, u32[]{:S(2)}, u32[]{:S(2)}) %all-to-all-start.1) | async-done | bytes 294944 | tf_op jit(solution)/shard_map/all_to_all | solution.py:361
  67.1 1.1 spread.1
  68.2 6.5 %all-to-all-start.2 = ((bf16[8,112,256]{2,1,0:T(8,128)(2,1)}), bf16[8,112,256]{2,1,0:T(8,128)(2,1)S(1)}, u32[]{:S(2)}, u32[]{:S(2)}) async-start(bf16[8,112,256]{2,1,0:T(8,128)(2,1)} %spread.1), calls=%async_computation.2 | async-start | bytes 917504 | tf_op jit(solution)/shard_map/all_to_all | solution.py:361
  74.7 0.1 fusion.2
  75.0 12.8 %all-to-all-done.2.gathered_ref = bf16[8,112,256]{2,1,0:T(8,128)(2,1)S(1)} async-done(((bf16[8,112,256]{2,1,0:T(8,128)(2,1)}), bf16[8,112,256]{2,1,0:T(8,128)(2,1)S(1)}, u32[]{:S(2)}, u32[]{:S(2)}) %all-to-all-start.2) | async-done | bytes 458784 | tf_op jit(solution)/shard_map/all_to_all | solution.py:361
  87.7 3.8 %expert.1 = (bf16[8,160,128]{2,1,0:T(8,128)(2,1)}, f32[4,256]{1,0:T(4,128)S(1)}) custom-call(bf16[8,112,256]{2,1,0:T(8,128)(2,1)S(1)} %all-to-all-done.2.gathered_ref, bf16[2048]{0:T(1024)(128)(2,1)S(1)} %copy-done.2, bf16[2048,256]{1,0:T(8,128)(2,1)S(1)} %bitcast.77, bf16[2048,256]{1,0:T(8,128)(2,1)} %bitcast.80, bf16[256,2048]{1,0:T(8,128)(2,1)} %bitcast.83, ...), custom_call_target="tpu_custom_call" | custom-call | tf_op jit(solution)/shard_map/expert/pallas_call | solution.py:344
  91.6 4.0 %all-to-all-start.3 = ((bf16[8,160,128]{2,1,0:T(8,128)(2,1)}), bf16[8,160,128]{2,1,0:T(8,128)(2,1)S(1)}, u32[]{:S(2)}, u32[]{:S(2)}) async-start(bf16[8,160,128]{2,1,0:T(8,128)(2,1)} %get-tuple-element.17), calls=%async_computation.3 | async-start | bytes 655360 | tf_op jit(solution)/shard_map/all_to_all | solution.py:361
  95.6 0.8 convolution_convert_fusion
  96.4 0.1 copy-done.5
  96.5 0.8 convolution_convert_fusion.1
  97.4 8.2 %all-to-all-done.3.summed_ref = bf16[8,160,128]{2,1,0:T(8,128)(2,1)S(1)} async-done(((bf16[8,160,128]{2,1,0:T(8,128)(2,1)}), bf16[8,160,128]{2,1,0:T(8,128)(2,1)S(1)}, u32[]{:S(2)}, u32[]{:S(2)}) %all-to-all-start.3) | async-done | bytes 327712 | tf_op jit(solution)/shard_map/all_to_all | solution.py:361
  105.7 1.0 merge.1
  106.6 9.2 %all-to-all-start.4 = ((bf16[48,24,128]{2,1,0:T(8,128)(2,1)}), bf16[48,24,128]{2,1,0:T(8,128)(2,1)S(1)}, u32[]{:S(2)}, u32[]{:S(2)}) async-start(bf16[48,24,128]{2,1,0:T(8,128)(2,1)} %merge.1), calls=%async_computation.4 | async-start | bytes 589824 | tf_op jit(solution)/shard_map/all_to_all | solution.py:361
  115.8 0.2 fusion.27
  116.1 0.2 fusion.29
  116.3 0.2 fusion.30
  116.6 0.2 slice_reduce_fusion.1
  116.8 13.4 %all-to-all-done.4 = bf16[48,24,128]{2,1,0:T(8,128)(2,1)S(1)} async-done(((bf16[48,24,128]{2,1,0:T(8,128)(2,1)}), bf16[48,24,128]{2,1,0:T(8,128)(2,1)S(1)}, u32[]{:S(2)}, u32[]{:S(2)}) %all-to-all-start.4) | async-done | bytes 294944 | tf_op jit(solution)/shard_map/all_to_all | solution.py:361
  130.2 0.3 fusion.42
  130.5 6.8 %all-gather.2 = f32[2,20,256]{2,1,0:T(8,128)S(1)} all-gather(f32[1,20,256]{2,1,0:T(8,128)S(1)} %maximum_bitcast_fusion), channel_id=3, replica_groups=mesh['ep'=48,'y'=8,'core'=2] {'core'}, dimensions={0}, use_global_device_ids=true | all-gather | bytes 61440 | tf_op jit(solution)/shard_map/all_gather | solution.py:541
  137.3 0.6 add_convert_fusion
  (60 shorter events, 1.9 us)
Async XLA Ops:
  0.6 95.0 %copy-start = (bf16[64,2048]{1,0:T(8,128)(2,1)S(1)}, bf16[64,2048]{1,0:T(8,128)(2,1)}, u32[]{:S(2)}) copy-start(bf16[64,2048]{1,0:T(8,128)(2,1)} %param.25) | copy-start | bytes 786436
  1.3 17.9 %copy-start.1 = (bf16[1,2048,256]{2,1,0:T(8,128)(2,1)S(1)}, bf16[1,2048,256]{2,1,0:T(8,128)(2,1)}, u32[]{:S(2)}) copy-start(bf16[1,2048,256]{2,1,0:T(8,128)(2,1)} %param.35) | copy-start | bytes 3145732
  1.3 20.0 %copy-start.3 = (bf16[1,2048,256]{2,1,0:T(8,128)(2,1)S(1)}, bf16[1,2048,256]{2,1,0:T(8,128)(2,1)}, u32[]{:S(2)}) copy-start(bf16[1,2048,256]{2,1,0:T(8,128)(2,1)} %param.36) | copy-start | bytes 3145732
  5.4 28.6 %all-to-all-start = ((bf16[16,24,128]{2,1,0:T(8,128)(2,1)}), bf16[16,24,128]{2,1,0:T(8,128)(2,1)S(1)}, u32[]{:S(2)}, u32[]{:S(2)}) async-start(bf16[16,24,128]{2,1,0:T(8,128)(2,1)} %get-tuple-element.11), calls=%async_computation | async-start | bytes 196608 | tf_op jit(solution)/shard_map/all_to_all | solution.py:361
  19.2 31.4 %collective-permute-start = (bf16[2048,256]{1,0:T(8,128)(2,1)S(1)}, bf16[2048,256]{1,0:T(8,128)(2,1)}, u32[]{:S(2)}, u32[]{:S(2)}) collective-permute-start(bf16[2048,256]{1,0:T(8,128)(2,1)S(1)} %bitcast.76), channel_id=1, source_target_pairs={{0,1},{1,0},{2,3},{3,2},{4,5},{5,4},{6,7},{7,6},{8,9},{9,8},{10,11... | collective-permute-start | bytes 3145736 | tf_op jit(solution)/shard_map/ppermute | solution.py:408
  21.4 29.3 %collective-permute-start.1 = (bf16[2048,256]{1,0:T(8,128)(2,1)S(1)}, bf16[2048,256]{1,0:T(8,128)(2,1)}, u32[]{:S(2)}, u32[]{:S(2)}) collective-permute-start(bf16[2048,256]{1,0:T(8,128)(2,1)S(1)} %bitcast.81), channel_id=1, source_target_pairs={{0,1},{1,0},{2,3},{3,2},{4,5},{5,4},{6,7},{7,6},{8,9},{9,8},{10,11... | collective-permute-start | bytes 3145736 | tf_op jit(solution)/shard_map/ppermute | solution.py:409
  23.6 27.1 %collective-permute-start.2 = (bf16[256,2048]{1,0:T(8,128)(2,1)}, bf16[256,2048]{1,0:T(8,128)(2,1)}, u32[]{:S(2)}, u32[]{:S(2)}) collective-permute-start(bf16[256,2048]{1,0:T(8,128)(2,1)} %bitcast.82), channel_id=1, source_target_pairs={{0,1},{1,0},{2,3},{3,2},{4,5},{5,4},{6,7},{7,6},{8,9},{9,8},{10,11... | collective-permute-start | bytes 3145736 | tf_op jit(solution)/shard_map/ppermute | solution.py:410
  25.8 0.7 copy-start.9
  28.2 0.8 copy-start.8
  28.3 0.8 copy-start.6
  28.3 0.8 copy-start.7
  30.6 0.7 copy-start.2
  36.8 30.3 %all-to-all-start.1 = ((bf16[48,24,128]{2,1,0:T(8,128)(2,1)}), bf16[48,24,128]{2,1,0:T(8,128)(2,1)S(1)}, u32[]{:S(2)}, u32[]{:S(2)}) async-start(bf16[48,24,128]{2,1,0:T(8,128)(2,1)} %pack.1), calls=%async_computation.1 | async-start | bytes 589824 | tf_op jit(solution)/shard_map/all_to_all | solution.py:361
  68.2 19.5 %all-to-all-start.2 = ((bf16[8,112,256]{2,1,0:T(8,128)(2,1)}), bf16[8,112,256]{2,1,0:T(8,128)(2,1)S(1)}, u32[]{:S(2)}, u32[]{:S(2)}) async-start(bf16[8,112,256]{2,1,0:T(8,128)(2,1)} %spread.1), calls=%async_computation.2 | async-start | bytes 917504 | tf_op jit(solution)/shard_map/all_to_all | solution.py:361
  91.6 4.0 %copy-start.4 = (bf16[20,2048]{1,0:T(8,128)(2,1)S(1)}, bf16[20,2048]{1,0:T(8,128)(2,1)}, u32[]{:S(2)}) copy-start(bf16[20,2048]{1,0:T(8,128)(2,1)} %get-tuple-element.18) | copy-start | bytes 245764
  91.6 14.1 %all-to-all-start.3 = ((bf16[8,160,128]{2,1,0:T(8,128)(2,1)}), bf16[8,160,128]{2,1,0:T(8,128)(2,1)S(1)}, u32[]{:S(2)}, u32[]{:S(2)}) async-start(bf16[8,160,128]{2,1,0:T(8,128)(2,1)} %get-tuple-element.17), calls=%async_computation.3 | async-start | bytes 655360 | tf_op jit(solution)/shard_map/all_to_all | solution.py:361
  95.6 0.9 copy-start.5
  106.6 23.5 %all-to-all-start.4 = ((bf16[48,24,128]{2,1,0:T(8,128)(2,1)}), bf16[48,24,128]{2,1,0:T(8,128)(2,1)S(1)}, u32[]{:S(2)}, u32[]{:S(2)}) async-start(bf16[48,24,128]{2,1,0:T(8,128)(2,1)} %merge.1), calls=%async_computation.4 | async-start | bytes 589824 | tf_op jit(solution)/shard_map/all_to_all | solution.py:361

commit v7 on v6

--- a/solution.py
+++ b/solution.py
@@ -19,14 +19,17 @@
 def attend_kernel(
     offset_ref,
     lengths_ref,
-    stream_ref,
-    gain_ref,
-    query_ref,
+    stream_hbm,
+    gain_hbm,
+    query_hbm,
     keys_hbm,
     values_hbm,
     out_weight_hbm,
     terms_ref,
     normed_ref,
+    stream_ref,
+    gain_ref,
+    query_ref,
     keys_ref,
     values_ref,
     out_weight_ref,
@@ -36,6 +39,9 @@
         pltpu.make_async_copy(source, target, sems.at[k])
         for k, (source, target) in enumerate(
             (
+                (stream_hbm, stream_ref),
+                (gain_hbm, gain_ref),
+                (query_hbm, query_ref),
                 (keys_hbm, keys_ref),
                 (values_hbm, values_ref),
                 (out_weight_hbm, out_weight_ref),
@@ -44,6 +50,8 @@
     ]
     for copy in copies:
         copy.start()
+    copies[0].wait()
+    copies[1].wait()
     count, _ = stream_ref.shape
     head_size, cache_len = keys_ref.shape[1:]
     n_blocks, rows, feat = terms_ref.shape
@@ -51,6 +59,7 @@
     inverse = lax.rsqrt(jnp.mean(stream_f * stream_f, -1, keepdims=True) + epsilon)
     normed = (stream_f * inverse * gain_ref[...].astype(jnp.float32)[None]).astype(jnp.bfloat16)
     normed_ref[...] = normed
+    copies[2].wait()
     queries = across(normed, query_ref[...])
     queries = jnp.concatenate([queries, jnp.zeros((rows - count, head_size), jnp.float32)], 0)
     queries = queries.astype(jnp.bfloat16)
@@ -59,7 +68,7 @@
         lax.broadcasted_iota(jnp.int32, (cache_len, cache_len), 0)
         > lax.broadcasted_iota(jnp.int32, (cache_len, cache_len), 1)
     ).astype(jnp.float32)
-    copies[0].wait()
+    copies[3].wait()
     scores = jnp.zeros((rows, cache_len), jnp.float32)
     for s in range(count):
         each = jnp.dot(queries, keys_ref[s], preferred_element_type=jnp.float32)
@@ -76,11 +85,11 @@
     )
     weights = jnp.where(inside, jnp.exp(jnp.minimum(scores, 0.0) - tail + remain), 0.0)
     weights = weights.astype(jnp.bfloat16)
-    copies[1].wait()
+    copies[4].wait()
     heads_out = jnp.zeros((rows, head_size), jnp.float32)
     for s in range(count):
         heads_out = jnp.where(row == s, across(weights, values_ref[s]), heads_out)
-    copies[2].wait()
+    copies[5].wait()
     terms = jnp.dot(
         heads_out.astype(jnp.bfloat16), out_weight_ref[...], preferred_element_type=jnp.float32
     ).astype(jnp.bfloat16)
@@ -98,13 +107,14 @@
             jax.ShapeDtypeStruct((count, width), jnp.bfloat16),
         ),
         in_specs=[pl.BlockSpec(memory_space=pltpu.SMEM)] * 2
-        + [whole] * 3
-        + [pl.BlockSpec(memory_space=pltpu.HBM)] * 3,
+        + [pl.BlockSpec(memory_space=pltpu.HBM)] * 6,
         out_specs=(whole, whole),
         scratch_shapes=[
-            pltpu.VMEM(each.shape, jnp.bfloat16) for each in (keys, values, out_weight)
+            pltpu.VMEM(each.shape, jnp.bfloat16)
+            for each in (stream, gain, query_w, keys, values, out_weight)
         ]
-        + [pltpu.SemaphoreType.DMA((3,))],
+        + [pltpu.SemaphoreType.DMA((6,))],
+        compiler_params=pltpu.CompilerParams(vmem_limit_bytes=67_043_328),
         name="attend",
     )(offset, lengths, stream, gain, query_w, keys, values, out_weight)
 

time: 139 us -> 139 us (level)
  no operation moved by 1% of the time
where the time goes in v7:
time: 139 us; the launch traced here: 138 us
  starting transfers between devices  52.7 us (38%)
  waiting for transfers between devices  50.8 us (37%)
  Pallas kernels  10.6 us (8%)
  blocking collectives  10.6 us (8%)
  local copies, waits for them, and re-layouts  5.45 us (4%)
  other arithmetic  3.81 us (3%)
  matrix products  1.96 us (1%)
  between operations  1.64 us (1%)
    all_to_all x5, waiting for transfers between devices, exchange(): return lax.all_to_all(array, axis, 0, 0, tiled=True)  50.8 us
    all_to_all x5, starting transfers between devices, exchange(): return lax.all_to_all(array, axis, 0, 0, tiled=True)  46.3 us
    all_gather x1, blocking collectives, local(): mixture = jnp.sum(lax.all_gather(jnp.concatenate(mixture, 1), 'core'), 0)  6.79 us
    pallas_call x1, Pallas kernels, run_expert(): pl.pallas_call(expert_kernel, out_shape=(jax.ShapeDtypeStruct((n_y, 2 * n...  3.84 us
    pallas_call x1, Pallas kernels, attend(): pl.pallas_call(attend_kernel, out_shape=(jax.ShapeDtypeStruct((n_tp, rows...  3.78 us
  transfers between devices with their start and end apart: 8, of which 4 were waited for; matrix products, arithmetic and copies ran while one was open for 6% of the time, Pallas kernels for 1%

profile of v7, /device:TPU:1, one launch (start us, length us, event | category | flops | bytes accessed | tf_op | source)
XLA Modules:
  0.0 137.6 jit_solution(9107096743212890958)
XLA Ops:
  1.3 3.8 %attend.1 = (bf16[16,24,128]{2,1,0:T(8,128)(2,1)}, bf16[20,2048]{1,0:T(8,128)(2,1)}) custom-call(f32[1]{0:T(128)S(6)} %copy.70.offset_ref, s32[20]{0:T(128)} %lengths_ref.1, bf16[20,2048]{1,0:T(8,128)(2,1)} %stream_hbm.1, bf16[2048]{0:T(1024)(128)(2,1)} %gain_hbm.1, bf16[64,2048]{1,0:T(8,128)(2,1)} %query_hbm.1, bf16[20,64,256]{2,1,0:T(8,128)(2,1)} %keys_hbm.1, ...), custom_call_target="tpu_custom_call" | custom-call | tf_op jit(solution)/shard_map/attend/pallas_call | solution.py:103
  5.1 13.8 %all-to-all-start = ((bf16[16,24,128]{2,1,0:T(8,128)(2,1)}), bf16[16,24,128]{2,1,0:T(8,128)(2,1)S(1)}, u32[]{:S(2)}, u32[]{:S(2)}) async-start(bf16[16,24,128]{2,1,0:T(8,128)(2,1)} %get-tuple-element.11), calls=%async_computation | async-start | bytes 196608 | tf_op jit(solution)/shard_map/all_to_all | solution.py:371
  18.8 2.1 %collective-permute-start = (bf16[2048,256]{1,0:T(8,128)(2,1)}, bf16[2048,256]{1,0:T(8,128)(2,1)S(1)}, u32[]{:S(2)}, u32[]{:S(2)}) collective-permute-start(bf16[2048,256]{1,0:T(8,128)(2,1)} %bitcast.76), channel_id=1, source_target_pairs={{0,1},{1,0},{2,3},{3,2},{4,5},{5,4},{6,7},{7,6},{8,9},{9,8},{10,11... | collective-permute-start | bytes 3145736 | tf_op jit(solution)/shard_map/ppermute | solution.py:418
  21.0 2.2 %collective-permute-start.1 = (bf16[2048,256]{1,0:T(8,128)(2,1)}, bf16[2048,256]{1,0:T(8,128)(2,1)S(1)}, u32[]{:S(2)}, u32[]{:S(2)}) collective-permute-start(bf16[2048,256]{1,0:T(8,128)(2,1)} %bitcast.80), channel_id=1, source_target_pairs={{0,1},{1,0},{2,3},{3,2},{4,5},{5,4},{6,7},{7,6},{8,9},{9,8},{10,11... | collective-permute-start | bytes 3145736 | tf_op jit(solution)/shard_map/ppermute | solution.py:419
  23.2 2.1 %collective-permute-start.2 = (bf16[256,2048]{1,0:T(8,128)(2,1)}, bf16[256,2048]{1,0:T(8,128)(2,1)}, u32[]{:S(2)}, u32[]{:S(2)}) collective-permute-start(bf16[256,2048]{1,0:T(8,128)(2,1)} %bitcast.82), channel_id=1, source_target_pairs={{0,1},{1,0},{2,3},{3,2},{4,5},{5,4},{6,7},{7,6},{8,9},{9,8},{10,11... | collective-permute-start | bytes 3145736 | tf_op jit(solution)/shard_map/ppermute | solution.py:420
  25.4 0.7 copy-done.10
  26.4 0.2 select_reduce_fusion
  26.8 0.1 copy.59
  26.9 0.7 dynamic-slice_convert_fusion
  27.6 0.1 fusion.10
  28.0 0.1 fusion
  28.1 0.1 fusion.1
  28.2 0.4 copy-done.9
  28.6 0.1 copy-done.7
  28.7 0.7 constant_dynamic-slice_fusion.1
  29.4 0.8 dynamic_slice.22
  30.2 0.1 copy.60.dispatch_ref
  30.3 0.6 copy-done.1
  31.0 1.9 %all-gather = bf16[256,384]{1,0:T(8,128)(2,1)S(1)} all-gather(bf16[128,384]{1,0:T(8,128)(2,1)S(1)} %pad_maximum_fusion), channel_id=2, replica_groups=mesh['ep'=48,'y'=8,'core'=2] {'core'}, dimensions={0}, use_global_device_ids=true | all-gather | bytes 294912 | tf_op jit(solution)/shard_map/all_gather | solution.py:421
  32.9 0.7 constant_dynamic-slice_fusion
  33.7 1.8 %all_gather.15.pair_ref = bf16[20,256]{1,0:T(8,128)(2,1)S(1)} all-gather(bf16[20,128]{1,0:T(8,128)(2,1)S(1)} %add_convert_fusion.1), channel_id=1, replica_groups=mesh['ep'=48,'y'=8,'core'=2] {'core'}, dimensions={1}, use_global_device_ids=true | all-gather | bytes 15360 | tf_op jit(solution)/shard_map/all_gather | solution.py:449
  35.5 0.9 pack.1
  36.4 12.8 %all-to-all-start.1 = ((bf16[48,24,128]{2,1,0:T(8,128)(2,1)}), bf16[48,24,128]{2,1,0:T(8,128)(2,1)S(1)}, u32[]{:S(2)}, u32[]{:S(2)}) async-start(bf16[48,24,128]{2,1,0:T(8,128)(2,1)} %pack.1), calls=%async_computation.1 | async-start | bytes 589824 | tf_op jit(solution)/shard_map/all_to_all | solution.py:371
  49.2 0.1 fusion.4
  49.4 0.2 select_reduce_fusion.2
  49.8 0.1 multiply_reduce_fusion
  50.1 0.1 reshape.135
  50.3 16.4 %all-to-all-done.1.arrived_ref = bf16[48,24,128]{2,1,0:T(8,128)(2,1)S(1)} async-done(((bf16[48,24,128]{2,1,0:T(8,128)(2,1)}), bf16[48,24,128]{2,1,0:T(8,128)(2,1)S(1)}, u32[]{:S(2)}, u32[]{:S(2)}) %all-to-all-start.1) | async-done | bytes 294944 | tf_op jit(solution)/shard_map/all_to_all | solution.py:371
  66.7 1.1 spread.1
  67.8 6.5 %all-to-all-start.2 = ((bf16[8,112,256]{2,1,0:T(8,128)(2,1)}), bf16[8,112,256]{2,1,0:T(8,128)(2,1)S(1)}, u32[]{:S(2)}, u32[]{:S(2)}) async-start(bf16[8,112,256]{2,1,0:T(8,128)(2,1)} %spread.1), calls=%async_computation.2 | async-start | bytes 917504 | tf_op jit(solution)/shard_map/all_to_all | solution.py:371
  74.4 0.1 fusion.2
  74.6 12.7 %all-to-all-done.2.gathered_ref = bf16[8,112,256]{2,1,0:T(8,128)(2,1)S(1)} async-done(((bf16[8,112,256]{2,1,0:T(8,128)(2,1)}), bf16[8,112,256]{2,1,0:T(8,128)(2,1)S(1)}, u32[]{:S(2)}, u32[]{:S(2)}) %all-to-all-start.2) | async-done | bytes 458784 | tf_op jit(solution)/shard_map/all_to_all | solution.py:371
  87.4 3.8 %expert.1 = (bf16[8,160,128]{2,1,0:T(8,128)(2,1)}, f32[4,256]{1,0:T(4,128)S(1)}) custom-call(bf16[8,112,256]{2,1,0:T(8,128)(2,1)S(1)} %all-to-all-done.2.gathered_ref, bf16[2048]{0:T(1024)(128)(2,1)S(1)} %copy-done.1, bf16[2048,256]{1,0:T(8,128)(2,1)S(1)} %bitcast.77, bf16[2048,256]{1,0:T(8,128)(2,1)} %bitcast.81, bf16[256,2048]{1,0:T(8,128)(2,1)} %bitcast.83, ...), custom_call_target="tpu_custom_call" | custom-call | tf_op jit(solution)/shard_map/expert/pallas_call | solution.py:354
  91.2 4.0 %all-to-all-start.3 = ((bf16[8,160,128]{2,1,0:T(8,128)(2,1)}), bf16[8,160,128]{2,1,0:T(8,128)(2,1)S(1)}, u32[]{:S(2)}, u32[]{:S(2)}) async-start(bf16[8,160,128]{2,1,0:T(8,128)(2,1)} %get-tuple-element.17), calls=%async_computation.3 | async-start | bytes 655360 | tf_op jit(solution)/shard_map/all_to_all | solution.py:371
  95.2 0.8 convolution_convert_fusion
  96.0 0.1 copy-done.6
  96.2 0.8 convolution_convert_fusion.1
  97.1 8.2 %all-to-all-done.3.summed_ref = bf16[8,160,128]{2,1,0:T(8,128)(2,1)S(1)} async-done(((bf16[8,160,128]{2,1,0:T(8,128)(2,1)}), bf16[8,160,128]{2,1,0:T(8,128)(2,1)S(1)}, u32[]{:S(2)}, u32[]{:S(2)}) %all-to-all-start.3) | async-done | bytes 327712 | tf_op jit(solution)/shard_map/all_to_all | solution.py:371
  105.3 1.0 merge.1
  106.3 9.2 %all-to-all-start.4 = ((bf16[48,24,128]{2,1,0:T(8,128)(2,1)}), bf16[48,24,128]{2,1,0:T(8,128)(2,1)S(1)}, u32[]{:S(2)}, u32[]{:S(2)}) async-start(bf16[48,24,128]{2,1,0:T(8,128)(2,1)} %merge.1), calls=%async_computation.4 | async-start | bytes 589824 | tf_op jit(solution)/shard_map/all_to_all | solution.py:371
  115.5 0.2 fusion.27
  115.7 0.2 fusion.29
  115.9 0.2 fusion.30
  116.2 0.2 slice_reduce_fusion.1
  116.4 13.4 %all-to-all-done.4 = bf16[48,24,128]{2,1,0:T(8,128)(2,1)S(1)} async-done(((bf16[48,24,128]{2,1,0:T(8,128)(2,1)}), bf16[48,24,128]{2,1,0:T(8,128)(2,1)S(1)}, u32[]{:S(2)}, u32[]{:S(2)}) %all-to-all-start.4) | async-done | bytes 294944 | tf_op jit(solution)/shard_map/all_to_all | solution.py:371
  129.8 0.3 fusion.42
  130.2 6.8 %all-gather.2 = f32[2,20,256]{2,1,0:T(8,128)S(1)} all-gather(f32[1,20,256]{2,1,0:T(8,128)S(1)} %maximum_bitcast_fusion), channel_id=3, replica_groups=mesh['ep'=48,'y'=8,'core'=2] {'core'}, dimensions={0}, use_global_device_ids=true | all-gather | bytes 61440 | tf_op jit(solution)/shard_map/all_gather | solution.py:551
  137.0 0.6 add_convert_fusion
  (62 shorter events, 1.9 us)
Async XLA Ops:
  5.1 28.6 %all-to-all-start = ((bf16[16,24,128]{2,1,0:T(8,128)(2,1)}), bf16[16,24,128]{2,1,0:T(8,128)(2,1)S(1)}, u32[]{:S(2)}, u32[]{:S(2)}) async-start(bf16[16,24,128]{2,1,0:T(8,128)(2,1)} %get-tuple-element.11), calls=%async_computation | async-start | bytes 196608 | tf_op jit(solution)/shard_map/all_to_all | solution.py:371
  18.8 31.4 %collective-permute-start = (bf16[2048,256]{1,0:T(8,128)(2,1)}, bf16[2048,256]{1,0:T(8,128)(2,1)S(1)}, u32[]{:S(2)}, u32[]{:S(2)}) collective-permute-start(bf16[2048,256]{1,0:T(8,128)(2,1)} %bitcast.76), channel_id=1, source_target_pairs={{0,1},{1,0},{2,3},{3,2},{4,5},{5,4},{6,7},{7,6},{8,9},{9,8},{10,11... | collective-permute-start | bytes 3145736 | tf_op jit(solution)/shard_map/ppermute | solution.py:418
  21.0 29.3 %collective-permute-start.1 = (bf16[2048,256]{1,0:T(8,128)(2,1)}, bf16[2048,256]{1,0:T(8,128)(2,1)S(1)}, u32[]{:S(2)}, u32[]{:S(2)}) collective-permute-start(bf16[2048,256]{1,0:T(8,128)(2,1)} %bitcast.80), channel_id=1, source_target_pairs={{0,1},{1,0},{2,3},{3,2},{4,5},{5,4},{6,7},{7,6},{8,9},{9,8},{10,11... | collective-permute-start | bytes 3145736 | tf_op jit(solution)/shard_map/ppermute | solution.py:419
  23.2 27.1 %collective-permute-start.2 = (bf16[256,2048]{1,0:T(8,128)(2,1)}, bf16[256,2048]{1,0:T(8,128)(2,1)}, u32[]{:S(2)}, u32[]{:S(2)}) collective-permute-start(bf16[256,2048]{1,0:T(8,128)(2,1)} %bitcast.82), channel_id=1, source_target_pairs={{0,1},{1,0},{2,3},{3,2},{4,5},{5,4},{6,7},{7,6},{8,9},{9,8},{10,11... | collective-permute-start | bytes 3145736 | tf_op jit(solution)/shard_map/ppermute | solution.py:420
  25.4 0.7 copy-start.10
  27.8 0.8 copy-start.9
  27.9 0.8 copy-start.7
  27.9 0.8 copy-start.8
  30.2 0.7 copy-start.1
  36.4 30.3 %all-to-all-start.1 = ((bf16[48,24,128]{2,1,0:T(8,128)(2,1)}), bf16[48,24,128]{2,1,0:T(8,128)(2,1)S(1)}, u32[]{:S(2)}, u32[]{:S(2)}) async-start(bf16[48,24,128]{2,1,0:T(8,128)(2,1)} %pack.1), calls=%async_computation.1 | async-start | bytes 589824 | tf_op jit(solution)/shard_map/all_to_all | solution.py:371
  50.2 24.4 %copy-start.2 = (bf16[2048,256]{1,0:T(8,128)(2,1)}, bf16[2048,256]{1,0:T(8,128)(2,1)S(1)}, u32[]{:S(2)}) copy-start(bf16[2048,256]{1,0:T(8,128)(2,1)S(1)} %collective-permute-done.other_gate_hbm) | copy-start | bytes 3145732
  50.3 16.4 %copy-start.3 = (bf16[2048,256]{1,0:T(8,128)(2,1)}, bf16[2048,256]{1,0:T(8,128)(2,1)S(1)}, u32[]{:S(2)}) copy-start(bf16[2048,256]{1,0:T(8,128)(2,1)S(1)} %collective-permute-done.1.other_up_hbm) | copy-start | bytes 3145732
  66.7 20.7 %copy-start = (bf16[1,2048,256]{2,1,0:T(8,128)(2,1)S(1)}, bf16[1,2048,256]{2,1,0:T(8,128)(2,1)}, u32[]{:S(2)}) copy-start(bf16[1,2048,256]{2,1,0:T(8,128)(2,1)} %param.35) | copy-start | bytes 3145732
  67.8 19.5 %all-to-all-start.2 = ((bf16[8,112,256]{2,1,0:T(8,128)(2,1)}), bf16[8,112,256]{2,1,0:T(8,128)(2,1)S(1)}, u32[]{:S(2)}, u32[]{:S(2)}) async-start(bf16[8,112,256]{2,1,0:T(8,128)(2,1)} %spread.1), calls=%async_computation.2 | async-start | bytes 917504 | tf_op jit(solution)/shard_map/all_to_all | solution.py:371
  91.2 4.0 %copy-start.4 = (bf16[20,2048]{1,0:T(8,128)(2,1)S(1)}, bf16[20,2048]{1,0:T(8,128)(2,1)}, u32[]{:S(2)}) copy-start(bf16[20,2048]{1,0:T(8,128)(2,1)} %get-tuple-element.18) | copy-start | bytes 245764
  91.2 4.0 %copy-start.5 = (bf16[64,2048]{1,0:T(8,128)(2,1)S(1)}, bf16[64,2048]{1,0:T(8,128)(2,1)}, u32[]{:S(2)}) copy-start(bf16[64,2048]{1,0:T(8,128)(2,1)} %param.25) | copy-start | bytes 786436
  91.2 14.1 %all-to-all-start.3 = ((bf16[8,160,128]{2,1,0:T(8,128)(2,1)}), bf16[8,160,128]{2,1,0:T(8,128)(2,1)S(1)}, u32[]{:S(2)}, u32[]{:S(2)}) async-start(bf16[8,160,128]{2,1,0:T(8,128)(2,1)} %get-tuple-element.17), calls=%async_computation.3 | async-start | bytes 655360 | tf_op jit(solution)/shard_map/all_to_all | solution.py:371
  95.2 0.9 copy-start.6
  106.3 23.5 %all-to-all-start.4 = ((bf16[48,24,128]{2,1,0:T(8,128)(2,1)}), bf16[48,24,128]{2,1,0:T(8,128)(2,1)S(1)}, u32[]{:S(2)}, u32[]{:S(2)}) async-start(bf16[48,24,128]{2,1,0:T(8,128)(2,1)} %merge.1), calls=%async_computation.4 | async-start | bytes 589824 | tf_op jit(solution)/shard_map/all_to_all | solution.py:371
